TPU v7x, 128 devices: a whole 4x4x4 slice. The times are simulated.
128 devices in a mesh: rep: 2 (over z_hi), fs: 32 (over z_lo, y, x), tp: 2 (over core).
Axes of the slice: x: 4, y: 4, z: 4 (z_hi: 2, z_lo: 2; z = z_hi * 2 + z_lo), core: 2. Of those that a mesh axis runs over, the one named last changes fastest.
Arguments:
- tokens: bfloat16 [49152, 2048], P(('rep', 'fs', 'tp')), may hold values from -6 to 6
- outer_weight: float32 [2048, 1536], P('fs', 'tp'), may hold values from -0.125 to 0.125
- inner_weight: float32 [2048, 1536], P('fs', 'tp'), may hold values from -0.125 to 0.125
- value_weight: float32 [2048, 1536], P('fs', 'tp'), may hold values from -0.125 to 0.125
- conv_taps: float32 [3, 1536], P(None, 'tp'), may hold values from -3 to 3
- mix_out: float32 [1536, 2048], P('tp', 'fs'), may hold values from -0.15625 to 0.15625
- norm_first: float32 [2048], replicated, may hold values from 0.1 to 1.9
- up_weight: float32 [2048, 4096], P('fs', 'tp'), may hold values from -0.125 to 0.125
- down_weight: float32 [4096, 2048], P('tp', 'fs'), may hold values from -0.09375 to 0.09375
- norm_second: float32 [2048], replicated, may hold values from 0.1 to 1.9
Outputs:
- encoded: bfloat16 [49152, 2048], P(('rep', 'fs', 'tp'))
All inputs are finite; a program needn't handle non-finite values.
Results may differ from a plain program's by a relative error of at most 0.015.
Values may be sent and summed in bfloat16 or wider, within the bound.
No kernel may reach another device: no remote copies, remote signals or barrier semaphores. Data moves between devices by JAX's collectives and lax.ppermute only.
A program may use at most 128 MiB of HBM per device.

v0:
```python
import functools

import jax
import jax.numpy as jnp
from jax import lax
from jax.experimental import pallas as pl
from jax.experimental.pallas import tpu as pltpu
from jax.sharding import Mesh
from jax.sharding import PartitionSpec as P


SEQ = 128
D = 2048
ROWS = 32
FS = ("fs_0", "fs_1", "fs_2")
REP_FS_TP = ("rep", "fs_0", "fs_1", "fs_2", "tp")
ORDERS = ("zxy", "xyz", "yzx")
CHANNELS = 256
HIDDEN = (768, 640, 640)


residual_scale = 2.0**0.25
norm_epsilon = 1e-05
bf = jnp.bfloat16
HBM = pl.BlockSpec(memory_space=pltpu.HBM)
VMEM = pl.BlockSpec(memory_space=pltpu.VMEM)
PARAMS = pltpu.CompilerParams(vmem_limit_bytes=48 * 1024 * 1024)


def in_hbm(arrays):
    return [pltpu.with_memory_space_constraint(a, pltpu.HBM) for a in arrays]


def stage_widths(part):
    return [4 * CHANNELS, 2 * HIDDEN[part]]


def position(axis):
    if axis == "z":
        return lax.axis_index("rep") * 2 + lax.axis_index("fs_0")
    return lax.axis_index({"y": "fs_1", "x": "fs_2"}[axis])


def source(axis, step):
    way = 2 * lax.axis_index("tp") - 1
    return (position(axis) + 4 + way * step) & 3


def ring_pairs(axis, step):
    at = "zyx".index(axis)
    pairs = []
    for z in range(4):
        for y in range(4):
            for x in range(4):
                for core in range(2):
                    to = [z, y, x]
                    to[at] = (to[at] + (step if core == 0 else 4 - step)) % 4
                    start = ((z * 4 + y) * 4 + x) * 2 + core
                    pairs.append((start, ((to[0] * 4 + to[1]) * 4 + to[2]) * 2 + core))
    return pairs


def moved(block, axis, step):
    return lax.ppermute(block, REP_FS_TP, ring_pairs(axis, step))


def around(block, axis):
    near, back = moved(block, axis, 1), moved(block, axis, 3)
    return [block, near, moved(near, axis, 1), back]


def swapped(x):
    return lax.ppermute(x, "tp", [(0, 1), (1, 0)])


def finish(copies):
    for copy in copies:
        copy.start()
    for copy in copies:
        copy.wait()


def pieces_kernel(*refs):
    weights, outs, held, sems = refs[:6], refs[6:9], refs[9:15], refs[15]
    rows = pl.ds(lax.axis_index("rep") * ROWS, ROWS)
    finish(
        [
            pltpu.make_async_copy(w.at[rows], h, sems.at[i])
            for i, (w, h) in enumerate(zip(weights, held))
        ]
    )
    outer, inner, value, mix, up, down = held
    for part, out in enumerate(outs):
        at = 0
        for w in (outer, inner, value, mix):
            out[:, at : at + CHANNELS] = w[:, part * CHANNELS : (part + 1) * CHANNELS].astype(bf)
            at += CHANNELS
        start, n = sum(HIDDEN[:part]), HIDDEN[part]
        for w in (up, down):
            out[:, at : at + n] = w[:, start : start + n].astype(bf)
            at += n


def pieces(*weights):
    return pl.pallas_call(
        pieces_kernel,
        out_shape=[jax.ShapeDtypeStruct((ROWS, sum(stage_widths(c))), bf) for c in range(3)],
        in_specs=[HBM] * 6,
        out_specs=[VMEM] * 3,
        scratch_shapes=[pltpu.VMEM((ROWS, w.shape[1]), jnp.float32) for w in weights]
        + [pltpu.SemaphoreType.DMA((6,))],
        compiler_params=PARAMS,
    )(*in_hbm(weights))


def place_kernel(axis, widths, *refs):
    parts, outs, sems = refs[:4], refs[4:-1], refs[-1]
    copies = []
    for k, part in enumerate(parts):
        at = 0
        for i, width in enumerate(widths):
            copies.append(
                pltpu.make_async_copy(
                    part.at[..., pl.ds(at, width)],
                    outs[i].at[source(axis, k)],
                    sems.at[len(copies)],
                )
            )
            at += width
    finish(copies)


def placed(parts, axis, widths):
    lead = parts[0].shape[:-1]
    return pl.pallas_call(
        functools.partial(place_kernel, axis, widths),
        out_shape=[pltpu.HBM((4, *lead, w), bf) for w in widths],
        in_specs=[HBM] * 4,
        out_specs=[HBM] * len(widths),
        scratch_shapes=[pltpu.SemaphoreType.DMA((4 * len(widths),))],
        compiler_params=PARAMS,
    )(*parts)


def fill(order, blocks, start, width, whole, at, sems, used):
    copies = []

    def add(src, dst):
        copies.append(pltpu.make_async_copy(src, dst, sems.at[used + len(copies)]))

    cs, cd = pl.ds(start, width), pl.ds(at, width)
    for k, block in enumerate(blocks):
        p = source(order[2], k)
        if order == "xyz":
            add(block.at[:, :, :, cs], whole.at[p & 1, :, :, p >> 1, :, cd])
        else:
            for z in range(4):
                if order == "zxy":
                    add(block.at[:, z, :, cs], whole.at[z & 1, p, :, z >> 1, :, cd])
                else:
                    add(block.at[z, :, :, cs], whole.at[z & 1, :, p, z >> 1, :, cd])
    return copies


def whole_scratch(width):
    return pltpu.VMEM((2, 4, 4, 2, ROWS, width), bf)


def dot(a, b):
    return jnp.dot(a, b, preferred_element_type=jnp.float32)


def dot_t(a, b):
    return lax.dot_general(a, b, (((1,), (1,)), ((), ())), preferred_element_type=jnp.float32)


def both_tokens(own, other, x, sems, used):
    half = own.shape[0]
    return [
        pltpu.make_async_copy(own, x.at[pl.ds(0, half)], sems.at[used]),
        pltpu.make_async_copy(other, x.at[pl.ds(half, half)], sems.at[used + 1]),
    ]


def mixer_kernel(order, own, other, taps, *refs):
    blocks, mixed, x, w, sems = refs[:4], refs[4], refs[5], refs[6], refs[7]
    copies = both_tokens(own, other, x, sems, 0)
    copies += fill(order, blocks, 0, 3 * CHANNELS, w, 0, sems, 2)
    finish(copies)

    def product(i):
        return dot(x[...], w[..., i * CHANNELS : (i + 1) * CHANNELS].reshape(D, CHANNELS))

    gated = product(1) * product(2)
    place = lax.broadcasted_iota(jnp.int32, gated.shape, 0) & (SEQ - 1)
    before = jnp.where(place > 0, pltpu.roll(gated, 1, 0), 0.0)
    after = jnp.where(place < SEQ - 1, pltpu.roll(gated, gated.shape[0] - 1, 0), 0.0)
    conv = taps[0:1] * before + taps[1:2] * gated + taps[2:3] * after
    mixed[...] = (product(0) * conv).astype(bf)


def mixer(order, own, other, taps, blocks):
    rows = 2 * own.shape[0]
    return pl.pallas_call(
        functools.partial(mixer_kernel, order),
        out_shape=jax.ShapeDtypeStruct((rows, CHANNELS), bf),
        in_specs=[HBM, HBM, VMEM] + [HBM] * 4,
        out_specs=VMEM,
        scratch_shapes=[
            pltpu.VMEM((rows, D), bf),
            whole_scratch(3 * CHANNELS),
            pltpu.SemaphoreType.DMA((18,)),
        ],
        compiler_params=PARAMS,
        cost_estimate=pl.CostEstimate(
            flops=2 * rows * D * 3 * CHANNELS, bytes_accessed=8_000_000, transcendentals=0
        ),
    )(own, other, taps, *blocks)


def projected(left, whole, own, other, more=None):
    half = own.shape[0]

    def step(j, _):
        rows = whole[j >> 2, j & 3].reshape(256, whole.shape[-1])
        cols = pl.ds(pl.multiple_of(j * 256, 256), 256)
        sums = dot_t(left[...], rows)
        if more is not None:
            sums = sums + more[:, cols]
        own[:, cols] = sums[:half].astype(own.dtype)
        other[:, cols] = sums[half:].astype(other.dtype)
        return 0

    lax.fori_loop(0, 8, step, 0)


def mix_out_kernel(*refs):
    mixed, blocks = refs[:3], refs[3:15]
    own, other, left, whole, sems = refs[15:]
    copies = []
    for c, order in enumerate(ORDERS):
        at = c * CHANNELS
        part = blocks[4 * c : 4 * c + 4]
        copies += fill(order, part, 3 * CHANNELS, CHANNELS, whole, at, sems, len(copies))
        left[:, at : at + CHANNELS] = mixed[c][...]
    finish(copies)
    projected(left, whole, own, other)


def mix_out_product(mixed, blocks):
    rows = mixed[0].shape[0]
    return pl.pallas_call(
        mix_out_kernel,
        out_shape=[
            jax.ShapeDtypeStruct((rows // 2, D), jnp.float32),
            jax.ShapeDtypeStruct((rows // 2, D), bf),
        ],
        in_specs=[VMEM] * 3 + [HBM] * 12,
        out_specs=[VMEM] * 2,
        scratch_shapes=[
            pltpu.VMEM((rows, 3 * CHANNELS), bf),
            whole_scratch(3 * CHANNELS),
            pltpu.SemaphoreType.DMA((36,)),
        ],
        compiler_params=PARAMS,
        cost_estimate=pl.CostEstimate(
            flops=2 * rows * D * 3 * CHANNELS, bytes_accessed=9_000_000, transcendentals=0
        ),
    )(*mixed, *blocks)


def feed_kernel(first_own, first_other, *refs):
    blocks = refs[:12]
    own, other, x, up, down, hidden, sems = refs[12:]
    tokens = both_tokens(first_own, first_other, x, sems, 0)
    used = 2
    ups, downs = [], []
    for start, whole, sets in ((0, up, ups), (1, down, downs)):
        for c, order in enumerate(ORDERS):
            n = HIDDEN[c]
            part = blocks[4 * c : 4 * c + 4]
            sets.append(fill(order, part, start * n, n, whole, sum(HIDDEN[:c]), sems, used))
            used += len(sets[-1])
    for copy in sum(ups + downs, tokens):
        copy.start()
    for copy in tokens:
        copy.wait()

    def step(j, _):
        cols = pl.ds(pl.multiple_of(j * 256, 256), 256)
        raised = jnp.maximum(dot(x[...], up[..., cols].reshape(D, 256)), 0.0)
        hidden[:, cols] = (raised * raised).astype(bf)
        return 0

    ready = [sum(HIDDEN[: c + 1]) // 256 for c in range(3)]
    for c in range(3):
        for copy in ups[c]:
            copy.wait()
        lax.fori_loop(ready[c - 1] if c else 0, ready[c], step, 0)
    for copy in sum(downs, []):
        copy.wait()
    projected(hidden, down, own, other)


def feed(own, other, blocks):
    rows = 2 * own.shape[0]
    width = sum(HIDDEN)
    return pl.pallas_call(
        feed_kernel,
        out_shape=[
            jax.ShapeDtypeStruct((rows // 2, D), jnp.float32),
            jax.ShapeDtypeStruct((rows // 2, D), bf),
        ],
        in_specs=[HBM] * 14,
        out_specs=[VMEM] * 2,
        scratch_shapes=[
            pltpu.VMEM((rows, D), bf),
            whole_scratch(width),
            whole_scratch(width),
            pltpu.VMEM((rows, width), bf),
            pltpu.SemaphoreType.DMA((80,)),
        ],
        compiler_params=PARAMS,
        cost_estimate=pl.CostEstimate(
            flops=4 * rows * D * width, bytes_accessed=30_000_000, transcendentals=0
        ),
    )(own, other, *blocks)


def joined_kernel(skip, own, other, gain, out):
    def step(i, _):
        rows = pl.ds(pl.multiple_of(i * 16, 16), 16)
        values = residual_scale * skip[rows].astype(jnp.float32)
        values = values + (own[rows] + other[rows].astype(jnp.float32))
        center = values - jnp.mean(values, axis=-1, keepdims=True)
        spread = jnp.mean(center * center, axis=-1, keepdims=True)
        out[rows] = (center * lax.rsqrt(spread + norm_epsilon) * gain[...]).astype(bf)
        return 0

    lax.fori_loop(0, out.shape[0] // 16, step, 0)


def joined(skip, own, other, gain):
    other = swapped(other)
    return pl.pallas_call(
        joined_kernel,
        out_shape=jax.ShapeDtypeStruct(skip.shape, bf),
        in_specs=[VMEM] * 4,
        out_specs=VMEM,
        compiler_params=PARAMS,
    )(skip, own, other, gain.reshape(1, -1))


def local(
    tokens,
    outer_weight,
    inner_weight,
    value_weight,
    conv_taps,
    mix_out,
    norm_first,
    up_weight,
    down_weight,
    norm_second,
):
    parts = pieces(outer_weight, inner_weight, value_weight, mix_out.T, up_weight, down_weight.T)
    tokens_other = swapped(tokens)
    near, far = [], []
    for c, order in enumerate(ORDERS):
        ring = around(parts[c], order[0])
        near.append(placed(ring, order[0], [parts[c].shape[-1]])[0])
    for c, order in enumerate(ORDERS):
        ring = around(near[c], order[1])
        far.append(placed(ring, order[1], stage_widths(c)))
    blocks = [[around(far[c][s], ORDERS[c][2]) for c in range(3)] for s in range(2)]

    mixed = []
    for c, order in enumerate(ORDERS):
        taps = conv_taps[:, c * CHANNELS : (c + 1) * CHANNELS]
        mixed.append(mixer(order, tokens, tokens_other, taps, blocks[0][c]))
    own, other = mix_out_product(mixed, sum(blocks[0], []))
    first = joined(tokens, own, other, norm_first)
    first_other = swapped(first)
    own, other = feed(first, first_other, sum(blocks[1], []))
    return joined(first, own, other, norm_second)


def solution(mesh):
    finer = Mesh(
        mesh.devices.reshape(2, 2, 4, 4, 2),
        ("rep", "fs_0", "fs_1", "fs_2", "tp"),
    )
    placement = (
        P(REP_FS_TP, None),
        P(FS, "tp"),
        P(FS, "tp"),
        P(FS, "tp"),
        P(None, "tp"),
        P("tp", FS),
        P(),
        P(FS, "tp"),
        P("tp", FS),
        P(),
    )
    return jax.shard_map(
        local, mesh=finer, in_specs=placement, out_specs=P(REP_FS_TP, None), check_vma=False
    )
```

profile of v0, /device:TPU:1, one launch (start us, length us, event | category | flops | bytes accessed | tf_op | source)
XLA Modules:
  0.0 243.6 jit_solution(11094956533687637395)
XLA Ops:
  1.3 3.6 %collective-permute-start.19 = (bf16[32,2304]{1,0:T(8,128)(2,1)S(1)}, bf16[32,2304]{1,0:T(8,128)(2,1)S(1)}, u32[]{:S(2)}, u32[]{:S(2)}) collective-permute-start(bf16[32,2304]{1,0:T(8,128)(2,1)S(1)} %get-tuple-element.22.refs_0_), channel_id=1, source_target_pairs={{0,8},{1,25},{2,10},{3,27},{4,12},{5,29},{6,14},{7,31},{8,16},{9,1... | collective-permute-start | bytes 442376 | tf_op jit(solution)/shard_map/ppermute | solution.py:64
  7.4 3.4 %collective-permute-start.20 = (bf16[32,2304]{1,0:T(8,128)(2,1)S(1)}, bf16[32,2304]{1,0:T(8,128)(2,1)S(1)}, u32[]{:S(2)}, u32[]{:S(2)}) collective-permute-start(bf16[32,2304]{1,0:T(8,128)(2,1)S(1)} %collective-permute-done.19.refs_1_), channel_id=1, source_target_pairs={{0,8},{1,25},{2,10},{3,27},{4,12},{5,29},{6,14},{7,31},{8,16},{9,1... | collective-permute-start | bytes 442376 | tf_op jit(solution)/shard_map/ppermute | solution.py:64
  13.8 3.7 %collective-permute-start.22 = (bf16[4,32,2304]{2,1,0:T(8,128)(2,1)}, bf16[4,32,2304]{2,1,0:T(8,128)(2,1)S(1)}, u32[]{:S(2)}, u32[]{:S(2)}) collective-permute-start(bf16[4,32,2304]{2,1,0:T(8,128)(2,1)} %shard_map.107.refs_0_), channel_id=1, source_target_pairs={{0,32},{1,97},{2,34},{3,99},{4,36},{5,101},{6,38},{7,103},{8,40},{... | collective-permute-start | bytes 1769480 | tf_op jit(solution)/shard_map/ppermute | solution.py:64
  22.1 3.4 %collective-permute-start.11 = (bf16[32,2304]{1,0:T(8,128)(2,1)S(1)}, bf16[32,2304]{1,0:T(8,128)(2,1)S(1)}, u32[]{:S(2)}, u32[]{:S(2)}) collective-permute-start(bf16[32,2304]{1,0:T(8,128)(2,1)S(1)} %collective-permute-done.10.refs_1_), channel_id=1, source_target_pairs={{0,2},{1,7},{2,4},{3,1},{4,6},{5,3},{6,0},{7,5},{8,10},{9,15},{10,... | collective-permute-start | bytes 442376 | tf_op jit(solution)/shard_map/ppermute | solution.py:64
  30.3 3.5 %collective-permute-start.13 = (bf16[4,32,2304]{2,1,0:T(8,128)(2,1)}, bf16[4,32,2304]{2,1,0:T(8,128)(2,1)S(1)}, u32[]{:S(2)}, u32[]{:S(2)}) collective-permute-start(bf16[4,32,2304]{2,1,0:T(8,128)(2,1)} %shard_map.104.refs_0_), channel_id=1, source_target_pairs={{0,8},{1,25},{2,10},{3,27},{4,12},{5,29},{6,14},{7,31},{8,16},{9,1... | collective-permute-start | bytes 1769480 | tf_op jit(solution)/shard_map/ppermute | solution.py:64
  43.9 4.5 %collective-permute-start = (bf16[384,2048]{1,0:T(8,128)(2,1)S(1)}, bf16[384,2048]{1,0:T(8,128)(2,1)}, u32[]{:S(2)}, u32[]{:S(2)}) collective-permute-start(bf16[384,2048]{1,0:T(8,128)(2,1)S(1)} %copy-done.5), channel_id=1, source_target_pairs={{0,1},{1,0},{2,3},{3,2},{4,5},{5,4},{6,7},{7,6},{8,9},{9,8},{10,11... | collective-permute-start | bytes 4718600 | tf_op jit(solution)/shard_map/ppermute | solution.py:73
  48.5 3.1 %collective-permute-start.6 = (bf16[4,32,2560]{2,1,0:T(8,128)(2,1)}, bf16[4,32,2560]{2,1,0:T(8,128)(2,1)S(1)}, u32[]{:S(2)}, u32[]{:S(2)}) collective-permute-start(bf16[4,32,2560]{2,1,0:T(8,128)(2,1)} %shard_map.101.refs_0_), channel_id=1, source_target_pairs={{0,6},{1,3},{2,0},{3,5},{4,2},{5,7},{6,4},{7,1},{8,14},{9,11},{10,... | collective-permute-start | bytes 1966088 | tf_op jit(solution)/shard_map/ppermute | solution.py:64
  57.8 3.1 %collective-permute-start.16 = (bf16[4,4,32,1024]{3,2,1,0:T(8,128)(2,1)}, bf16[4,4,32,1024]{3,2,1,0:T(8,128)(2,1)S(1)}, u32[]{:S(2)}, u32[]{:S(2)}) collective-permute-start(bf16[4,4,32,1024]{3,2,1,0:T(8,128)(2,1)} %get-tuple-element.21.refs_0_.refs_7_), channel_id=1, source_target_pairs={{0,32},{1,97},{2,34},{3,99},{4,36},{5,101},{6,38},{7,103},{8,40},{... | collective-permute-start | bytes 3145736 | tf_op jit(solution)/shard_map/ppermute | solution.py:64
  60.9 3.5 %collective-permute-done.6.refs_3_ = bf16[4,32,2560]{2,1,0:T(8,128)(2,1)S(1)} collective-permute-done((bf16[4,32,2560]{2,1,0:T(8,128)(2,1)}, bf16[4,32,2560]{2,1,0:T(8,128)(2,1)S(1)}, u32[]{:S(2)}, u32[]{:S(2)}) %collective-permute-start.6) | collective-permute-done | bytes 655392 | tf_op jit(solution)/shard_map/ppermute | solution.py:64
  69.1 3.2 %collective-permute-start.7 = (bf16[4,4,32,1024]{3,2,1,0:T(8,128)(2,1)}, bf16[4,4,32,1024]{3,2,1,0:T(8,128)(2,1)S(1)}, u32[]{:S(2)}, u32[]{:S(2)}) collective-permute-start(bf16[4,4,32,1024]{3,2,1,0:T(8,128)(2,1)} %get-tuple-element.19.refs_0_.refs_3_), channel_id=1, source_target_pairs={{0,8},{1,25},{2,10},{3,27},{4,12},{5,29},{6,14},{7,31},{8,16},{9,1... | collective-permute-start | bytes 3145736 | tf_op jit(solution)/shard_map/ppermute | solution.py:64
  72.3 14.2 %collective-permute-done.25.refs_1_.refs_12_ = bf16[4,4,32,1024]{3,2,1,0:T(8,128)(2,1)S(1)} collective-permute-done((bf16[4,4,32,1024]{3,2,1,0:T(8,128)(2,1)}, bf16[4,4,32,1024]{3,2,1,0:T(8,128)(2,1)S(1)}, u32[]{:S(2)}, u32[]{:S(2)}) %collective-permute-start.25) | collective-permute-done | bytes 1048608 | tf_op jit(solution)/shard_map/ppermute | solution.py:64
  94.3 7.9 %collective-permute-done.26.refs_2_.refs_13_ = bf16[4,4,32,1024]{3,2,1,0:T(8,128)(2,1)S(1)} collective-permute-done((bf16[4,4,32,1024]{3,2,1,0:T(8,128)(2,1)S(1)}, bf16[4,4,32,1024]{3,2,1,0:T(8,128)(2,1)S(1)}, u32[]{:S(2)}, u32[]{:S(2)}) %collective-permute-start.26) | collective-permute-done | bytes 1048608 | tf_op jit(solution)/shard_map/ppermute | solution.py:64
  102.1 4.7 %shard_map.109.refs_2_ = bf16[768,256]{1,0:T(8,128)(2,1)S(1)} custom-call(bf16[384,2048]{1,0:T(8,128)(2,1)S(1)} %copy-done.5, bf16[384,2048]{1,0:T(8,128)(2,1)} %collective-permute-done.other, f32[3,256]{1,0:T(4,128)S(1)} %get-tuple-element.31.taps, bf16[4,4,32,1024]{3,2,1,0:T(8,128)(2,1)S(1)} %copy-done.6, ...), custom_call_target="tpu_custom_call" | custom-call | flops 2415919104 | bytes 8000000 | tf_op jit(solution)/shard_map/pallas_call | solution.py:204
  111.8 4.8 %shard_map.106.refs_1_ = bf16[768,256]{1,0:T(8,128)(2,1)S(1)} custom-call(bf16[384,2048]{1,0:T(8,128)(2,1)S(1)} %copy-done.5, bf16[384,2048]{1,0:T(8,128)(2,1)} %collective-permute-done.other, f32[3,256]{1,0:T(4,128)S(1)} %get-tuple-element.33.taps, bf16[4,4,32,1024]{3,2,1,0:T(8,128)(2,1)S(1)} %copy-done.8, ...), custom_call_target="tpu_custom_call" | custom-call | flops 2415919104 | bytes 8000000 | tf_op jit(solution)/shard_map/pallas_call | solution.py:204
  116.7 4.4 %shard_map.103.refs_0_ = bf16[768,256]{1,0:T(8,128)(2,1)S(1)} custom-call(bf16[384,2048]{1,0:T(8,128)(2,1)S(1)} %copy-done.5, bf16[384,2048]{1,0:T(8,128)(2,1)} %collective-permute-done.other, f32[3,256]{1,0:T(4,128)S(1)} %get-tuple-element.32.taps, bf16[4,4,32,1024]{3,2,1,0:T(8,128)(2,1)S(1)} %copy-done.11, ...), custom_call_target="tpu_custom_call" | custom-call | flops 2415919104 | bytes 8000000 | tf_op jit(solution)/shard_map/pallas_call | solution.py:204
  123.4 8.3 %shard_map.110 = (f32[384,2048]{1,0:T(8,128)}, bf16[384,2048]{1,0:T(8,128)(2,1)}) custom-call(bf16[768,256]{1,0:T(8,128)(2,1)S(1)} %shard_map.103.refs_0_, bf16[768,256]{1,0:T(8,128)(2,1)S(1)} %shard_map.106.refs_1_, bf16[768,256]{1,0:T(8,128)(2,1)S(1)} %shard_map.109.refs_2_, bf16[4,4,32,1024]{3,2,1,0:T(8,128)(2,1)S(1)} %copy-done.11, ...), custom_call_target="tpu_custom_call" | custom-call | flops 2415919104 | bytes 9000000 | tf_op jit(solution)/shard_map/pallas_call | solution.py:252
  131.7 3.6 %collective-permute-start.28 = (bf16[384,2048]{1,0:T(8,128)(2,1)}, bf16[384,2048]{1,0:T(8,128)(2,1)S(1)}, u32[]{:S(2)}, u32[]{:S(2)}) collective-permute-start(bf16[384,2048]{1,0:T(8,128)(2,1)} %get-tuple-element.25), channel_id=1, source_target_pairs={{0,1},{1,0},{2,3},{3,2},{4,5},{5,4},{6,7},{7,6},{8,9},{9,8},{10,11... | collective-permute-start | bytes 4718600 | tf_op jit(solution)/shard_map/ppermute | solution.py:73
  142.6 7.2 %shard_map.111.first_own.skip = bf16[384,2048]{1,0:T(8,128)(2,1)S(1)} custom-call(bf16[384,2048]{1,0:T(8,128)(2,1)S(1)} %copy-done.5, f32[384,2048]{1,0:T(8,128)} %get-tuple-element.24.own, bf16[384,2048]{1,0:T(8,128)(2,1)S(1)} %collective-permute-done.28.other, f32[1,2048]{1,0:T(1,128)S(1)} %bitcast.4), custom_call_target="tpu_custom_call" | custom-call | tf_op jit(solution)/shard_map/pallas_call | solution.py:345
  149.8 18.5 %collective-permute-done.36.refs_9_ = bf16[4,4,32,1280]{3,2,1,0:T(8,128)(2,1)S(1)} collective-permute-done((bf16[4,4,32,1280]{3,2,1,0:T(8,128)(2,1)S(1)}, bf16[4,4,32,1280]{3,2,1,0:T(8,128)(2,1)S(1)}, u32[]{:S(2)}, u32[]{:S(2)}) %collective-permute-start.36) | collective-permute-done | bytes 1310752 | tf_op jit(solution)/shard_map/ppermute | solution.py:64
  171.6 4.9 %collective-permute-start.34 = (bf16[4,4,32,1280]{3,2,1,0:T(8,128)(2,1)S(1)}, bf16[4,4,32,1280]{3,2,1,0:T(8,128)(2,1)S(1)}, u32[]{:S(2)}, u32[]{:S(2)}) collective-permute-start(bf16[4,4,32,1280]{3,2,1,0:T(8,128)(2,1)S(1)} %collective-permute-done.33.refs_5_), channel_id=1, source_target_pairs={{0,32},{1,97},{2,34},{3,99},{4,36},{5,101},{6,38},{7,103},{8,40},{... | collective-permute-start | bytes 3932168 | tf_op jit(solution)/shard_map/ppermute | solution.py:64
  176.5 28.1 %collective-permute-done.32.refs_3_ = bf16[4,4,32,1536]{3,2,1,0:T(8,128)(2,1)S(1)} collective-permute-done((bf16[4,4,32,1536]{3,2,1,0:T(8,128)(2,1)S(1)}, bf16[4,4,32,1536]{3,2,1,0:T(8,128)(2,1)S(1)}, u32[]{:S(2)}, u32[]{:S(2)}) %collective-permute-start.32) | collective-permute-done | bytes 1572896 | tf_op jit(solution)/shard_map/ppermute | solution.py:64
  207.8 22.0 %shard_map.112 = (f32[384,2048]{1,0:T(8,128)}, bf16[384,2048]{1,0:T(8,128)(2,1)}) custom-call(bf16[384,2048]{1,0:T(8,128)(2,1)} %copy-done, bf16[384,2048]{1,0:T(8,128)(2,1)} %copy-done.25, bf16[4,4,32,1536]{3,2,1,0:T(8,128)(2,1)} %get-tuple-element.26.refs_0_, bf16[4,4,32,1536]{3,2,1,0:T(8,128)(2,1)} %copy-done.22, bf16[4,4,32,1536]{3,2,1,0:T(8,128)(2,1)} %copy-done.24, ...), custom_call_target="tpu_custom_call" | custom-call | flops 12884901888 | bytes 30000000 | tf_op jit(solution)/shard_map/pallas_call | solution.py:308
  230.7 3.2 %collective-permute-done.39.other = bf16[384,2048]{1,0:T(8,128)(2,1)S(1)} collective-permute-done((bf16[384,2048]{1,0:T(8,128)(2,1)}, bf16[384,2048]{1,0:T(8,128)(2,1)S(1)}, u32[]{:S(2)}, u32[]{:S(2)}) %collective-permute-start.39) | collective-permute-done | bytes 1572896 | tf_op jit(solution)/shard_map/ppermute | solution.py:73
  235.4 8.2 %shard_map.113 = bf16[384,2048]{1,0:T(8,128)(2,1)} custom-call(bf16[384,2048]{1,0:T(8,128)(2,1)S(1)} %copy-done.1, f32[384,2048]{1,0:T(8,128)} %get-tuple-element.29.own, bf16[384,2048]{1,0:T(8,128)(2,1)S(1)} %collective-permute-done.39.other, f32[1,2048]{1,0:T(1,128)S(1)} %bitcast.5), custom_call_target="tpu_custom_call" | custom-call | tf_op jit(solution)/shard_map/pallas_call | solution.py:345
  (129 shorter events, 68.2 us)
Async XLA Ops:
  13.8 23.1 %collective-permute-start.22 = (bf16[4,32,2304]{2,1,0:T(8,128)(2,1)}, bf16[4,32,2304]{2,1,0:T(8,128)(2,1)S(1)}, u32[]{:S(2)}, u32[]{:S(2)}) collective-permute-start(bf16[4,32,2304]{2,1,0:T(8,128)(2,1)} %shard_map.107.refs_0_), channel_id=1, source_target_pairs={{0,32},{1,97},{2,34},{3,99},{4,36},{5,101},{6,38},{7,103},{8,40},{... | collective-permute-start | bytes 1769480 | tf_op jit(solution)/shard_map/ppermute | solution.py:64
  40.9 15.3 %collective-permute-start.14 = (bf16[4,32,2304]{2,1,0:T(8,128)(2,1)S(1)}, bf16[4,32,2304]{2,1,0:T(8,128)(2,1)S(1)}, u32[]{:S(2)}, u32[]{:S(2)}) collective-permute-start(bf16[4,32,2304]{2,1,0:T(8,128)(2,1)S(1)} %collective-permute-done.13.refs_1_), channel_id=1, source_target_pairs={{0,8},{1,25},{2,10},{3,27},{4,12},{5,29},{6,14},{7,31},{8,16},{9,1... | collective-permute-start | bytes 1769480 | tf_op jit(solution)/shard_map/ppermute | solution.py:64
  43.9 43.3 %collective-permute-start = (bf16[384,2048]{1,0:T(8,128)(2,1)S(1)}, bf16[384,2048]{1,0:T(8,128)(2,1)}, u32[]{:S(2)}, u32[]{:S(2)}) collective-permute-start(bf16[384,2048]{1,0:T(8,128)(2,1)S(1)} %copy-done.5), channel_id=1, source_target_pairs={{0,1},{1,0},{2,3},{3,2},{4,5},{5,4},{6,7},{7,6},{8,9},{9,8},{10,11... | collective-permute-start | bytes 4718600 | tf_op jit(solution)/shard_map/ppermute | solution.py:73
  48.5 15.9 %collective-permute-start.6 = (bf16[4,32,2560]{2,1,0:T(8,128)(2,1)}, bf16[4,32,2560]{2,1,0:T(8,128)(2,1)S(1)}, u32[]{:S(2)}, u32[]{:S(2)}) collective-permute-start(bf16[4,32,2560]{2,1,0:T(8,128)(2,1)} %shard_map.101.refs_0_), channel_id=1, source_target_pairs={{0,6},{1,3},{2,0},{3,5},{4,2},{5,7},{6,4},{7,1},{8,14},{9,11},{10,... | collective-permute-start | bytes 1966088 | tf_op jit(solution)/shard_map/ppermute | solution.py:64
  51.6 15.9 %collective-permute-start.5 = (bf16[4,32,2560]{2,1,0:T(8,128)(2,1)S(1)}, bf16[4,32,2560]{2,1,0:T(8,128)(2,1)S(1)}, u32[]{:S(2)}, u32[]{:S(2)}) collective-permute-start(bf16[4,32,2560]{2,1,0:T(8,128)(2,1)S(1)} %collective-permute-done.4.refs_1_), channel_id=1, source_target_pairs={{0,2},{1,7},{2,4},{3,1},{4,6},{5,3},{6,0},{7,5},{8,10},{9,15},{10,... | collective-permute-start | bytes 1966088 | tf_op jit(solution)/shard_map/ppermute | solution.py:64
  54.5 32.0 %collective-permute-start.25 = (bf16[4,4,32,1024]{3,2,1,0:T(8,128)(2,1)}, bf16[4,4,32,1024]{3,2,1,0:T(8,128)(2,1)S(1)}, u32[]{:S(2)}, u32[]{:S(2)}) collective-permute-start(bf16[4,4,32,1024]{3,2,1,0:T(8,128)(2,1)} %get-tuple-element.23.refs_0_.refs_11_), channel_id=1, source_target_pairs={{0,2},{1,7},{2,4},{3,1},{4,6},{5,3},{6,0},{7,5},{8,10},{9,15},{10,... | collective-permute-start | bytes 3145736 | tf_op jit(solution)/shard_map/ppermute | solution.py:64
  57.8 31.4 %collective-permute-start.16 = (bf16[4,4,32,1024]{3,2,1,0:T(8,128)(2,1)}, bf16[4,4,32,1024]{3,2,1,0:T(8,128)(2,1)S(1)}, u32[]{:S(2)}, u32[]{:S(2)}) collective-permute-start(bf16[4,4,32,1024]{3,2,1,0:T(8,128)(2,1)} %get-tuple-element.21.refs_0_.refs_7_), channel_id=1, source_target_pairs={{0,32},{1,97},{2,34},{3,99},{4,36},{5,101},{6,38},{7,103},{8,40},{... | collective-permute-start | bytes 3145736 | tf_op jit(solution)/shard_map/ppermute | solution.py:64
  64.4 26.9 %collective-permute-start.27 = (bf16[4,4,32,1024]{3,2,1,0:T(8,128)(2,1)S(1)}, bf16[4,4,32,1024]{3,2,1,0:T(8,128)(2,1)S(1)}, u32[]{:S(2)}, u32[]{:S(2)}) collective-permute-start(bf16[4,4,32,1024]{3,2,1,0:T(8,128)(2,1)S(1)} %copy-done.6), channel_id=1, source_target_pairs={{0,6},{1,3},{2,0},{3,5},{4,2},{5,7},{6,4},{7,1},{8,14},{9,11},{10,... | collective-permute-start | bytes 3145736 | tf_op jit(solution)/shard_map/ppermute | solution.py:64
  69.1 22.3 %collective-permute-start.7 = (bf16[4,4,32,1024]{3,2,1,0:T(8,128)(2,1)}, bf16[4,4,32,1024]{3,2,1,0:T(8,128)(2,1)S(1)}, u32[]{:S(2)}, u32[]{:S(2)}) collective-permute-start(bf16[4,4,32,1024]{3,2,1,0:T(8,128)(2,1)} %get-tuple-element.19.refs_0_.refs_3_), channel_id=1, source_target_pairs={{0,8},{1,25},{2,10},{3,27},{4,12},{5,29},{6,14},{7,31},{8,16},{9,1... | collective-permute-start | bytes 3145736 | tf_op jit(solution)/shard_map/ppermute | solution.py:64
  86.4 15.7 %collective-permute-start.26 = (bf16[4,4,32,1024]{3,2,1,0:T(8,128)(2,1)S(1)}, bf16[4,4,32,1024]{3,2,1,0:T(8,128)(2,1)S(1)}, u32[]{:S(2)}, u32[]{:S(2)}) collective-permute-start(bf16[4,4,32,1024]{3,2,1,0:T(8,128)(2,1)S(1)} %collective-permute-done.25.refs_1_.refs_12_), channel_id=1, source_target_pairs={{0,2},{1,7},{2,4},{3,1},{4,6},{5,3},{6,0},{7,5},{8,10},{9,15},{10,... | collective-permute-start | bytes 3145736 | tf_op jit(solution)/shard_map/ppermute | solution.py:64
  87.3 22.1 %collective-permute-start.18 = (bf16[4,4,32,1024]{3,2,1,0:T(8,128)(2,1)S(1)}, bf16[4,4,32,1024]{3,2,1,0:T(8,128)(2,1)S(1)}, u32[]{:S(2)}, u32[]{:S(2)}) collective-permute-start(bf16[4,4,32,1024]{3,2,1,0:T(8,128)(2,1)S(1)} %copy-done.8), channel_id=1, source_target_pairs={{0,96},{1,33},{2,98},{3,35},{4,100},{5,37},{6,102},{7,39},{8,104},... | collective-permute-start | bytes 3145736 | tf_op jit(solution)/shard_map/ppermute | solution.py:64
  89.2 22.7 %collective-permute-start.17 = (bf16[4,4,32,1024]{3,2,1,0:T(8,128)(2,1)S(1)}, bf16[4,4,32,1024]{3,2,1,0:T(8,128)(2,1)S(1)}, u32[]{:S(2)}, u32[]{:S(2)}) collective-permute-start(bf16[4,4,32,1024]{3,2,1,0:T(8,128)(2,1)S(1)} %collective-permute-done.16.refs_1_.refs_8_), channel_id=1, source_target_pairs={{0,32},{1,97},{2,34},{3,99},{4,36},{5,101},{6,38},{7,103},{8,40},{... | collective-permute-start | bytes 3145736 | tf_op jit(solution)/shard_map/ppermute | solution.py:64
  91.4 25.3 %collective-permute-start.9 = (bf16[4,4,32,1024]{3,2,1,0:T(8,128)(2,1)}, bf16[4,4,32,1024]{3,2,1,0:T(8,128)(2,1)S(1)}, u32[]{:S(2)}, u32[]{:S(2)}) collective-permute-start(bf16[4,4,32,1024]{3,2,1,0:T(8,128)(2,1)} %get-tuple-element.19.refs_0_.refs_3_), channel_id=1, source_target_pairs={{0,24},{1,9},{2,26},{3,11},{4,28},{5,13},{6,30},{7,15},{8,0},{9,17... | collective-permute-start | bytes 3145736 | tf_op jit(solution)/shard_map/ppermute | solution.py:64
  91.4 25.3 %collective-permute-start.8 = (bf16[4,4,32,1024]{3,2,1,0:T(8,128)(2,1)S(1)}, bf16[4,4,32,1024]{3,2,1,0:T(8,128)(2,1)S(1)}, u32[]{:S(2)}, u32[]{:S(2)}) collective-permute-start(bf16[4,4,32,1024]{3,2,1,0:T(8,128)(2,1)S(1)} %collective-permute-done.7.refs_1_.refs_4_), channel_id=1, source_target_pairs={{0,8},{1,25},{2,10},{3,27},{4,12},{5,29},{6,14},{7,31},{8,16},{9,1... | collective-permute-start | bytes 3145736 | tf_op jit(solution)/shard_map/ppermute | solution.py:64
  135.3 34.0 %collective-permute-start.30 = (bf16[4,4,32,1536]{3,2,1,0:T(8,128)(2,1)S(1)}, bf16[4,4,32,1536]{3,2,1,0:T(8,128)(2,1)S(1)}, u32[]{:S(2)}, u32[]{:S(2)}) collective-permute-start(bf16[4,4,32,1536]{3,2,1,0:T(8,128)(2,1)S(1)} %copy-done.21), channel_id=1, source_target_pairs={{0,8},{1,25},{2,10},{3,27},{4,12},{5,29},{6,14},{7,31},{8,16},{9,1... | collective-permute-start | bytes 4718600 | tf_op jit(solution)/shard_map/ppermute | solution.py:64
  138.2 30.1 %collective-permute-start.36 = (bf16[4,4,32,1280]{3,2,1,0:T(8,128)(2,1)S(1)}, bf16[4,4,32,1280]{3,2,1,0:T(8,128)(2,1)S(1)}, u32[]{:S(2)}, u32[]{:S(2)}) collective-permute-start(bf16[4,4,32,1280]{3,2,1,0:T(8,128)(2,1)S(1)} %copy-done.26), channel_id=1, source_target_pairs={{0,2},{1,7},{2,4},{3,1},{4,6},{5,3},{6,0},{7,5},{8,10},{9,15},{10,... | collective-permute-start | bytes 3932168 | tf_op jit(solution)/shard_map/ppermute | solution.py:64
  139.2 31.8 %collective-permute-start.33 = (bf16[4,4,32,1280]{3,2,1,0:T(8,128)(2,1)S(1)}, bf16[4,4,32,1280]{3,2,1,0:T(8,128)(2,1)S(1)}, u32[]{:S(2)}, u32[]{:S(2)}) collective-permute-start(bf16[4,4,32,1280]{3,2,1,0:T(8,128)(2,1)S(1)} %copy-done.19), channel_id=1, source_target_pairs={{0,32},{1,97},{2,34},{3,99},{4,36},{5,101},{6,38},{7,103},{8,40},{... | collective-permute-start | bytes 3932168 | tf_op jit(solution)/shard_map/ppermute | solution.py:64
  142.3 28.8 %collective-permute-start.38 = (bf16[4,4,32,1280]{3,2,1,0:T(8,128)(2,1)S(1)}, bf16[4,4,32,1280]{3,2,1,0:T(8,128)(2,1)}, u32[]{:S(2)}, u32[]{:S(2)}) collective-permute-start(bf16[4,4,32,1280]{3,2,1,0:T(8,128)(2,1)S(1)} %copy-done.26), channel_id=1, source_target_pairs={{0,6},{1,3},{2,0},{3,5},{4,2},{5,7},{6,4},{7,1},{8,14},{9,11},{10,... | collective-permute-start | bytes 3932168 | tf_op jit(solution)/shard_map/ppermute | solution.py:64
  142.6 29.0 %collective-permute-start.35 = (bf16[4,4,32,1280]{3,2,1,0:T(8,128)(2,1)S(1)}, bf16[4,4,32,1280]{3,2,1,0:T(8,128)(2,1)S(1)}, u32[]{:S(2)}, u32[]{:S(2)}) collective-permute-start(bf16[4,4,32,1280]{3,2,1,0:T(8,128)(2,1)S(1)} %copy-done.19), channel_id=1, source_target_pairs={{0,96},{1,33},{2,98},{3,35},{4,100},{5,37},{6,102},{7,39},{8,104},... | collective-permute-start | bytes 3932168 | tf_op jit(solution)/shard_map/ppermute | solution.py:64
  168.3 36.3 %collective-permute-start.32 = (bf16[4,4,32,1536]{3,2,1,0:T(8,128)(2,1)S(1)}, bf16[4,4,32,1536]{3,2,1,0:T(8,128)(2,1)S(1)}, u32[]{:S(2)}, u32[]{:S(2)}) collective-permute-start(bf16[4,4,32,1536]{3,2,1,0:T(8,128)(2,1)S(1)} %copy-done.21), channel_id=1, source_target_pairs={{0,24},{1,9},{2,26},{3,11},{4,28},{5,13},{6,30},{7,15},{8,0},{9,17... | collective-permute-start | bytes 4718600 | tf_op jit(solution)/shard_map/ppermute | solution.py:64
  169.4 35.3 %collective-permute-start.31 = (bf16[4,4,32,1536]{3,2,1,0:T(8,128)(2,1)S(1)}, bf16[4,4,32,1536]{3,2,1,0:T(8,128)(2,1)S(1)}, u32[]{:S(2)}, u32[]{:S(2)}) collective-permute-start(bf16[4,4,32,1536]{3,2,1,0:T(8,128)(2,1)S(1)} %collective-permute-done.30.refs_1_), channel_id=1, source_target_pairs={{0,8},{1,25},{2,10},{3,27},{4,12},{5,29},{6,14},{7,31},{8,16},{9,1... | collective-permute-start | bytes 4718600 | tf_op jit(solution)/shard_map/ppermute | solution.py:64
  171.1 33.6 %collective-permute-start.29 = (bf16[384,2048]{1,0:T(8,128)(2,1)S(1)}, bf16[384,2048]{1,0:T(8,128)(2,1)S(1)}, u32[]{:S(2)}, u32[]{:S(2)}) collective-permute-start(bf16[384,2048]{1,0:T(8,128)(2,1)S(1)} %shard_map.111.first_own.skip), channel_id=1, source_target_pairs={{0,1},{1,0},{2,3},{3,2},{4,5},{5,4},{6,7},{7,6},{8,9},{9,8},{10,11... | collective-permute-start | bytes 4718600 | tf_op jit(solution)/shard_map/ppermute | solution.py:73
  171.1 33.5 %collective-permute-start.37 = (bf16[4,4,32,1280]{3,2,1,0:T(8,128)(2,1)}, bf16[4,4,32,1280]{3,2,1,0:T(8,128)(2,1)S(1)}, u32[]{:S(2)}, u32[]{:S(2)}) collective-permute-start(bf16[4,4,32,1280]{3,2,1,0:T(8,128)(2,1)} %copy-done.27), channel_id=1, source_target_pairs={{0,2},{1,7},{2,4},{3,1},{4,6},{5,3},{6,0},{7,5},{8,10},{9,15},{10,... | collective-permute-start | bytes 3932168 | tf_op jit(solution)/shard_map/ppermute | solution.py:64
  171.6 33.0 %collective-permute-start.34 = (bf16[4,4,32,1280]{3,2,1,0:T(8,128)(2,1)S(1)}, bf16[4,4,32,1280]{3,2,1,0:T(8,128)(2,1)S(1)}, u32[]{:S(2)}, u32[]{:S(2)}) collective-permute-start(bf16[4,4,32,1280]{3,2,1,0:T(8,128)(2,1)S(1)} %collective-permute-done.33.refs_5_), channel_id=1, source_target_pairs={{0,32},{1,97},{2,34},{3,99},{4,36},{5,101},{6,38},{7,103},{8,40},{... | collective-permute-start | bytes 3932168 | tf_op jit(solution)/shard_map/ppermute | solution.py:64
  (45 other events, 663.9 us)
where the time goes:
time: 244 us
  waiting for transfers between devices  91 us (37%)
  starting transfers between devices  76.2 us (31%)
  Pallas kernels  68.1 us (28%)
  local copies, waits for them, and re-layouts  7.92 us (3%)
    ppermute x36, waiting for transfers between devices, moved(): return lax.ppermute(block, REP_FS_TP, ring_pairs(axis, step))  87.8 us
    ppermute x36, starting transfers between devices, moved(): return lax.ppermute(block, REP_FS_TP, ring_pairs(axis, step))  67.1 us
    pallas_call x1, Pallas kernels, feed(): pl.pallas_call(feed_kernel, out_shape=[jax.ShapeDtypeStruct((rows // 2, D...  22 us
    pallas_call x2, Pallas kernels, joined(): pl.pallas_call(joined_kernel, out_shape=jax.ShapeDtypeStruct(skip.shape,...  15.4 us
    pallas_call x3, Pallas kernels, mixer(): pl.pallas_call(functools.partial(mixer_kernel, order), out_shape=jax.Shap...  13.9 us
    ppermute x4, starting transfers between devices, swapped(): return lax.ppermute(x, 'tp', [(0, 1), (1, 0)])  9.09 us
    pallas_call x1, Pallas kernels, mix_out_product(): pl.pallas_call(mix_out_kernel, out_shape=[jax.ShapeDtypeStruct((rows // 2...  8.32 us
    unnamed x58, local copies, waits for them, and re-layouts  7.92 us
  transfers between devices with their start and end apart: 40, of which 15 were waited for; matrix products, arithmetic and copies ran while one was open for 0% of the time, Pallas kernels for 9%

commit v1 on v0

--- a/solution.py
+++ b/solution.py
@@ -24,7 +24,10 @@
 bf = jnp.bfloat16
 HBM = pl.BlockSpec(memory_space=pltpu.HBM)
 VMEM = pl.BlockSpec(memory_space=pltpu.VMEM)
-PARAMS = pltpu.CompilerParams(vmem_limit_bytes=48 * 1024 * 1024)
+
+
+def limit(mebibytes):
+    return pltpu.CompilerParams(vmem_limit_bytes=mebibytes * 1024 * 1024)
 
 
 def in_hbm(arrays):
@@ -109,36 +112,31 @@
         out_specs=[VMEM] * 3,
         scratch_shapes=[pltpu.VMEM((ROWS, w.shape[1]), jnp.float32) for w in weights]
         + [pltpu.SemaphoreType.DMA((6,))],
-        compiler_params=PARAMS,
+        compiler_params=limit(6),
     )(*in_hbm(weights))
 
 
-def place_kernel(axis, widths, *refs):
-    parts, outs, sems = refs[:4], refs[4:-1], refs[-1]
-    copies = []
-    for k, part in enumerate(parts):
-        at = 0
-        for i, width in enumerate(widths):
-            copies.append(
-                pltpu.make_async_copy(
-                    part.at[..., pl.ds(at, width)],
-                    outs[i].at[source(axis, k)],
-                    sems.at[len(copies)],
-                )
+def place_kernel(axis, start, *refs):
+    parts, out, sems = refs[:4], refs[4], refs[5]
+    width = out.shape[-1]
+    finish(
+        [
+            pltpu.make_async_copy(
+                part.at[..., pl.ds(start, width)], out.at[source(axis, k)], sems.at[k]
             )
-            at += width
-    finish(copies)
-
-
-def placed(parts, axis, widths):
-    lead = parts[0].shape[:-1]
-    return pl.pallas_call(
-        functools.partial(place_kernel, axis, widths),
-        out_shape=[pltpu.HBM((4, *lead, w), bf) for w in widths],
+            for k, part in enumerate(parts)
+        ]
+    )
+
+
+def placed(parts, axis, start, width):
+    return pl.pallas_call(
+        functools.partial(place_kernel, axis, start),
+        out_shape=pltpu.HBM((4, *parts[0].shape[:-1], width), bf),
         in_specs=[HBM] * 4,
-        out_specs=[HBM] * len(widths),
-        scratch_shapes=[pltpu.SemaphoreType.DMA((4 * len(widths),))],
-        compiler_params=PARAMS,
+        out_specs=HBM,
+        scratch_shapes=[pltpu.SemaphoreType.DMA((4,))],
+        compiler_params=limit(4),
     )(*parts)
 
 
@@ -211,7 +209,7 @@
             whole_scratch(3 * CHANNELS),
             pltpu.SemaphoreType.DMA((18,)),
         ],
-        compiler_params=PARAMS,
+        compiler_params=limit(16),
         cost_estimate=pl.CostEstimate(
             flops=2 * rows * D * 3 * CHANNELS, bytes_accessed=8_000_000, transcendentals=0
         ),
@@ -225,10 +223,11 @@
         rows = whole[j >> 2, j & 3].reshape(256, whole.shape[-1])
         cols = pl.ds(pl.multiple_of(j * 256, 256), 256)
         sums = dot_t(left[...], rows)
+        ours, theirs = sums[:half], sums[half:]
         if more is not None:
-            sums = sums + more[:, cols]
-        own[:, cols] = sums[:half].astype(own.dtype)
-        other[:, cols] = sums[half:].astype(other.dtype)
+            ours, theirs = ours + more[0][:, cols], theirs + more[1][:, cols]
+        own[:, cols] = ours.astype(own.dtype)
+        other[:, cols] = theirs.astype(other.dtype)
         return 0
 
     lax.fori_loop(0, 8, step, 0)
@@ -262,24 +261,28 @@
             whole_scratch(3 * CHANNELS),
             pltpu.SemaphoreType.DMA((36,)),
         ],
-        compiler_params=PARAMS,
+        compiler_params=limit(16),
         cost_estimate=pl.CostEstimate(
             flops=2 * rows * D * 3 * CHANNELS, bytes_accessed=9_000_000, transcendentals=0
         ),
     )(*mixed, *blocks)
 
 
-def feed_kernel(first_own, first_other, *refs):
-    blocks = refs[:12]
-    own, other, x, up, down, hidden, sems = refs[12:]
+def feed_kernel(parts, first_own, first_other, *refs):
+    blocks, refs = refs[: 4 * len(parts)], refs[4 * len(parts) :]
+    more = None
+    if len(refs) == 9:
+        more, refs = refs[:2], refs[2:]
+    own, other, x, up, down, hidden, sems = refs
     tokens = both_tokens(first_own, first_other, x, sems, 0)
     used = 2
+    ends = [sum(HIDDEN[c] for c in parts[: i + 1]) for i in range(len(parts))]
     ups, downs = [], []
-    for start, whole, sets in ((0, up, ups), (1, down, downs)):
-        for c, order in enumerate(ORDERS):
+    for second, whole, sets in ((0, up, ups), (1, down, downs)):
+        for i, c in enumerate(parts):
             n = HIDDEN[c]
-            part = blocks[4 * c : 4 * c + 4]
-            sets.append(fill(order, part, start * n, n, whole, sum(HIDDEN[:c]), sems, used))
+            ring = blocks[4 * i : 4 * i + 4]
+            sets.append(fill(ORDERS[c], ring, second * n, n, whole, ends[i] - n, sems, used))
             used += len(sets[-1])
     for copy in sum(ups + downs, tokens):
         copy.start()
@@ -292,44 +295,47 @@
         hidden[:, cols] = (raised * raised).astype(bf)
         return 0
 
-    ready = [sum(HIDDEN[: c + 1]) // 256 for c in range(3)]
-    for c in range(3):
-        for copy in ups[c]:
+    done = 0
+    for copies, end in zip(ups, ends):
+        for copy in copies:
             copy.wait()
-        lax.fori_loop(ready[c - 1] if c else 0, ready[c], step, 0)
+        lax.fori_loop(done, end // 256, step, 0)
+        done = end // 256
     for copy in sum(downs, []):
         copy.wait()
-    projected(hidden, down, own, other)
-
-
-def feed(own, other, blocks):
-    rows = 2 * own.shape[0]
-    width = sum(HIDDEN)
-    return pl.pallas_call(
-        feed_kernel,
+    projected(hidden, down, own, other, more)
+
+
+def feed(parts, own, other, blocks, more=None):
+    half = own.shape[0]
+    width = sum(HIDDEN[c] for c in parts)
+    extra = [] if more is None else list(more)
+    last = jnp.float32 if more is None else bf
+    return pl.pallas_call(
+        functools.partial(feed_kernel, parts),
         out_shape=[
-            jax.ShapeDtypeStruct((rows // 2, D), jnp.float32),
-            jax.ShapeDtypeStruct((rows // 2, D), bf),
+            jax.ShapeDtypeStruct((half, D), jnp.float32),
+            jax.ShapeDtypeStruct((half, D), last),
         ],
-        in_specs=[HBM] * 14,
+        in_specs=[HBM] * (2 + len(blocks)) + [VMEM] * len(extra),
         out_specs=[VMEM] * 2,
         scratch_shapes=[
-            pltpu.VMEM((rows, D), bf),
+            pltpu.VMEM((2 * half, D), bf),
             whole_scratch(width),
             whole_scratch(width),
-            pltpu.VMEM((rows, width), bf),
+            pltpu.VMEM((2 * half, width), bf),
             pltpu.SemaphoreType.DMA((80,)),
         ],
-        compiler_params=PARAMS,
+        compiler_params=limit(32),
         cost_estimate=pl.CostEstimate(
-            flops=4 * rows * D * width, bytes_accessed=30_000_000, transcendentals=0
+            flops=8 * half * D * width, bytes_accessed=20_000_000, transcendentals=0
         ),
-    )(own, other, *blocks)
+    )(own, other, *blocks, *extra)
 
 
 def joined_kernel(skip, own, other, gain, out):
     def step(i, _):
-        rows = pl.ds(pl.multiple_of(i * 16, 16), 16)
+        rows = pl.ds(pl.multiple_of(i * 128, 128), 128)
         values = residual_scale * skip[rows].astype(jnp.float32)
         values = values + (own[rows] + other[rows].astype(jnp.float32))
         center = values - jnp.mean(values, axis=-1, keepdims=True)
@@ -337,7 +343,7 @@
         out[rows] = (center * lax.rsqrt(spread + norm_epsilon) * gain[...]).astype(bf)
         return 0
 
-    lax.fori_loop(0, out.shape[0] // 16, step, 0)
+    lax.fori_loop(0, out.shape[0] // 128, step, 0)
 
 
 def joined(skip, own, other, gain):
@@ -347,7 +353,7 @@
         out_shape=jax.ShapeDtypeStruct(skip.shape, bf),
         in_specs=[VMEM] * 4,
         out_specs=VMEM,
-        compiler_params=PARAMS,
+        compiler_params=limit(16),
     )(skip, own, other, gain.reshape(1, -1))
 
 
@@ -368,10 +374,13 @@
     near, far = [], []
     for c, order in enumerate(ORDERS):
         ring = around(parts[c], order[0])
-        near.append(placed(ring, order[0], [parts[c].shape[-1]])[0])
+        near.append(placed(ring, order[0], 0, parts[c].shape[-1]))
     for c, order in enumerate(ORDERS):
         ring = around(near[c], order[1])
-        far.append(placed(ring, order[1], stage_widths(c)))
+        both = []
+        for s, width in enumerate(stage_widths(c)):
+            both.append(placed(ring, order[1], s * 4 * CHANNELS, width))
+        far.append(both)
     blocks = [[around(far[c][s], ORDERS[c][2]) for c in range(3)] for s in range(2)]
 
     mixed = []
@@ -381,7 +390,8 @@
     own, other = mix_out_product(mixed, sum(blocks[0], []))
     first = joined(tokens, own, other, norm_first)
     first_other = swapped(first)
-    own, other = feed(first, first_other, sum(blocks[1], []))
+    sums = feed((0,), first, first_other, blocks[1][0])
+    own, other = feed((1, 2), first, first_other, blocks[1][1] + blocks[1][2], sums)
     return joined(first, own, other, norm_second)
 
 

time: 244 us -> 212 us (0.87)
  waiting for transfers between devices: 91 us -> 75.6 us
  Pallas kernels: 68.1 us -> 53.1 us
  local copies, waits for them, and re-layouts: 7.92 us -> 1.7 us
  starting transfers between devices: 76.2 us -> 81.1 us
    ppermute x36, waiting for transfers between devices: 87.8 us -> 72.6 us  [moved(): return lax.ppermute(block, REP_FS_TP, ring_pairs(axis, step))]
    pallas_call x2, Pallas kernels: 15.4 us -> 3.83 us  [joined(): pl.pallas_call(joined_kernel, out_shape=jax.ShapeDtypeStruct(skip.shape,...]
    unnamed x58 -> x28, local copies, waits for them, and re-layouts: 7.92 us -> 1.7 us
    ppermute x4, starting transfers between devices: 9.09 us -> 12.5 us  [swapped(): return lax.ppermute(x, 'tp', [(0, 1), (1, 0)])]
    pallas_call x3, Pallas kernels: 13.9 us -> 10.6 us  [mixer(): pl.pallas_call(functools.partial(mixer_kernel, order), out_shape=jax.Shap...]
    pallas_call x1, Pallas kernels: 8.32 us -> 5.04 us  [mix_out_product(): pl.pallas_call(mix_out_kernel, out_shape=[jax.ShapeDtypeStruct((rows // 2...]
    pallas_call x7 -> x11, Pallas kernels: 29.1 us -> 32.3 us  [the longest x2 23.3 us: feed(): pl.pallas_call(functools.partial(feed_kernel, parts), out_shape=[jax.Shap...]
  transfers between devices with their start and end apart: 40 -> 40, of which waited for: 15 -> 21; matrix products, arithmetic and copies ran while one was open for 0% -> 0% of each run, Pallas kernels for 9% -> 16%
where the time goes in v1:
time: 212 us
  starting transfers between devices  81.1 us (38%)
  waiting for transfers between devices  75.6 us (36%)
  Pallas kernels  53.1 us (25%)
    ppermute x36, waiting for transfers between devices, moved(): return lax.ppermute(block, REP_FS_TP, ring_pairs(axis, step))  72.6 us
    ppermute x36, starting transfers between devices, moved(): return lax.ppermute(block, REP_FS_TP, ring_pairs(axis, step))  68.6 us
    pallas_call x2, Pallas kernels, feed(): pl.pallas_call(functools.partial(feed_kernel, parts), out_shape=[jax.Shap...  23.3 us
    ppermute x4, starting transfers between devices, swapped(): return lax.ppermute(x, 'tp', [(0, 1), (1, 0)])  12.5 us
    pallas_call x3, Pallas kernels, mixer(): pl.pallas_call(functools.partial(mixer_kernel, order), out_shape=jax.Shap...  10.6 us
    pallas_call x9, Pallas kernels, placed(): pl.pallas_call(functools.partial(place_kernel, axis, start), out_shape=pl...  9.04 us
    pallas_call x1, Pallas kernels, mix_out_product(): pl.pallas_call(mix_out_kernel, out_shape=[jax.ShapeDtypeStruct((rows // 2...  5.04 us
  transfers between devices with their start and end apart: 40, of which 21 were waited for; matrix products, arithmetic and copies ran while one was open for 0% of the time, Pallas kernels for 16%

profile of v1, /device:TPU:1, one launch (start us, length us, event | category | flops | bytes accessed | tf_op | source)
XLA Modules:
  0.0 211.9 jit_solution(10434470782477672190)
XLA Ops:
  1.3 3.6 %collective-permute-start.19 = (bf16[32,2304]{1,0:T(8,128)(2,1)S(1)}, bf16[32,2304]{1,0:T(8,128)(2,1)S(1)}, u32[]{:S(2)}, u32[]{:S(2)}) collective-permute-start(bf16[32,2304]{1,0:T(8,128)(2,1)S(1)} %get-tuple-element.16.refs_0_), channel_id=1, source_target_pairs={{0,8},{1,25},{2,10},{3,27},{4,12},{5,29},{6,14},{7,31},{8,16},{9,1... | collective-permute-start | bytes 442376 | tf_op jit(solution)/shard_map/ppermute | solution.py:67
  7.4 3.4 %collective-permute-start.20 = (bf16[32,2304]{1,0:T(8,128)(2,1)S(1)}, bf16[32,2304]{1,0:T(8,128)(2,1)S(1)}, u32[]{:S(2)}, u32[]{:S(2)}) collective-permute-start(bf16[32,2304]{1,0:T(8,128)(2,1)S(1)} %collective-permute-done.19.refs_1_), channel_id=1, source_target_pairs={{0,8},{1,25},{2,10},{3,27},{4,12},{5,29},{6,14},{7,31},{8,16},{9,1... | collective-permute-start | bytes 442376 | tf_op jit(solution)/shard_map/ppermute | solution.py:67
  13.8 3.7 %collective-permute-start.22 = (bf16[4,32,2304]{2,1,0:T(8,128)(2,1)}, bf16[4,32,2304]{2,1,0:T(8,128)(2,1)S(1)}, u32[]{:S(2)}, u32[]{:S(2)}) collective-permute-start(bf16[4,32,2304]{2,1,0:T(8,128)(2,1)} %shard_map.107.refs_0_), channel_id=1, source_target_pairs={{0,32},{1,97},{2,34},{3,99},{4,36},{5,101},{6,38},{7,103},{8,40},{... | collective-permute-start | bytes 1769480 | tf_op jit(solution)/shard_map/ppermute | solution.py:67
  22.1 3.4 %collective-permute-start.11 = (bf16[32,2304]{1,0:T(8,128)(2,1)S(1)}, bf16[32,2304]{1,0:T(8,128)(2,1)S(1)}, u32[]{:S(2)}, u32[]{:S(2)}) collective-permute-start(bf16[32,2304]{1,0:T(8,128)(2,1)S(1)} %collective-permute-done.10.refs_1_), channel_id=1, source_target_pairs={{0,2},{1,7},{2,4},{3,1},{4,6},{5,3},{6,0},{7,5},{8,10},{9,15},{10,... | collective-permute-start | bytes 442376 | tf_op jit(solution)/shard_map/ppermute | solution.py:67
  26.3 3.1 %collective-permute-start.2 = (bf16[32,2560]{1,0:T(8,128)(2,1)S(1)}, bf16[32,2560]{1,0:T(8,128)(2,1)S(1)}, u32[]{:S(2)}, u32[]{:S(2)}) collective-permute-start(bf16[32,2560]{1,0:T(8,128)(2,1)S(1)} %collective-permute-done.1.refs_1_), channel_id=1, source_target_pairs={{0,32},{1,97},{2,34},{3,99},{4,36},{5,101},{6,38},{7,103},{8,40},{... | collective-permute-start | bytes 491528 | tf_op jit(solution)/shard_map/ppermute | solution.py:67
  30.3 3.4 %collective-permute-start.13 = (bf16[4,32,2304]{2,1,0:T(8,128)(2,1)}, bf16[4,32,2304]{2,1,0:T(8,128)(2,1)S(1)}, u32[]{:S(2)}, u32[]{:S(2)}) collective-permute-start(bf16[4,32,2304]{2,1,0:T(8,128)(2,1)} %shard_map.104.refs_0_), channel_id=1, source_target_pairs={{0,8},{1,25},{2,10},{3,27},{4,12},{5,29},{6,14},{7,31},{8,16},{9,1... | collective-permute-start | bytes 1769480 | tf_op jit(solution)/shard_map/ppermute | solution.py:67
  43.9 4.6 %collective-permute-start = (bf16[384,2048]{1,0:T(8,128)(2,1)S(1)}, bf16[384,2048]{1,0:T(8,128)(2,1)S(1)}, u32[]{:S(2)}, u32[]{:S(2)}) collective-permute-start(bf16[384,2048]{1,0:T(8,128)(2,1)S(1)} %copy-done.6), channel_id=1, source_target_pairs={{0,1},{1,0},{2,3},{3,2},{4,5},{5,4},{6,7},{7,6},{8,9},{9,8},{10,11... | collective-permute-start | bytes 4718600 | tf_op jit(solution)/shard_map/ppermute | solution.py:76
  48.5 3.1 %collective-permute-start.6 = (bf16[4,32,2560]{2,1,0:T(8,128)(2,1)}, bf16[4,32,2560]{2,1,0:T(8,128)(2,1)S(1)}, u32[]{:S(2)}, u32[]{:S(2)}) collective-permute-start(bf16[4,32,2560]{2,1,0:T(8,128)(2,1)} %shard_map.101.refs_0_), channel_id=1, source_target_pairs={{0,6},{1,3},{2,0},{3,5},{4,2},{5,7},{6,4},{7,1},{8,14},{9,11},{10,... | collective-permute-start | bytes 1966088 | tf_op jit(solution)/shard_map/ppermute | solution.py:67
  59.9 4.4 %collective-permute-done.6.refs_3_ = bf16[4,32,2560]{2,1,0:T(8,128)(2,1)S(1)} collective-permute-done((bf16[4,32,2560]{2,1,0:T(8,128)(2,1)}, bf16[4,32,2560]{2,1,0:T(8,128)(2,1)S(1)}, u32[]{:S(2)}, u32[]{:S(2)}) %collective-permute-start.6) | collective-permute-done | bytes 655392 | tf_op jit(solution)/shard_map/ppermute | solution.py:67
  68.4 3.4 %collective-permute-start.7 = (bf16[4,4,32,1024]{3,2,1,0:T(8,128)(2,1)}, bf16[4,4,32,1024]{3,2,1,0:T(8,128)(2,1)S(1)}, u32[]{:S(2)}, u32[]{:S(2)}) collective-permute-start(bf16[4,4,32,1024]{3,2,1,0:T(8,128)(2,1)} %shard_map.102.refs_0_.refs_3_), channel_id=1, source_target_pairs={{0,8},{1,25},{2,10},{3,27},{4,12},{5,29},{6,14},{7,31},{8,16},{9,1... | collective-permute-start | bytes 3145736 | tf_op jit(solution)/shard_map/ppermute | solution.py:67
  71.8 14.5 %collective-permute-done.25.refs_1_.refs_12_ = bf16[4,4,32,1024]{3,2,1,0:T(8,128)(2,1)S(1)} collective-permute-done((bf16[4,4,32,1024]{3,2,1,0:T(8,128)(2,1)}, bf16[4,4,32,1024]{3,2,1,0:T(8,128)(2,1)S(1)}, u32[]{:S(2)}, u32[]{:S(2)}) %collective-permute-start.25) | collective-permute-done | bytes 1048608 | tf_op jit(solution)/shard_map/ppermute | solution.py:67
  95.3 6.8 %collective-permute-done.26.refs_2_.refs_13_ = bf16[4,4,32,1024]{3,2,1,0:T(8,128)(2,1)S(1)} collective-permute-done((bf16[4,4,32,1024]{3,2,1,0:T(8,128)(2,1)S(1)}, bf16[4,4,32,1024]{3,2,1,0:T(8,128)(2,1)S(1)}, u32[]{:S(2)}, u32[]{:S(2)}) %collective-permute-start.26) | collective-permute-done | bytes 1048608 | tf_op jit(solution)/shard_map/ppermute | solution.py:67
  104.4 3.5 %shard_map.109.refs_2_ = bf16[768,256]{1,0:T(8,128)(2,1)S(1)} custom-call(bf16[384,2048]{1,0:T(8,128)(2,1)S(1)} %copy-done.6, bf16[384,2048]{1,0:T(8,128)(2,1)S(1)} %collective-permute-done.other, f32[3,256]{1,0:T(4,128)S(1)} %get-tuple-element.23.taps, bf16[4,4,32,1024]{3,2,1,0:T(8,128)(2,1)S(1)} %copy-done.4, ...), custom_call_target="tpu_custom_call" | custom-call | flops 2415919104 | bytes 8000000 | tf_op jit(solution)/shard_map/pallas_call | solution.py:202
  111.8 3.5 %shard_map.106.refs_1_ = bf16[768,256]{1,0:T(8,128)(2,1)S(1)} custom-call(bf16[384,2048]{1,0:T(8,128)(2,1)S(1)} %copy-done.6, bf16[384,2048]{1,0:T(8,128)(2,1)S(1)} %collective-permute-done.other, f32[3,256]{1,0:T(4,128)S(1)} %get-tuple-element.25.taps, bf16[4,4,32,1024]{3,2,1,0:T(8,128)(2,1)S(1)} %copy-done.5, ...), custom_call_target="tpu_custom_call" | custom-call | flops 2415919104 | bytes 8000000 | tf_op jit(solution)/shard_map/pallas_call | solution.py:202
  115.4 3.6 %shard_map.103.refs_0_ = bf16[768,256]{1,0:T(8,128)(2,1)S(1)} custom-call(bf16[384,2048]{1,0:T(8,128)(2,1)S(1)} %copy-done.6, bf16[384,2048]{1,0:T(8,128)(2,1)S(1)} %collective-permute-done.other, f32[3,256]{1,0:T(4,128)S(1)} %get-tuple-element.24.taps, bf16[4,4,32,1024]{3,2,1,0:T(8,128)(2,1)S(1)} %copy-done.3, ...), custom_call_target="tpu_custom_call" | custom-call | flops 2415919104 | bytes 8000000 | tf_op jit(solution)/shard_map/pallas_call | solution.py:202
  119.0 5.0 %shard_map.110 = (f32[384,2048]{1,0:T(8,128)S(1)}, bf16[384,2048]{1,0:T(8,128)(2,1)S(1)}) custom-call(bf16[768,256]{1,0:T(8,128)(2,1)S(1)} %shard_map.103.refs_0_, bf16[768,256]{1,0:T(8,128)(2,1)S(1)} %shard_map.106.refs_1_, bf16[768,256]{1,0:T(8,128)(2,1)S(1)} %shard_map.109.refs_2_, bf16[4,4,32,1024]{3,2,1,0:T(8,128)(2,1)S(1)} %copy-done.3, ...), custom_call_target="tpu_custom_call" | custom-call | flops 2415919104 | bytes 9000000 | tf_op jit(solution)/shard_map/pallas_call | solution.py:251
  124.0 5.8 %collective-permute-start.28 = (bf16[384,2048]{1,0:T(8,128)(2,1)S(1)}, bf16[384,2048]{1,0:T(8,128)(2,1)S(1)}, u32[]{:S(2)}, u32[]{:S(2)}) collective-permute-start(bf16[384,2048]{1,0:T(8,128)(2,1)S(1)} %get-tuple-element.18), channel_id=1, source_target_pairs={{0,1},{1,0},{2,3},{3,2},{4,5},{5,4},{6,7},{7,6},{8,9},{9,8},{10,11... | collective-permute-start | bytes 4718600 | tf_op jit(solution)/shard_map/ppermute | solution.py:76
  129.8 4.2 %collective-permute-done.36.refs_1_ = bf16[4,4,32,1536]{3,2,1,0:T(8,128)(2,1)S(1)} collective-permute-done((bf16[4,4,32,1536]{3,2,1,0:T(8,128)(2,1)}, bf16[4,4,32,1536]{3,2,1,0:T(8,128)(2,1)S(1)}, u32[]{:S(2)}, u32[]{:S(2)}) %collective-permute-start.36) | collective-permute-done | bytes 1572896 | tf_op jit(solution)/shard_map/ppermute | solution.py:67
  145.1 10.4 %collective-permute-done.30.refs_1_ = bf16[4,4,32,1280]{3,2,1,0:T(8,128)(2,1)S(1)} collective-permute-done((bf16[4,4,32,1280]{3,2,1,0:T(8,128)(2,1)}, bf16[4,4,32,1280]{3,2,1,0:T(8,128)(2,1)S(1)}, u32[]{:S(2)}, u32[]{:S(2)}) %collective-permute-start.30) | collective-permute-done | bytes 1310752 | tf_op jit(solution)/shard_map/ppermute | solution.py:67
  159.4 3.9 %collective-permute-done.38.refs_3_ = bf16[4,4,32,1536]{3,2,1,0:T(8,128)(2,1)S(1)} collective-permute-done((bf16[4,4,32,1536]{3,2,1,0:T(8,128)(2,1)S(1)}, bf16[4,4,32,1536]{3,2,1,0:T(8,128)(2,1)S(1)}, u32[]{:S(2)}, u32[]{:S(2)}) %collective-permute-start.38) | collective-permute-done | bytes 1572896 | tf_op jit(solution)/shard_map/ppermute | solution.py:67
  169.6 8.5 %shard_map.115 = (f32[384,2048]{1,0:T(8,128)S(1)}, f32[384,2048]{1,0:T(8,128)S(1)}) custom-call(bf16[384,2048]{1,0:T(8,128)(2,1)S(1)} %shard_map.111.first_own.skip, bf16[384,2048]{1,0:T(8,128)(2,1)S(1)} %collective-permute-done.29.first_other, bf16[4,4,32,1536]{3,2,1,0:T(8,128)(2,1)S(1)} %copy-done.7, ...), custom_call_target="tpu_custom_call" | custom-call | flops 4831838208 | bytes 20000000 | tf_op jit(solution)/shard_map/pallas_call | solution.py:314
  180.9 6.2 %collective-permute-done.31.refs_2_ = bf16[4,4,32,1280]{3,2,1,0:T(8,128)(2,1)S(1)} collective-permute-done((bf16[4,4,32,1280]{3,2,1,0:T(8,128)(2,1)S(1)}, bf16[4,4,32,1280]{3,2,1,0:T(8,128)(2,1)S(1)}, u32[]{:S(2)}, u32[]{:S(2)}) %collective-permute-start.31) | collective-permute-done | bytes 1310752 | tf_op jit(solution)/shard_map/ppermute | solution.py:67
  189.5 14.7 %shard_map.116 = (f32[384,2048]{1,0:T(8,128)S(1)}, bf16[384,2048]{1,0:T(8,128)(2,1)S(1)}) custom-call(bf16[384,2048]{1,0:T(8,128)(2,1)S(1)} %shard_map.111.first_own.skip, bf16[384,2048]{1,0:T(8,128)(2,1)S(1)} %collective-permute-done.29.first_other, bf16[4,4,32,1280]{3,2,1,0:T(8,128)(2,1)S(1)} %copy-done.8, ...), custom_call_target="tpu_custom_call" | custom-call | flops 8053063680 | bytes 20000000 | tf_op jit(solution)/shard_map/pallas_call | solution.py:314
  206.3 3.0 %collective-permute-done.39.other = bf16[384,2048]{1,0:T(8,128)(2,1)S(1)} collective-permute-done((bf16[384,2048]{1,0:T(8,128)(2,1)S(1)}, bf16[384,2048]{1,0:T(8,128)(2,1)S(1)}, u32[]{:S(2)}, u32[]{:S(2)}) %collective-permute-start.39) | collective-permute-done | bytes 1572896 | tf_op jit(solution)/shard_map/ppermute | solution.py:76
  (103 shorter events, 81.5 us)
Async XLA Ops:
  13.8 23.1 %collective-permute-start.22 = (bf16[4,32,2304]{2,1,0:T(8,128)(2,1)}, bf16[4,32,2304]{2,1,0:T(8,128)(2,1)S(1)}, u32[]{:S(2)}, u32[]{:S(2)}) collective-permute-start(bf16[4,32,2304]{2,1,0:T(8,128)(2,1)} %shard_map.107.refs_0_), channel_id=1, source_target_pairs={{0,32},{1,97},{2,34},{3,99},{4,36},{5,101},{6,38},{7,103},{8,40},{... | collective-permute-start | bytes 1769480 | tf_op jit(solution)/shard_map/ppermute | solution.py:67
  43.9 43.3 %collective-permute-start = (bf16[384,2048]{1,0:T(8,128)(2,1)S(1)}, bf16[384,2048]{1,0:T(8,128)(2,1)S(1)}, u32[]{:S(2)}, u32[]{:S(2)}) collective-permute-start(bf16[384,2048]{1,0:T(8,128)(2,1)S(1)} %copy-done.6), channel_id=1, source_target_pairs={{0,1},{1,0},{2,3},{3,2},{4,5},{5,4},{6,7},{7,6},{8,9},{9,8},{10,11... | collective-permute-start | bytes 4718600 | tf_op jit(solution)/shard_map/ppermute | solution.py:76
  48.5 15.8 %collective-permute-start.6 = (bf16[4,32,2560]{2,1,0:T(8,128)(2,1)}, bf16[4,32,2560]{2,1,0:T(8,128)(2,1)S(1)}, u32[]{:S(2)}, u32[]{:S(2)}) collective-permute-start(bf16[4,32,2560]{2,1,0:T(8,128)(2,1)} %shard_map.101.refs_0_), channel_id=1, source_target_pairs={{0,6},{1,3},{2,0},{3,5},{4,2},{5,7},{6,4},{7,1},{8,14},{9,11},{10,... | collective-permute-start | bytes 1966088 | tf_op jit(solution)/shard_map/ppermute | solution.py:67
  51.6 15.8 %collective-permute-start.5 = (bf16[4,32,2560]{2,1,0:T(8,128)(2,1)S(1)}, bf16[4,32,2560]{2,1,0:T(8,128)(2,1)S(1)}, u32[]{:S(2)}, u32[]{:S(2)}) collective-permute-start(bf16[4,32,2560]{2,1,0:T(8,128)(2,1)S(1)} %collective-permute-done.4.refs_1_), channel_id=1, source_target_pairs={{0,2},{1,7},{2,4},{3,1},{4,6},{5,3},{6,0},{7,5},{8,10},{9,15},{10,... | collective-permute-start | bytes 1966088 | tf_op jit(solution)/shard_map/ppermute | solution.py:67
  54.0 32.2 %collective-permute-start.25 = (bf16[4,4,32,1024]{3,2,1,0:T(8,128)(2,1)}, bf16[4,4,32,1024]{3,2,1,0:T(8,128)(2,1)S(1)}, u32[]{:S(2)}, u32[]{:S(2)}) collective-permute-start(bf16[4,4,32,1024]{3,2,1,0:T(8,128)(2,1)} %shard_map.108.refs_0_.refs_11_), channel_id=1, source_target_pairs={{0,2},{1,7},{2,4},{3,1},{4,6},{5,3},{6,0},{7,5},{8,10},{9,15},{10,... | collective-permute-start | bytes 3145736 | tf_op jit(solution)/shard_map/ppermute | solution.py:67
  57.1 31.9 %collective-permute-start.16 = (bf16[4,4,32,1024]{3,2,1,0:T(8,128)(2,1)}, bf16[4,4,32,1024]{3,2,1,0:T(8,128)(2,1)S(1)}, u32[]{:S(2)}, u32[]{:S(2)}) collective-permute-start(bf16[4,4,32,1024]{3,2,1,0:T(8,128)(2,1)} %shard_map.105.refs_0_.refs_7_), channel_id=1, source_target_pairs={{0,32},{1,97},{2,34},{3,99},{4,36},{5,101},{6,38},{7,103},{8,40},{... | collective-permute-start | bytes 3145736 | tf_op jit(solution)/shard_map/ppermute | solution.py:67
  64.3 27.0 %collective-permute-start.27 = (bf16[4,4,32,1024]{3,2,1,0:T(8,128)(2,1)S(1)}, bf16[4,4,32,1024]{3,2,1,0:T(8,128)(2,1)S(1)}, u32[]{:S(2)}, u32[]{:S(2)}) collective-permute-start(bf16[4,4,32,1024]{3,2,1,0:T(8,128)(2,1)S(1)} %copy-done.4), channel_id=1, source_target_pairs={{0,6},{1,3},{2,0},{3,5},{4,2},{5,7},{6,4},{7,1},{8,14},{9,11},{10,... | collective-permute-start | bytes 3145736 | tf_op jit(solution)/shard_map/ppermute | solution.py:67
  68.4 22.9 %collective-permute-start.7 = (bf16[4,4,32,1024]{3,2,1,0:T(8,128)(2,1)}, bf16[4,4,32,1024]{3,2,1,0:T(8,128)(2,1)S(1)}, u32[]{:S(2)}, u32[]{:S(2)}) collective-permute-start(bf16[4,4,32,1024]{3,2,1,0:T(8,128)(2,1)} %shard_map.102.refs_0_.refs_3_), channel_id=1, source_target_pairs={{0,8},{1,25},{2,10},{3,27},{4,12},{5,29},{6,14},{7,31},{8,16},{9,1... | collective-permute-start | bytes 3145736 | tf_op jit(solution)/shard_map/ppermute | solution.py:67
  86.3 15.8 %collective-permute-start.26 = (bf16[4,4,32,1024]{3,2,1,0:T(8,128)(2,1)S(1)}, bf16[4,4,32,1024]{3,2,1,0:T(8,128)(2,1)S(1)}, u32[]{:S(2)}, u32[]{:S(2)}) collective-permute-start(bf16[4,4,32,1024]{3,2,1,0:T(8,128)(2,1)S(1)} %collective-permute-done.25.refs_1_.refs_12_), channel_id=1, source_target_pairs={{0,2},{1,7},{2,4},{3,1},{4,6},{5,3},{6,0},{7,5},{8,10},{9,15},{10,... | collective-permute-start | bytes 3145736 | tf_op jit(solution)/shard_map/ppermute | solution.py:67
  87.1 22.2 %collective-permute-start.18 = (bf16[4,4,32,1024]{3,2,1,0:T(8,128)(2,1)S(1)}, bf16[4,4,32,1024]{3,2,1,0:T(8,128)(2,1)S(1)}, u32[]{:S(2)}, u32[]{:S(2)}) collective-permute-start(bf16[4,4,32,1024]{3,2,1,0:T(8,128)(2,1)S(1)} %copy-done.5), channel_id=1, source_target_pairs={{0,96},{1,33},{2,98},{3,35},{4,100},{5,37},{6,102},{7,39},{8,104},... | collective-permute-start | bytes 3145736 | tf_op jit(solution)/shard_map/ppermute | solution.py:67
  89.0 22.8 %collective-permute-start.17 = (bf16[4,4,32,1024]{3,2,1,0:T(8,128)(2,1)S(1)}, bf16[4,4,32,1024]{3,2,1,0:T(8,128)(2,1)S(1)}, u32[]{:S(2)}, u32[]{:S(2)}) collective-permute-start(bf16[4,4,32,1024]{3,2,1,0:T(8,128)(2,1)S(1)} %collective-permute-done.16.refs_1_.refs_8_), channel_id=1, source_target_pairs={{0,32},{1,97},{2,34},{3,99},{4,36},{5,101},{6,38},{7,103},{8,40},{... | collective-permute-start | bytes 3145736 | tf_op jit(solution)/shard_map/ppermute | solution.py:67
  91.3 24.0 %collective-permute-start.9 = (bf16[4,4,32,1024]{3,2,1,0:T(8,128)(2,1)}, bf16[4,4,32,1024]{3,2,1,0:T(8,128)(2,1)S(1)}, u32[]{:S(2)}, u32[]{:S(2)}) collective-permute-start(bf16[4,4,32,1024]{3,2,1,0:T(8,128)(2,1)} %shard_map.102.refs_0_.refs_3_), channel_id=1, source_target_pairs={{0,24},{1,9},{2,26},{3,11},{4,28},{5,13},{6,30},{7,15},{8,0},{9,17... | collective-permute-start | bytes 3145736 | tf_op jit(solution)/shard_map/ppermute | solution.py:67
  91.3 24.0 %collective-permute-start.8 = (bf16[4,4,32,1024]{3,2,1,0:T(8,128)(2,1)S(1)}, bf16[4,4,32,1024]{3,2,1,0:T(8,128)(2,1)S(1)}, u32[]{:S(2)}, u32[]{:S(2)}) collective-permute-start(bf16[4,4,32,1024]{3,2,1,0:T(8,128)(2,1)S(1)} %collective-permute-done.7.refs_1_.refs_4_), channel_id=1, source_target_pairs={{0,8},{1,25},{2,10},{3,27},{4,12},{5,29},{6,14},{7,31},{8,16},{9,1... | collective-permute-start | bytes 3145736 | tf_op jit(solution)/shard_map/ppermute | solution.py:67
  102.1 31.9 %collective-permute-start.36 = (bf16[4,4,32,1536]{3,2,1,0:T(8,128)(2,1)}, bf16[4,4,32,1536]{3,2,1,0:T(8,128)(2,1)S(1)}, u32[]{:S(2)}, u32[]{:S(2)}) collective-permute-start(bf16[4,4,32,1536]{3,2,1,0:T(8,128)(2,1)} %shard_map.114.refs_0_), channel_id=1, source_target_pairs={{0,8},{1,25},{2,10},{3,27},{4,12},{5,29},{6,14},{7,31},{8,16},{9,1... | collective-permute-start | bytes 4718600 | tf_op jit(solution)/shard_map/ppermute | solution.py:67
  124.0 19.6 %collective-permute-start.28 = (bf16[384,2048]{1,0:T(8,128)(2,1)S(1)}, bf16[384,2048]{1,0:T(8,128)(2,1)S(1)}, u32[]{:S(2)}, u32[]{:S(2)}) collective-permute-start(bf16[384,2048]{1,0:T(8,128)(2,1)S(1)} %get-tuple-element.18), channel_id=1, source_target_pairs={{0,1},{1,0},{2,3},{3,2},{4,5},{5,4},{6,7},{7,6},{8,9},{9,8},{10,11... | collective-permute-start | bytes 4718600 | tf_op jit(solution)/shard_map/ppermute | solution.py:76
  129.8 33.5 %collective-permute-start.38 = (bf16[4,4,32,1536]{3,2,1,0:T(8,128)(2,1)S(1)}, bf16[4,4,32,1536]{3,2,1,0:T(8,128)(2,1)S(1)}, u32[]{:S(2)}, u32[]{:S(2)}) collective-permute-start(bf16[4,4,32,1536]{3,2,1,0:T(8,128)(2,1)S(1)} %copy-done.7), channel_id=1, source_target_pairs={{0,24},{1,9},{2,26},{3,11},{4,28},{5,13},{6,30},{7,15},{8,0},{9,17... | collective-permute-start | bytes 4718600 | tf_op jit(solution)/shard_map/ppermute | solution.py:67
  134.0 33.8 %collective-permute-start.37 = (bf16[4,4,32,1536]{3,2,1,0:T(8,128)(2,1)S(1)}, bf16[4,4,32,1536]{3,2,1,0:T(8,128)(2,1)S(1)}, u32[]{:S(2)}, u32[]{:S(2)}) collective-permute-start(bf16[4,4,32,1536]{3,2,1,0:T(8,128)(2,1)S(1)} %collective-permute-done.36.refs_1_), channel_id=1, source_target_pairs={{0,8},{1,25},{2,10},{3,27},{4,12},{5,29},{6,14},{7,31},{8,16},{9,1... | collective-permute-start | bytes 4718600 | tf_op jit(solution)/shard_map/ppermute | solution.py:67
  138.1 17.4 %collective-permute-start.30 = (bf16[4,4,32,1280]{3,2,1,0:T(8,128)(2,1)}, bf16[4,4,32,1280]{3,2,1,0:T(8,128)(2,1)S(1)}, u32[]{:S(2)}, u32[]{:S(2)}) collective-permute-start(bf16[4,4,32,1280]{3,2,1,0:T(8,128)(2,1)} %shard_map.112.refs_0_), channel_id=1, source_target_pairs={{0,32},{1,97},{2,34},{3,99},{4,36},{5,101},{6,38},{7,103},{8,40},{... | collective-permute-start | bytes 3932168 | tf_op jit(solution)/shard_map/ppermute | solution.py:67
  141.8 17.0 %collective-permute-start.33 = (bf16[4,4,32,1280]{3,2,1,0:T(8,128)(2,1)}, bf16[4,4,32,1280]{3,2,1,0:T(8,128)(2,1)S(1)}, u32[]{:S(2)}, u32[]{:S(2)}) collective-permute-start(bf16[4,4,32,1280]{3,2,1,0:T(8,128)(2,1)} %shard_map.113.refs_4_), channel_id=1, source_target_pairs={{0,2},{1,7},{2,4},{3,1},{4,6},{5,3},{6,0},{7,5},{8,10},{9,15},{10,... | collective-permute-start | bytes 3932168 | tf_op jit(solution)/shard_map/ppermute | solution.py:67
  145.0 24.6 %collective-permute-start.29 = (bf16[384,2048]{1,0:T(8,128)(2,1)S(1)}, bf16[384,2048]{1,0:T(8,128)(2,1)S(1)}, u32[]{:S(2)}, u32[]{:S(2)}) collective-permute-start(bf16[384,2048]{1,0:T(8,128)(2,1)S(1)} %shard_map.111.first_own.skip), channel_id=1, source_target_pairs={{0,1},{1,0},{2,3},{3,2},{4,5},{5,4},{6,7},{7,6},{8,9},{9,8},{10,11... | collective-permute-start | bytes 4718600 | tf_op jit(solution)/shard_map/ppermute | solution.py:76
  155.5 24.3 %collective-permute-start.32 = (bf16[4,4,32,1280]{3,2,1,0:T(8,128)(2,1)S(1)}, bf16[4,4,32,1280]{3,2,1,0:T(8,128)(2,1)S(1)}, u32[]{:S(2)}, u32[]{:S(2)}) collective-permute-start(bf16[4,4,32,1280]{3,2,1,0:T(8,128)(2,1)S(1)} %copy-done.8), channel_id=1, source_target_pairs={{0,96},{1,33},{2,98},{3,35},{4,100},{5,37},{6,102},{7,39},{8,104},... | collective-permute-start | bytes 3932168 | tf_op jit(solution)/shard_map/ppermute | solution.py:67
  158.8 22.1 %collective-permute-start.35 = (bf16[4,4,32,1280]{3,2,1,0:T(8,128)(2,1)S(1)}, bf16[4,4,32,1280]{3,2,1,0:T(8,128)(2,1)S(1)}, u32[]{:S(2)}, u32[]{:S(2)}) collective-permute-start(bf16[4,4,32,1280]{3,2,1,0:T(8,128)(2,1)S(1)} %copy-done.9), channel_id=1, source_target_pairs={{0,6},{1,3},{2,0},{3,5},{4,2},{5,7},{6,4},{7,1},{8,14},{9,11},{10,... | collective-permute-start | bytes 3932168 | tf_op jit(solution)/shard_map/ppermute | solution.py:67
  163.3 23.8 %collective-permute-start.31 = (bf16[4,4,32,1280]{3,2,1,0:T(8,128)(2,1)S(1)}, bf16[4,4,32,1280]{3,2,1,0:T(8,128)(2,1)S(1)}, u32[]{:S(2)}, u32[]{:S(2)}) collective-permute-start(bf16[4,4,32,1280]{3,2,1,0:T(8,128)(2,1)S(1)} %collective-permute-done.30.refs_1_), channel_id=1, source_target_pairs={{0,32},{1,97},{2,34},{3,99},{4,36},{5,101},{6,38},{7,103},{8,40},{... | collective-permute-start | bytes 3932168 | tf_op jit(solution)/shard_map/ppermute | solution.py:67
  167.8 21.7 %collective-permute-start.34 = (bf16[4,4,32,1280]{3,2,1,0:T(8,128)(2,1)S(1)}, bf16[4,4,32,1280]{3,2,1,0:T(8,128)(2,1)S(1)}, u32[]{:S(2)}, u32[]{:S(2)}) collective-permute-start(bf16[4,4,32,1280]{3,2,1,0:T(8,128)(2,1)S(1)} %collective-permute-done.33.refs_5_), channel_id=1, source_target_pairs={{0,2},{1,7},{2,4},{3,1},{4,6},{5,3},{6,0},{7,5},{8,10},{9,15},{10,... | collective-permute-start | bytes 3932168 | tf_op jit(solution)/shard_map/ppermute | solution.py:67
  (30 other events, 406.9 us)

commit v2 on v1

--- a/solution.py
+++ b/solution.py
@@ -16,7 +16,7 @@
 REP_FS_TP = ("rep", "fs_0", "fs_1", "fs_2", "tp")
 ORDERS = ("zxy", "xyz", "yzx")
 CHANNELS = 256
-HIDDEN = (768, 640, 640)
+HIDDEN = ((384, 384, 256), (384, 256, 384))
 
 
 residual_scale = 2.0**0.25
@@ -35,7 +35,7 @@
 
 
 def stage_widths(part):
-    return [4 * CHANNELS, 2 * HIDDEN[part]]
+    return [4 * CHANNELS] + [2 * HIDDEN[s][part] for s in range(2)]
 
 
 def position(axis):
@@ -98,10 +98,11 @@
         for w in (outer, inner, value, mix):
             out[:, at : at + CHANNELS] = w[:, part * CHANNELS : (part + 1) * CHANNELS].astype(bf)
             at += CHANNELS
-        start, n = sum(HIDDEN[:part]), HIDDEN[part]
-        for w in (up, down):
-            out[:, at : at + n] = w[:, start : start + n].astype(bf)
-            at += n
+        for s in range(2):
+            start, n = s * sum(HIDDEN[0]) + sum(HIDDEN[s][:part]), HIDDEN[s][part]
+            for w in (up, down):
+                out[:, at : at + n] = w[:, start : start + n].astype(bf)
+                at += n
 
 
 def pieces(*weights):
@@ -116,39 +117,38 @@
     )(*in_hbm(weights))
 
 
-def place_kernel(axis, start, *refs):
-    parts, out, sems = refs[:4], refs[4], refs[5]
-    width = out.shape[-1]
-    finish(
-        [
-            pltpu.make_async_copy(
-                part.at[..., pl.ds(start, width)], out.at[source(axis, k)], sems.at[k]
-            )
-            for k, part in enumerate(parts)
-        ]
-    )
-
-
-def placed(parts, axis, start, width):
-    return pl.pallas_call(
-        functools.partial(place_kernel, axis, start),
-        out_shape=pltpu.HBM((4, *parts[0].shape[:-1], width), bf),
+def place_kernel(axis, columns, *refs):
+    parts, outs, sems = refs[:4], refs[4:-1], refs[-1]
+    copies = []
+    for k, part in enumerate(parts):
+        for (start, width), out in zip(columns, outs):
+            src, dst = part.at[..., pl.ds(start, width)], out.at[source(axis, k)]
+            copies.append(pltpu.make_async_copy(src, dst, sems.at[len(copies)]))
+    finish(copies)
+
+
+def placed(parts, axis, columns):
+    lead = parts[0].shape[:-1]
+    return pl.pallas_call(
+        functools.partial(place_kernel, axis, columns),
+        out_shape=[pltpu.HBM((4, *lead, width), bf) for _, width in columns],
         in_specs=[HBM] * 4,
-        out_specs=HBM,
-        scratch_shapes=[pltpu.SemaphoreType.DMA((4,))],
+        out_specs=[HBM] * len(columns),
+        scratch_shapes=[pltpu.SemaphoreType.DMA((4 * len(columns),))],
         compiler_params=limit(4),
     )(*parts)
 
 
-def fill(order, blocks, start, width, whole, at, sems, used):
+def fill(order, blocks, start, width, whole, at, sems, used, shift=0):
     copies = []
 
     def add(src, dst):
         copies.append(pltpu.make_async_copy(src, dst, sems.at[used + len(copies)]))
 
-    cs, cd = pl.ds(start, width), pl.ds(at, width)
+    cd = pl.ds(at, width)
     for k, block in enumerate(blocks):
         p = source(order[2], k)
+        cs = pl.ds(start + (shift if k == 3 else 0), width)
         if order == "xyz":
             add(block.at[:, :, :, cs], whole.at[p & 1, :, :, p >> 1, :, cd])
         else:
@@ -268,21 +268,22 @@
     )(*mixed, *blocks)
 
 
-def feed_kernel(parts, first_own, first_other, *refs):
-    blocks, refs = refs[: 4 * len(parts)], refs[4 * len(parts) :]
+def feed_kernel(stage, first_own, first_other, *refs):
+    blocks, refs = refs[:12], refs[12:]
     more = None
     if len(refs) == 9:
         more, refs = refs[:2], refs[2:]
     own, other, x, up, down, hidden, sems = refs
     tokens = both_tokens(first_own, first_other, x, sems, 0)
     used = 2
-    ends = [sum(HIDDEN[c] for c in parts[: i + 1]) for i in range(len(parts))]
+    ends = [sum(HIDDEN[stage][: c + 1]) for c in range(3)]
     ups, downs = [], []
     for second, whole, sets in ((0, up, ups), (1, down, downs)):
-        for i, c in enumerate(parts):
-            n = HIDDEN[c]
-            ring = blocks[4 * i : 4 * i + 4]
-            sets.append(fill(ORDERS[c], ring, second * n, n, whole, ends[i] - n, sems, used))
+        for c, order in enumerate(ORDERS):
+            n = HIDDEN[stage][c]
+            ring = blocks[4 * c : 4 * c + 4]
+            shift = stage * 2 * HIDDEN[0][c]
+            sets.append(fill(order, ring, second * n, n, whole, ends[c] - n, sems, used, shift))
             used += len(sets[-1])
     for copy in sum(ups + downs, tokens):
         copy.start()
@@ -306,13 +307,13 @@
     projected(hidden, down, own, other, more)
 
 
-def feed(parts, own, other, blocks, more=None):
+def feed(stage, own, other, blocks, more=None):
     half = own.shape[0]
-    width = sum(HIDDEN[c] for c in parts)
+    width = sum(HIDDEN[stage])
     extra = [] if more is None else list(more)
     last = jnp.float32 if more is None else bf
     return pl.pallas_call(
-        functools.partial(feed_kernel, parts),
+        functools.partial(feed_kernel, stage),
         out_shape=[
             jax.ShapeDtypeStruct((half, D), jnp.float32),
             jax.ShapeDtypeStruct((half, D), last),
@@ -371,27 +372,32 @@
 ):
     parts = pieces(outer_weight, inner_weight, value_weight, mix_out.T, up_weight, down_weight.T)
     tokens_other = swapped(tokens)
-    near, far = [], []
+    near = []
     for c, order in enumerate(ORDERS):
         ring = around(parts[c], order[0])
-        near.append(placed(ring, order[0], 0, parts[c].shape[-1]))
+        near += placed(ring, order[0], [(0, parts[c].shape[-1])])
+    blocks = [[], [], []]
     for c, order in enumerate(ORDERS):
         ring = around(near[c], order[1])
-        both = []
-        for s, width in enumerate(stage_widths(c)):
-            both.append(placed(ring, order[1], s * 4 * CHANNELS, width))
-        far.append(both)
-    blocks = [[around(far[c][s], ORDERS[c][2]) for c in range(3)] for s in range(2)]
+        head, one, two = stage_widths(c)
+        (own,) = placed(ring, order[1], [(0, head)])
+        columns = [(head, one), (head + one, two), (head, one + two)]
+        *own_stages, own_both = placed(ring, order[1], columns)
+        blocks[0] += around(own, order[2])
+        back = moved(own_both, order[2], 3)
+        for s, own in enumerate(own_stages, 1):
+            ahead = moved(own, order[2], 1)
+            blocks[s] += [own, ahead, moved(ahead, order[2], 1), back]
 
     mixed = []
     for c, order in enumerate(ORDERS):
         taps = conv_taps[:, c * CHANNELS : (c + 1) * CHANNELS]
-        mixed.append(mixer(order, tokens, tokens_other, taps, blocks[0][c]))
-    own, other = mix_out_product(mixed, sum(blocks[0], []))
+        mixed.append(mixer(order, tokens, tokens_other, taps, blocks[0][4 * c : 4 * c + 4]))
+    own, other = mix_out_product(mixed, blocks[0])
     first = joined(tokens, own, other, norm_first)
     first_other = swapped(first)
-    sums = feed((0,), first, first_other, blocks[1][0])
-    own, other = feed((1, 2), first, first_other, blocks[1][1] + blocks[1][2], sums)
+    sums = feed(0, first, first_other, blocks[1])
+    own, other = feed(1, first, first_other, blocks[2], sums)
     return joined(first, own, other, norm_second)
 
 

time: 212 us -> 231 us (1.090)
  starting transfers between devices: 81.1 us -> 94 us
  Pallas kernels: 53.1 us -> 57.6 us
    ppermute x36 -> x42, starting transfers between devices: 68.6 us -> 77.4 us  [moved(): return lax.ppermute(block, REP_FS_TP, ring_pairs(axis, step))]
    pallas_call x11, Pallas kernels: 32.3 us -> 36.8 us  [the longest x2 26.2 us: feed(): pl.pallas_call(functools.partial(feed_kernel, stage), out_shape=[jax.Shap...]
    ppermute x4, starting transfers between devices: 12.5 us -> 16.6 us  [swapped(): return lax.ppermute(x, 'tp', [(0, 1), (1, 0)])]
    ppermute x36 -> x42, waiting for transfers between devices: 72.6 us -> 73.7 us  [moved(): return lax.ppermute(block, REP_FS_TP, ring_pairs(axis, step))]
  transfers between devices with their start and end apart: 40 -> 46, of which waited for: 21 -> 19; matrix products, arithmetic and copies ran while one was open for 0% -> 0% of each run, Pallas kernels for 16% -> 13%
where the time goes in v2:
time: 231 us; the launch traced here: 230 us
  starting transfers between devices  94 us (41%)
  waiting for transfers between devices  76.7 us (33%)
  Pallas kernels  57.6 us (25%)
    ppermute x42, starting transfers between devices, moved(): return lax.ppermute(block, REP_FS_TP, ring_pairs(axis, step))  77.4 us
    ppermute x42, waiting for transfers between devices, moved(): return lax.ppermute(block, REP_FS_TP, ring_pairs(axis, step))  73.7 us
    pallas_call x2, Pallas kernels, feed(): pl.pallas_call(functools.partial(feed_kernel, stage), out_shape=[jax.Shap...  26.2 us
    ppermute x4, starting transfers between devices, swapped(): return lax.ppermute(x, 'tp', [(0, 1), (1, 0)])  16.6 us
    pallas_call x3, Pallas kernels, mixer(): pl.pallas_call(functools.partial(mixer_kernel, order), out_shape=jax.Shap...  10.6 us
    pallas_call x9, Pallas kernels, placed(): pl.pallas_call(functools.partial(place_kernel, axis, columns), out_shape=...  10.6 us
    pallas_call x1, Pallas kernels, mix_out_product(): pl.pallas_call(mix_out_kernel, out_shape=[jax.ShapeDtypeStruct((rows // 2...  5.04 us
  transfers between devices with their start and end apart: 46, of which 19 were waited for; matrix products, arithmetic and copies ran while one was open for 0% of the time, Pallas kernels for 13%

profile of v2, /device:TPU:1, one launch (start us, length us, event | category | flops | bytes accessed | tf_op | source)
XLA Modules:
  0.0 230.4 jit_solution(23745329451316555)
XLA Ops:
  1.3 3.6 %collective-permute-start.19 = (bf16[32,2304]{1,0:T(8,128)(2,1)S(1)}, bf16[32,2304]{1,0:T(8,128)(2,1)S(1)}, u32[]{:S(2)}, u32[]{:S(2)}) collective-permute-start(bf16[32,2304]{1,0:T(8,128)(2,1)S(1)} %get-tuple-element.25.refs_0_), channel_id=1, source_target_pairs={{0,8},{1,25},{2,10},{3,27},{4,12},{5,29},{6,14},{7,31},{8,16},{9,1... | collective-permute-start | bytes 442376 | tf_op jit(solution)/shard_map/ppermute | solution.py:67
  7.4 3.4 %collective-permute-start.20 = (bf16[32,2304]{1,0:T(8,128)(2,1)S(1)}, bf16[32,2304]{1,0:T(8,128)(2,1)S(1)}, u32[]{:S(2)}, u32[]{:S(2)}) collective-permute-start(bf16[32,2304]{1,0:T(8,128)(2,1)S(1)} %collective-permute-done.19.refs_1_), channel_id=1, source_target_pairs={{0,8},{1,25},{2,10},{3,27},{4,12},{5,29},{6,14},{7,31},{8,16},{9,1... | collective-permute-start | bytes 442376 | tf_op jit(solution)/shard_map/ppermute | solution.py:67
  13.8 3.7 %collective-permute-start.22 = (bf16[4,32,2304]{2,1,0:T(8,128)(2,1)}, bf16[4,32,2304]{2,1,0:T(8,128)(2,1)S(1)}, u32[]{:S(2)}, u32[]{:S(2)}) collective-permute-start(bf16[4,32,2304]{2,1,0:T(8,128)(2,1)} %shard_map.107.refs_0_), channel_id=1, source_target_pairs={{0,32},{1,97},{2,34},{3,99},{4,36},{5,101},{6,38},{7,103},{8,40},{... | collective-permute-start | bytes 1769480 | tf_op jit(solution)/shard_map/ppermute | solution.py:67
  22.1 3.4 %collective-permute-start.11 = (bf16[32,2304]{1,0:T(8,128)(2,1)S(1)}, bf16[32,2304]{1,0:T(8,128)(2,1)S(1)}, u32[]{:S(2)}, u32[]{:S(2)}) collective-permute-start(bf16[32,2304]{1,0:T(8,128)(2,1)S(1)} %collective-permute-done.10.refs_1_), channel_id=1, source_target_pairs={{0,2},{1,7},{2,4},{3,1},{4,6},{5,3},{6,0},{7,5},{8,10},{9,15},{10,... | collective-permute-start | bytes 442376 | tf_op jit(solution)/shard_map/ppermute | solution.py:67
  26.3 3.1 %collective-permute-start.2 = (bf16[32,2560]{1,0:T(8,128)(2,1)S(1)}, bf16[32,2560]{1,0:T(8,128)(2,1)S(1)}, u32[]{:S(2)}, u32[]{:S(2)}) collective-permute-start(bf16[32,2560]{1,0:T(8,128)(2,1)S(1)} %collective-permute-done.1.refs_1_), channel_id=1, source_target_pairs={{0,32},{1,97},{2,34},{3,99},{4,36},{5,101},{6,38},{7,103},{8,40},{... | collective-permute-start | bytes 491528 | tf_op jit(solution)/shard_map/ppermute | solution.py:67
  30.3 3.5 %collective-permute-start.13 = (bf16[4,32,2304]{2,1,0:T(8,128)(2,1)}, bf16[4,32,2304]{2,1,0:T(8,128)(2,1)S(1)}, u32[]{:S(2)}, u32[]{:S(2)}) collective-permute-start(bf16[4,32,2304]{2,1,0:T(8,128)(2,1)} %shard_map.104.refs_0_), channel_id=1, source_target_pairs={{0,8},{1,25},{2,10},{3,27},{4,12},{5,29},{6,14},{7,31},{8,16},{9,1... | collective-permute-start | bytes 1769480 | tf_op jit(solution)/shard_map/ppermute | solution.py:67
  43.9 4.5 %collective-permute-start = (bf16[384,2048]{1,0:T(8,128)(2,1)S(1)}, bf16[384,2048]{1,0:T(8,128)(2,1)S(1)}, u32[]{:S(2)}, u32[]{:S(2)}) collective-permute-start(bf16[384,2048]{1,0:T(8,128)(2,1)S(1)} %copy-done.6), channel_id=1, source_target_pairs={{0,1},{1,0},{2,3},{3,2},{4,5},{5,4},{6,7},{7,6},{8,9},{9,8},{10,11... | collective-permute-start | bytes 4718600 | tf_op jit(solution)/shard_map/ppermute | solution.py:76
  48.4 3.1 %collective-permute-start.6 = (bf16[4,32,2560]{2,1,0:T(8,128)(2,1)}, bf16[4,32,2560]{2,1,0:T(8,128)(2,1)S(1)}, u32[]{:S(2)}, u32[]{:S(2)}) collective-permute-start(bf16[4,32,2560]{2,1,0:T(8,128)(2,1)} %shard_map.101.refs_0_), channel_id=1, source_target_pairs={{0,6},{1,3},{2,0},{3,5},{4,2},{5,7},{6,4},{7,1},{8,14},{9,11},{10,... | collective-permute-start | bytes 1966088 | tf_op jit(solution)/shard_map/ppermute | solution.py:67
  59.9 4.4 %collective-permute-done.6.refs_3_ = bf16[4,32,2560]{2,1,0:T(8,128)(2,1)S(1)} collective-permute-done((bf16[4,32,2560]{2,1,0:T(8,128)(2,1)}, bf16[4,32,2560]{2,1,0:T(8,128)(2,1)S(1)}, u32[]{:S(2)}, u32[]{:S(2)}) %collective-permute-start.6) | collective-permute-done | bytes 655392 | tf_op jit(solution)/shard_map/ppermute | solution.py:67
  68.4 3.4 %collective-permute-start.7 = (bf16[4,4,32,1024]{3,2,1,0:T(8,128)(2,1)}, bf16[4,4,32,1024]{3,2,1,0:T(8,128)(2,1)S(1)}, u32[]{:S(2)}, u32[]{:S(2)}) collective-permute-start(bf16[4,4,32,1024]{3,2,1,0:T(8,128)(2,1)} %shard_map.102.refs_0_.refs_3_), channel_id=1, source_target_pairs={{0,8},{1,25},{2,10},{3,27},{4,12},{5,29},{6,14},{7,31},{8,16},{9,1... | collective-permute-start | bytes 3145736 | tf_op jit(solution)/shard_map/ppermute | solution.py:67
  71.8 14.5 %collective-permute-done.25.refs_1_.refs_12_ = bf16[4,4,32,1024]{3,2,1,0:T(8,128)(2,1)S(1)} collective-permute-done((bf16[4,4,32,1024]{3,2,1,0:T(8,128)(2,1)}, bf16[4,4,32,1024]{3,2,1,0:T(8,128)(2,1)S(1)}, u32[]{:S(2)}, u32[]{:S(2)}) %collective-permute-start.25) | collective-permute-done | bytes 1048608 | tf_op jit(solution)/shard_map/ppermute | solution.py:67
  94.3 7.8 %collective-permute-done.26.refs_2_.refs_13_ = bf16[4,4,32,1024]{3,2,1,0:T(8,128)(2,1)S(1)} collective-permute-done((bf16[4,4,32,1024]{3,2,1,0:T(8,128)(2,1)S(1)}, bf16[4,4,32,1024]{3,2,1,0:T(8,128)(2,1)S(1)}, u32[]{:S(2)}, u32[]{:S(2)}) %collective-permute-start.26) | collective-permute-done | bytes 1048608 | tf_op jit(solution)/shard_map/ppermute | solution.py:67
  102.1 3.6 %shard_map.109.refs_2_ = bf16[768,256]{1,0:T(8,128)(2,1)S(1)} custom-call(bf16[384,2048]{1,0:T(8,128)(2,1)S(1)} %copy-done.6, bf16[384,2048]{1,0:T(8,128)(2,1)S(1)} %collective-permute-done.other, f32[3,256]{1,0:T(4,128)S(1)} %get-tuple-element.41.taps, bf16[4,4,32,1024]{3,2,1,0:T(8,128)(2,1)S(1)} %copy-done.4, ...), custom_call_target="tpu_custom_call" | custom-call | flops 2415919104 | bytes 8000000 | tf_op jit(solution)/shard_map/pallas_call | solution.py:202
  105.7 3.6 %collective-permute-done.18.refs_3_.refs_10_ = bf16[4,4,32,1024]{3,2,1,0:T(8,128)(2,1)S(1)} collective-permute-done((bf16[4,4,32,1024]{3,2,1,0:T(8,128)(2,1)S(1)}, bf16[4,4,32,1024]{3,2,1,0:T(8,128)(2,1)S(1)}, u32[]{:S(2)}, u32[]{:S(2)}) %collective-permute-start.18) | collective-permute-done | bytes 1048608 | tf_op jit(solution)/shard_map/ppermute | solution.py:67
  111.9 3.5 %shard_map.106.refs_1_ = bf16[768,256]{1,0:T(8,128)(2,1)S(1)} custom-call(bf16[384,2048]{1,0:T(8,128)(2,1)S(1)} %copy-done.6, bf16[384,2048]{1,0:T(8,128)(2,1)S(1)} %collective-permute-done.other, f32[3,256]{1,0:T(4,128)S(1)} %get-tuple-element.43.taps, bf16[4,4,32,1024]{3,2,1,0:T(8,128)(2,1)S(1)} %copy-done.5, ...), custom_call_target="tpu_custom_call" | custom-call | flops 2415919104 | bytes 8000000 | tf_op jit(solution)/shard_map/pallas_call | solution.py:202
  115.4 3.6 %shard_map.103.refs_0_ = bf16[768,256]{1,0:T(8,128)(2,1)S(1)} custom-call(bf16[384,2048]{1,0:T(8,128)(2,1)S(1)} %copy-done.6, bf16[384,2048]{1,0:T(8,128)(2,1)S(1)} %collective-permute-done.other, f32[3,256]{1,0:T(4,128)S(1)} %get-tuple-element.42.taps, bf16[4,4,32,1024]{3,2,1,0:T(8,128)(2,1)S(1)} %copy-done.3, ...), custom_call_target="tpu_custom_call" | custom-call | flops 2415919104 | bytes 8000000 | tf_op jit(solution)/shard_map/pallas_call | solution.py:202
  119.0 5.0 %shard_map.110 = (f32[384,2048]{1,0:T(8,128)S(1)}, bf16[384,2048]{1,0:T(8,128)(2,1)S(1)}) custom-call(bf16[768,256]{1,0:T(8,128)(2,1)S(1)} %shard_map.103.refs_0_, bf16[768,256]{1,0:T(8,128)(2,1)S(1)} %shard_map.106.refs_1_, bf16[768,256]{1,0:T(8,128)(2,1)S(1)} %shard_map.109.refs_2_, bf16[4,4,32,1024]{3,2,1,0:T(8,128)(2,1)S(1)} %copy-done.3, ...), custom_call_target="tpu_custom_call" | custom-call | flops 2415919104 | bytes 9000000 | tf_op jit(solution)/shard_map/pallas_call | solution.py:251
  124.0 3.5 %collective-permute-start.28 = (bf16[384,2048]{1,0:T(8,128)(2,1)S(1)}, bf16[384,2048]{1,0:T(8,128)(2,1)S(1)}, u32[]{:S(2)}, u32[]{:S(2)}) collective-permute-start(bf16[384,2048]{1,0:T(8,128)(2,1)S(1)} %get-tuple-element.27), channel_id=1, source_target_pairs={{0,1},{1,0},{2,3},{3,2},{4,5},{5,4},{6,7},{7,6},{8,9},{9,8},{10,11... | collective-permute-start | bytes 4718600 | tf_op jit(solution)/shard_map/ppermute | solution.py:76
  145.8 9.4 %collective-permute-done.41.refs_5_ = bf16[4,4,32,768]{3,2,1,0:T(8,128)(2,1)S(1)} collective-permute-done((bf16[4,4,32,768]{3,2,1,0:T(8,128)(2,1)}, bf16[4,4,32,768]{3,2,1,0:T(8,128)(2,1)S(1)}, u32[]{:S(2)}, u32[]{:S(2)}) %collective-permute-start.41) | collective-permute-done | bytes 786464 | tf_op jit(solution)/shard_map/ppermute | solution.py:67
  161.9 12.8 %collective-permute-done.44.refs_10_ = bf16[4,4,32,512]{3,2,1,0:T(8,128)(2,1)S(1)} collective-permute-done((bf16[4,4,32,512]{3,2,1,0:T(8,128)(2,1)S(1)}, bf16[4,4,32,512]{3,2,1,0:T(8,128)(2,1)S(1)}, u32[]{:S(2)}, u32[]{:S(2)}) %collective-permute-start.44) | collective-permute-done | bytes 524320 | tf_op jit(solution)/shard_map/ppermute | solution.py:67
  178.8 3.6 %collective-permute-done.38.refs_11_ = bf16[4,4,32,1280]{3,2,1,0:T(8,128)(2,1)S(1)} collective-permute-done((bf16[4,4,32,1280]{3,2,1,0:T(8,128)(2,1)S(1)}, bf16[4,4,32,1280]{3,2,1,0:T(8,128)(2,1)S(1)}, u32[]{:S(2)}, u32[]{:S(2)}) %collective-permute-start.38) | collective-permute-done | bytes 1310752 | tf_op jit(solution)/shard_map/ppermute | solution.py:67
  191.1 11.4 %shard_map.115 = (f32[384,2048]{1,0:T(8,128)S(1)}, f32[384,2048]{1,0:T(8,128)S(1)}) custom-call(bf16[384,2048]{1,0:T(8,128)(2,1)S(1)} %shard_map.111.first_own.skip, bf16[384,2048]{1,0:T(8,128)(2,1)S(1)} %collective-permute-done.29.first_other, bf16[4,4,32,768]{3,2,1,0:T(8,128)(2,1)S(1)} %copy-done.12, ...), custom_call_target="tpu_custom_call" | custom-call | flops 6442450944 | bytes 20000000 | tf_op jit(solution)/shard_map/pallas_call | solution.py:315
  204.2 14.8 %shard_map.116 = (f32[384,2048]{1,0:T(8,128)S(1)}, bf16[384,2048]{1,0:T(8,128)(2,1)S(1)}) custom-call(bf16[384,2048]{1,0:T(8,128)(2,1)S(1)} %shard_map.111.first_own.skip, bf16[384,2048]{1,0:T(8,128)(2,1)S(1)} %collective-permute-done.29.first_other, bf16[4,4,32,768]{3,2,1,0:T(8,128)(2,1)S(1)} %copy-done.10, ...), custom_call_target="tpu_custom_call" | custom-call | flops 6442450944 | bytes 20000000 | tf_op jit(solution)/shard_map/pallas_call | solution.py:315
  219.0 5.9 %collective-permute-start.45 = (bf16[384,2048]{1,0:T(8,128)(2,1)S(1)}, bf16[384,2048]{1,0:T(8,128)(2,1)S(1)}, u32[]{:S(2)}, u32[]{:S(2)}) collective-permute-start(bf16[384,2048]{1,0:T(8,128)(2,1)S(1)} %get-tuple-element.40), channel_id=1, source_target_pairs={{0,1},{1,0},{2,3},{3,2},{4,5},{5,4},{6,7},{7,6},{8,9},{9,8},{10,11... | collective-permute-start | bytes 4718600 | tf_op jit(solution)/shard_map/ppermute | solution.py:76
  (127 shorter events, 90.8 us)
Async XLA Ops:
  13.8 23.1 %collective-permute-start.22 = (bf16[4,32,2304]{2,1,0:T(8,128)(2,1)}, bf16[4,32,2304]{2,1,0:T(8,128)(2,1)S(1)}, u32[]{:S(2)}, u32[]{:S(2)}) collective-permute-start(bf16[4,32,2304]{2,1,0:T(8,128)(2,1)} %shard_map.107.refs_0_), channel_id=1, source_target_pairs={{0,32},{1,97},{2,34},{3,99},{4,36},{5,101},{6,38},{7,103},{8,40},{... | collective-permute-start | bytes 1769480 | tf_op jit(solution)/shard_map/ppermute | solution.py:67
  43.9 43.2 %collective-permute-start = (bf16[384,2048]{1,0:T(8,128)(2,1)S(1)}, bf16[384,2048]{1,0:T(8,128)(2,1)S(1)}, u32[]{:S(2)}, u32[]{:S(2)}) collective-permute-start(bf16[384,2048]{1,0:T(8,128)(2,1)S(1)} %copy-done.6), channel_id=1, source_target_pairs={{0,1},{1,0},{2,3},{3,2},{4,5},{5,4},{6,7},{7,6},{8,9},{9,8},{10,11... | collective-permute-start | bytes 4718600 | tf_op jit(solution)/shard_map/ppermute | solution.py:76
  51.6 15.8 %collective-permute-start.5 = (bf16[4,32,2560]{2,1,0:T(8,128)(2,1)S(1)}, bf16[4,32,2560]{2,1,0:T(8,128)(2,1)S(1)}, u32[]{:S(2)}, u32[]{:S(2)}) collective-permute-start(bf16[4,32,2560]{2,1,0:T(8,128)(2,1)S(1)} %collective-permute-done.4.refs_1_), channel_id=1, source_target_pairs={{0,2},{1,7},{2,4},{3,1},{4,6},{5,3},{6,0},{7,5},{8,10},{9,15},{10,... | collective-permute-start | bytes 1966088 | tf_op jit(solution)/shard_map/ppermute | solution.py:67
  54.0 32.3 %collective-permute-start.25 = (bf16[4,4,32,1024]{3,2,1,0:T(8,128)(2,1)}, bf16[4,4,32,1024]{3,2,1,0:T(8,128)(2,1)S(1)}, u32[]{:S(2)}, u32[]{:S(2)}) collective-permute-start(bf16[4,4,32,1024]{3,2,1,0:T(8,128)(2,1)} %shard_map.108.refs_0_.refs_11_), channel_id=1, source_target_pairs={{0,2},{1,7},{2,4},{3,1},{4,6},{5,3},{6,0},{7,5},{8,10},{9,15},{10,... | collective-permute-start | bytes 3145736 | tf_op jit(solution)/shard_map/ppermute | solution.py:67
  57.2 31.9 %collective-permute-start.16 = (bf16[4,4,32,1024]{3,2,1,0:T(8,128)(2,1)}, bf16[4,4,32,1024]{3,2,1,0:T(8,128)(2,1)S(1)}, u32[]{:S(2)}, u32[]{:S(2)}) collective-permute-start(bf16[4,4,32,1024]{3,2,1,0:T(8,128)(2,1)} %shard_map.105.refs_0_.refs_7_), channel_id=1, source_target_pairs={{0,32},{1,97},{2,34},{3,99},{4,36},{5,101},{6,38},{7,103},{8,40},{... | collective-permute-start | bytes 3145736 | tf_op jit(solution)/shard_map/ppermute | solution.py:67
  64.3 27.1 %collective-permute-start.27 = (bf16[4,4,32,1024]{3,2,1,0:T(8,128)(2,1)S(1)}, bf16[4,4,32,1024]{3,2,1,0:T(8,128)(2,1)S(1)}, u32[]{:S(2)}, u32[]{:S(2)}) collective-permute-start(bf16[4,4,32,1024]{3,2,1,0:T(8,128)(2,1)S(1)} %copy-done.4), channel_id=1, source_target_pairs={{0,6},{1,3},{2,0},{3,5},{4,2},{5,7},{6,4},{7,1},{8,14},{9,11},{10,... | collective-permute-start | bytes 3145736 | tf_op jit(solution)/shard_map/ppermute | solution.py:67
  68.4 22.9 %collective-permute-start.7 = (bf16[4,4,32,1024]{3,2,1,0:T(8,128)(2,1)}, bf16[4,4,32,1024]{3,2,1,0:T(8,128)(2,1)S(1)}, u32[]{:S(2)}, u32[]{:S(2)}) collective-permute-start(bf16[4,4,32,1024]{3,2,1,0:T(8,128)(2,1)} %shard_map.102.refs_0_.refs_3_), channel_id=1, source_target_pairs={{0,8},{1,25},{2,10},{3,27},{4,12},{5,29},{6,14},{7,31},{8,16},{9,1... | collective-permute-start | bytes 3145736 | tf_op jit(solution)/shard_map/ppermute | solution.py:67
  86.3 15.8 %collective-permute-start.26 = (bf16[4,4,32,1024]{3,2,1,0:T(8,128)(2,1)S(1)}, bf16[4,4,32,1024]{3,2,1,0:T(8,128)(2,1)S(1)}, u32[]{:S(2)}, u32[]{:S(2)}) collective-permute-start(bf16[4,4,32,1024]{3,2,1,0:T(8,128)(2,1)S(1)} %collective-permute-done.25.refs_1_.refs_12_), channel_id=1, source_target_pairs={{0,2},{1,7},{2,4},{3,1},{4,6},{5,3},{6,0},{7,5},{8,10},{9,15},{10,... | collective-permute-start | bytes 3145736 | tf_op jit(solution)/shard_map/ppermute | solution.py:67
  87.1 22.2 %collective-permute-start.18 = (bf16[4,4,32,1024]{3,2,1,0:T(8,128)(2,1)S(1)}, bf16[4,4,32,1024]{3,2,1,0:T(8,128)(2,1)S(1)}, u32[]{:S(2)}, u32[]{:S(2)}) collective-permute-start(bf16[4,4,32,1024]{3,2,1,0:T(8,128)(2,1)S(1)} %copy-done.5), channel_id=1, source_target_pairs={{0,96},{1,33},{2,98},{3,35},{4,100},{5,37},{6,102},{7,39},{8,104},... | collective-permute-start | bytes 3145736 | tf_op jit(solution)/shard_map/ppermute | solution.py:67
  89.1 22.8 %collective-permute-start.17 = (bf16[4,4,32,1024]{3,2,1,0:T(8,128)(2,1)S(1)}, bf16[4,4,32,1024]{3,2,1,0:T(8,128)(2,1)S(1)}, u32[]{:S(2)}, u32[]{:S(2)}) collective-permute-start(bf16[4,4,32,1024]{3,2,1,0:T(8,128)(2,1)S(1)} %collective-permute-done.16.refs_1_.refs_8_), channel_id=1, source_target_pairs={{0,32},{1,97},{2,34},{3,99},{4,36},{5,101},{6,38},{7,103},{8,40},{... | collective-permute-start | bytes 3145736 | tf_op jit(solution)/shard_map/ppermute | solution.py:67
  91.3 24.1 %collective-permute-start.9 = (bf16[4,4,32,1024]{3,2,1,0:T(8,128)(2,1)}, bf16[4,4,32,1024]{3,2,1,0:T(8,128)(2,1)S(1)}, u32[]{:S(2)}, u32[]{:S(2)}) collective-permute-start(bf16[4,4,32,1024]{3,2,1,0:T(8,128)(2,1)} %shard_map.102.refs_0_.refs_3_), channel_id=1, source_target_pairs={{0,24},{1,9},{2,26},{3,11},{4,28},{5,13},{6,30},{7,15},{8,0},{9,17... | collective-permute-start | bytes 3145736 | tf_op jit(solution)/shard_map/ppermute | solution.py:67
  91.3 24.1 %collective-permute-start.8 = (bf16[4,4,32,1024]{3,2,1,0:T(8,128)(2,1)S(1)}, bf16[4,4,32,1024]{3,2,1,0:T(8,128)(2,1)S(1)}, u32[]{:S(2)}, u32[]{:S(2)}) collective-permute-start(bf16[4,4,32,1024]{3,2,1,0:T(8,128)(2,1)S(1)} %collective-permute-done.7.refs_1_.refs_4_), channel_id=1, source_target_pairs={{0,8},{1,25},{2,10},{3,27},{4,12},{5,29},{6,14},{7,31},{8,16},{9,1... | collective-permute-start | bytes 3145736 | tf_op jit(solution)/shard_map/ppermute | solution.py:67
  124.0 20.0 %collective-permute-start.28 = (bf16[384,2048]{1,0:T(8,128)(2,1)S(1)}, bf16[384,2048]{1,0:T(8,128)(2,1)S(1)}, u32[]{:S(2)}, u32[]{:S(2)}) collective-permute-start(bf16[384,2048]{1,0:T(8,128)(2,1)S(1)} %get-tuple-element.27), channel_id=1, source_target_pairs={{0,1},{1,0},{2,3},{3,2},{4,5},{5,4},{6,7},{7,6},{8,9},{9,8},{10,11... | collective-permute-start | bytes 4718600 | tf_op jit(solution)/shard_map/ppermute | solution.py:76
  135.6 19.6 %collective-permute-start.41 = (bf16[4,4,32,768]{3,2,1,0:T(8,128)(2,1)}, bf16[4,4,32,768]{3,2,1,0:T(8,128)(2,1)S(1)}, u32[]{:S(2)}, u32[]{:S(2)}) collective-permute-start(bf16[4,4,32,768]{3,2,1,0:T(8,128)(2,1)} %get-tuple-element.35.refs_4_), channel_id=1, source_target_pairs={{0,32},{1,97},{2,34},{3,99},{4,36},{5,101},{6,38},{7,103},{8,40},{... | collective-permute-start | bytes 2359304 | tf_op jit(solution)/shard_map/ppermute | solution.py:67
  135.7 19.5 %collective-permute-start.36 = (bf16[4,4,32,768]{3,2,1,0:T(8,128)(2,1)S(1)}, bf16[4,4,32,768]{3,2,1,0:T(8,128)(2,1)S(1)}, u32[]{:S(2)}, u32[]{:S(2)}) collective-permute-start(bf16[4,4,32,768]{3,2,1,0:T(8,128)(2,1)S(1)} %copy-done.9), channel_id=1, source_target_pairs={{0,2},{1,7},{2,4},{3,1},{4,6},{5,3},{6,0},{7,5},{8,10},{9,15},{10,... | collective-permute-start | bytes 2359304 | tf_op jit(solution)/shard_map/ppermute | solution.py:67
  138.0 19.8 %collective-permute-start.39 = (bf16[4,4,32,768]{3,2,1,0:T(8,128)(2,1)}, bf16[4,4,32,768]{3,2,1,0:T(8,128)(2,1)S(1)}, u32[]{:S(2)}, u32[]{:S(2)}) collective-permute-start(bf16[4,4,32,768]{3,2,1,0:T(8,128)(2,1)} %get-tuple-element.34.refs_0_), channel_id=1, source_target_pairs={{0,8},{1,25},{2,10},{3,27},{4,12},{5,29},{6,14},{7,31},{8,16},{9,1... | collective-permute-start | bytes 2359304 | tf_op jit(solution)/shard_map/ppermute | solution.py:67
  142.0 18.7 %collective-permute-start.30 = (bf16[4,4,32,768]{3,2,1,0:T(8,128)(2,1)}, bf16[4,4,32,768]{3,2,1,0:T(8,128)(2,1)S(1)}, u32[]{:S(2)}, u32[]{:S(2)}) collective-permute-start(bf16[4,4,32,768]{3,2,1,0:T(8,128)(2,1)} %get-tuple-element.28.refs_0_), channel_id=1, source_target_pairs={{0,8},{1,25},{2,10},{3,27},{4,12},{5,29},{6,14},{7,31},{8,16},{9,1... | collective-permute-start | bytes 2359304 | tf_op jit(solution)/shard_map/ppermute | solution.py:67
  144.0 33.2 %collective-permute-start.35 = (bf16[4,4,32,1280]{3,2,1,0:T(8,128)(2,1)S(1)}, bf16[4,4,32,1280]{3,2,1,0:T(8,128)(2,1)S(1)}, u32[]{:S(2)}, u32[]{:S(2)}) collective-permute-start(bf16[4,4,32,1280]{3,2,1,0:T(8,128)(2,1)S(1)} %copy-done.19), channel_id=1, source_target_pairs={{0,96},{1,33},{2,98},{3,35},{4,100},{5,37},{6,102},{7,39},{8,104},... | collective-permute-start | bytes 3932168 | tf_op jit(solution)/shard_map/ppermute | solution.py:67
  155.2 35.9 %collective-permute-start.32 = (bf16[4,4,32,1536]{3,2,1,0:T(8,128)(2,1)S(1)}, bf16[4,4,32,1536]{3,2,1,0:T(8,128)(2,1)S(1)}, u32[]{:S(2)}, u32[]{:S(2)}) collective-permute-start(bf16[4,4,32,1536]{3,2,1,0:T(8,128)(2,1)S(1)} %copy-done.17), channel_id=1, source_target_pairs={{0,24},{1,9},{2,26},{3,11},{4,28},{5,13},{6,30},{7,15},{8,0},{9,17... | collective-permute-start | bytes 4718600 | tf_op jit(solution)/shard_map/ppermute | solution.py:67
  155.2 35.9 %collective-permute-start.29 = (bf16[384,2048]{1,0:T(8,128)(2,1)S(1)}, bf16[384,2048]{1,0:T(8,128)(2,1)S(1)}, u32[]{:S(2)}, u32[]{:S(2)}) collective-permute-start(bf16[384,2048]{1,0:T(8,128)(2,1)S(1)} %shard_map.111.first_own.skip), channel_id=1, source_target_pairs={{0,1},{1,0},{2,3},{3,2},{4,5},{5,4},{6,7},{7,6},{8,9},{9,8},{10,11... | collective-permute-start | bytes 4718600 | tf_op jit(solution)/shard_map/ppermute | solution.py:76
  157.9 24.5 %collective-permute-start.38 = (bf16[4,4,32,1280]{3,2,1,0:T(8,128)(2,1)S(1)}, bf16[4,4,32,1280]{3,2,1,0:T(8,128)(2,1)S(1)}, u32[]{:S(2)}, u32[]{:S(2)}) collective-permute-start(bf16[4,4,32,1280]{3,2,1,0:T(8,128)(2,1)S(1)} %copy-done.18), channel_id=1, source_target_pairs={{0,6},{1,3},{2,0},{3,5},{4,2},{5,7},{6,4},{7,1},{8,14},{9,11},{10,... | collective-permute-start | bytes 3932168 | tf_op jit(solution)/shard_map/ppermute | solution.py:67
  182.4 21.8 %collective-permute-start.37 = (bf16[4,4,32,768]{3,2,1,0:T(8,128)(2,1)S(1)}, bf16[4,4,32,768]{3,2,1,0:T(8,128)(2,1)S(1)}, u32[]{:S(2)}, u32[]{:S(2)}) collective-permute-start(bf16[4,4,32,768]{3,2,1,0:T(8,128)(2,1)S(1)} %collective-permute-done.36.refs_9_), channel_id=1, source_target_pairs={{0,2},{1,7},{2,4},{3,1},{4,6},{5,3},{6,0},{7,5},{8,10},{9,15},{10,... | collective-permute-start | bytes 2359304 | tf_op jit(solution)/shard_map/ppermute | solution.py:67
  186.1 18.1 %collective-permute-start.31 = (bf16[4,4,32,768]{3,2,1,0:T(8,128)(2,1)S(1)}, bf16[4,4,32,768]{3,2,1,0:T(8,128)(2,1)S(1)}, u32[]{:S(2)}, u32[]{:S(2)}) collective-permute-start(bf16[4,4,32,768]{3,2,1,0:T(8,128)(2,1)S(1)} %collective-permute-done.30.refs_1_), channel_id=1, source_target_pairs={{0,8},{1,25},{2,10},{3,27},{4,12},{5,29},{6,14},{7,31},{8,16},{9,1... | collective-permute-start | bytes 2359304 | tf_op jit(solution)/shard_map/ppermute | solution.py:67
  188.3 15.8 %collective-permute-start.34 = (bf16[4,4,32,512]{3,2,1,0:T(8,128)(2,1)S(1)}, bf16[4,4,32,512]{3,2,1,0:T(8,128)(2,1)S(1)}, u32[]{:S(2)}, u32[]{:S(2)}) collective-permute-start(bf16[4,4,32,512]{3,2,1,0:T(8,128)(2,1)S(1)} %collective-permute-done.33.refs_5_), channel_id=1, source_target_pairs={{0,32},{1,97},{2,34},{3,99},{4,36},{5,101},{6,38},{7,103},{8,40},{... | collective-permute-start | bytes 1572872 | tf_op jit(solution)/shard_map/ppermute | solution.py:67
  (42 other events, 728.3 us)

commit v3 on v2

--- a/solution.py
+++ b/solution.py
@@ -16,7 +16,9 @@
 REP_FS_TP = ("rep", "fs_0", "fs_1", "fs_2", "tp")
 ORDERS = ("zxy", "xyz", "yzx")
 CHANNELS = 256
-HIDDEN = ((384, 384, 256), (384, 256, 384))
+HIDDEN = 1024
+UPS = ((384, 384, 256), (384, 384, 256))
+DOWNS = ((256, 384, 384), (384, 256, 384))
 
 
 residual_scale = 2.0**0.25
@@ -35,7 +37,7 @@
 
 
 def stage_widths(part):
-    return [4 * CHANNELS] + [2 * HIDDEN[s][part] for s in range(2)]
+    return [4 * CHANNELS] + [UPS[s][part] + DOWNS[s][part] for s in range(2)]
 
 
 def position(axis):
@@ -99,8 +101,8 @@
             out[:, at : at + CHANNELS] = w[:, part * CHANNELS : (part + 1) * CHANNELS].astype(bf)
             at += CHANNELS
         for s in range(2):
-            start, n = s * sum(HIDDEN[0]) + sum(HIDDEN[s][:part]), HIDDEN[s][part]
-            for w in (up, down):
+            for w, shares in ((up, UPS[s]), (down, DOWNS[s])):
+                start, n = s * HIDDEN + sum(shares[:part]), shares[part]
                 out[:, at : at + n] = w[:, start : start + n].astype(bf)
                 at += n
 
@@ -270,21 +272,24 @@
 
 def feed_kernel(stage, first_own, first_other, *refs):
     blocks, refs = refs[:12], refs[12:]
-    more = None
-    if len(refs) == 9:
-        more, refs = refs[:2], refs[2:]
-    own, other, x, up, down, hidden, sems = refs
+    more, sums = refs[:2], refs[9:]
+    own, other, x, up, down, hidden, sems = refs[2:9] if stage else refs
     tokens = both_tokens(first_own, first_other, x, sems, 0)
     used = 2
-    ends = [sum(HIDDEN[stage][: c + 1]) for c in range(3)]
     ups, downs = [], []
-    for second, whole, sets in ((0, up, ups), (1, down, downs)):
+    for whole, table, sets in ((up, UPS, ups), (down, DOWNS, downs)):
         for c, order in enumerate(ORDERS):
-            n = HIDDEN[stage][c]
+            n = table[stage][c]
             ring = blocks[4 * c : 4 * c + 4]
-            shift = stage * 2 * HIDDEN[0][c]
-            sets.append(fill(order, ring, second * n, n, whole, ends[c] - n, sems, used, shift))
+            start = UPS[stage][c] if sets is downs else 0
+            shift = stage * (UPS[0][c] + DOWNS[0][c])
+            at = sum(table[stage][:c])
+            sets.append(fill(order, ring, start, n, whole, at, sems, used, shift))
             used += len(sets[-1])
+    if stage:
+        for src, dst in zip(more, sums):
+            downs.append([pltpu.make_async_copy(src, dst, sems.at[used])])
+            used += 1
     for copy in sum(ups + downs, tokens):
         copy.start()
     for copy in tokens:
@@ -297,19 +302,20 @@
         return 0
 
     done = 0
-    for copies, end in zip(ups, ends):
+    for c, copies in enumerate(ups):
         for copy in copies:
             copy.wait()
-        lax.fori_loop(done, end // 256, step, 0)
-        done = end // 256
+        ready = sum(UPS[stage][: c + 1]) // 256
+        lax.fori_loop(done, ready, step, 0)
+        done = ready
     for copy in sum(downs, []):
         copy.wait()
-    projected(hidden, down, own, other, more)
+    projected(hidden, down, own, other, sums if stage else None)
 
 
 def feed(stage, own, other, blocks, more=None):
     half = own.shape[0]
-    width = sum(HIDDEN[stage])
+    width = HIDDEN
     extra = [] if more is None else list(more)
     last = jnp.float32 if more is None else bf
     return pl.pallas_call(
@@ -318,7 +324,7 @@
             jax.ShapeDtypeStruct((half, D), jnp.float32),
             jax.ShapeDtypeStruct((half, D), last),
         ],
-        in_specs=[HBM] * (2 + len(blocks)) + [VMEM] * len(extra),
+        in_specs=[HBM] * (2 + len(blocks) + len(extra)),
         out_specs=[VMEM] * 2,
         scratch_shapes=[
             pltpu.VMEM((2 * half, D), bf),
@@ -326,8 +332,9 @@
             whole_scratch(width),
             pltpu.VMEM((2 * half, width), bf),
             pltpu.SemaphoreType.DMA((80,)),
-        ],
-        compiler_params=limit(32),
+        ]
+        + [pltpu.VMEM((half, D), jnp.float32) for _ in extra],
+        compiler_params=limit(21 + 5 * stage),
         cost_estimate=pl.CostEstimate(
             flops=8 * half * D * width, bytes_accessed=20_000_000, transcendentals=0
         ),

time: 231 us -> 221 us (0.957)
  starting transfers between devices: 94 us -> 66.4 us
  waiting for transfers between devices: 76.7 us -> 98.9 us
  Pallas kernels: 57.6 us -> 54.8 us
    ppermute x42, waiting for transfers between devices: 73.7 us -> 95.5 us  [moved(): return lax.ppermute(block, REP_FS_TP, ring_pairs(axis, step))]
    ppermute x4, starting transfers between devices: 16.6 us -> 1.7 us  [swapped(): return lax.ppermute(x, 'tp', [(0, 1), (1, 0)])]
    ppermute x42, starting transfers between devices: 77.4 us -> 64.7 us  [moved(): return lax.ppermute(block, REP_FS_TP, ring_pairs(axis, step))]
    pallas_call x2, Pallas kernels: 26.2 us -> 23.2 us  [feed(): pl.pallas_call(functools.partial(feed_kernel, stage), out_shape=[jax.Shap...]
  transfers between devices with their start and end apart: 46 -> 46, of which waited for: 19 -> 23; matrix products, arithmetic and copies ran while one was open for 0% -> 0% of each run, Pallas kernels for 13% -> 13%
where the time goes in v3:
time: 221 us
  waiting for transfers between devices  98.9 us (45%)
  starting transfers between devices  66.4 us (30%)
  Pallas kernels  54.8 us (25%)
    ppermute x42, waiting for transfers between devices, moved(): return lax.ppermute(block, REP_FS_TP, ring_pairs(axis, step))  95.5 us
    ppermute x42, starting transfers between devices, moved(): return lax.ppermute(block, REP_FS_TP, ring_pairs(axis, step))  64.7 us
    pallas_call x2, Pallas kernels, feed(): pl.pallas_call(functools.partial(feed_kernel, stage), out_shape=[jax.Shap...  23.2 us
    pallas_call x9, Pallas kernels, placed(): pl.pallas_call(functools.partial(place_kernel, axis, columns), out_shape=...  10.8 us
    pallas_call x3, Pallas kernels, mixer(): pl.pallas_call(functools.partial(mixer_kernel, order), out_shape=jax.Shap...  10.6 us
    pallas_call x1, Pallas kernels, mix_out_product(): pl.pallas_call(mix_out_kernel, out_shape=[jax.ShapeDtypeStruct((rows // 2...  5.04 us
  transfers between devices with their start and end apart: 46, of which 23 were waited for; matrix products, arithmetic and copies ran while one was open for 0% of the time, Pallas kernels for 13%

profile of v3, /device:TPU:1, one launch (start us, length us, event | category | flops | bytes accessed | tf_op | source)
XLA Modules:
  0.0 220.7 jit_solution(5115192555165190055)
XLA Ops:
  1.3 3.6 %collective-permute-start.19 = (bf16[32,2304]{1,0:T(8,128)(2,1)S(1)}, bf16[32,2304]{1,0:T(8,128)(2,1)S(1)}, u32[]{:S(2)}, u32[]{:S(2)}) collective-permute-start(bf16[32,2304]{1,0:T(8,128)(2,1)S(1)} %get-tuple-element.25.refs_0_), channel_id=1, source_target_pairs={{0,8},{1,25},{2,10},{3,27},{4,12},{5,29},{6,14},{7,31},{8,16},{9,1... | collective-permute-start | bytes 442376 | tf_op jit(solution)/shard_map/ppermute | solution.py:69
  7.4 3.4 %collective-permute-start.20 = (bf16[32,2304]{1,0:T(8,128)(2,1)S(1)}, bf16[32,2304]{1,0:T(8,128)(2,1)S(1)}, u32[]{:S(2)}, u32[]{:S(2)}) collective-permute-start(bf16[32,2304]{1,0:T(8,128)(2,1)S(1)} %collective-permute-done.19.refs_1_), channel_id=1, source_target_pairs={{0,8},{1,25},{2,10},{3,27},{4,12},{5,29},{6,14},{7,31},{8,16},{9,1... | collective-permute-start | bytes 442376 | tf_op jit(solution)/shard_map/ppermute | solution.py:69
  13.8 3.7 %collective-permute-start.22 = (bf16[4,32,2304]{2,1,0:T(8,128)(2,1)}, bf16[4,32,2304]{2,1,0:T(8,128)(2,1)S(1)}, u32[]{:S(2)}, u32[]{:S(2)}) collective-permute-start(bf16[4,32,2304]{2,1,0:T(8,128)(2,1)} %shard_map.107.refs_0_), channel_id=1, source_target_pairs={{0,32},{1,97},{2,34},{3,99},{4,36},{5,101},{6,38},{7,103},{8,40},{... | collective-permute-start | bytes 1769480 | tf_op jit(solution)/shard_map/ppermute | solution.py:69
  22.2 3.4 %collective-permute-start.11 = (bf16[32,2432]{1,0:T(8,128)(2,1)S(1)}, bf16[32,2432]{1,0:T(8,128)(2,1)S(1)}, u32[]{:S(2)}, u32[]{:S(2)}) collective-permute-start(bf16[32,2432]{1,0:T(8,128)(2,1)S(1)} %collective-permute-done.10.refs_1_), channel_id=1, source_target_pairs={{0,2},{1,7},{2,4},{3,1},{4,6},{5,3},{6,0},{7,5},{8,10},{9,15},{10,... | collective-permute-start | bytes 466952 | tf_op jit(solution)/shard_map/ppermute | solution.py:69
  28.6 4.8 %collective-permute-start.13 = (bf16[4,32,2432]{2,1,0:T(8,128)(2,1)}, bf16[4,32,2432]{2,1,0:T(8,128)(2,1)S(1)}, u32[]{:S(2)}, u32[]{:S(2)}) collective-permute-start(bf16[4,32,2432]{2,1,0:T(8,128)(2,1)} %shard_map.104.refs_0_), channel_id=1, source_target_pairs={{0,8},{1,25},{2,10},{3,27},{4,12},{5,29},{6,14},{7,31},{8,16},{9,1... | collective-permute-start | bytes 1867784 | tf_op jit(solution)/shard_map/ppermute | solution.py:69
  40.4 3.6 %collective-permute-start.4 = (bf16[4,32,2432]{2,1,0:T(8,128)(2,1)}, bf16[4,32,2432]{2,1,0:T(8,128)(2,1)S(1)}, u32[]{:S(2)}, u32[]{:S(2)}) collective-permute-start(bf16[4,32,2432]{2,1,0:T(8,128)(2,1)} %shard_map.101.refs_0_), channel_id=1, source_target_pairs={{0,2},{1,7},{2,4},{3,1},{4,6},{5,3},{6,0},{7,5},{8,10},{9,15},{10,... | collective-permute-start | bytes 1867784 | tf_op jit(solution)/shard_map/ppermute | solution.py:69
  44.0 3.4 %collective-permute-start.23 = (bf16[4,32,2304]{2,1,0:T(8,128)(2,1)S(1)}, bf16[4,32,2304]{2,1,0:T(8,128)(2,1)S(1)}, u32[]{:S(2)}, u32[]{:S(2)}) collective-permute-start(bf16[4,32,2304]{2,1,0:T(8,128)(2,1)S(1)} %collective-permute-done.22.refs_1_), channel_id=1, source_target_pairs={{0,32},{1,97},{2,34},{3,99},{4,36},{5,101},{6,38},{7,103},{8,40},{... | collective-permute-start | bytes 1769480 | tf_op jit(solution)/shard_map/ppermute | solution.py:69
  55.9 8.2 %collective-permute-done.15.refs_3_ = bf16[4,32,2432]{2,1,0:T(8,128)(2,1)S(1)} collective-permute-done((bf16[4,32,2432]{2,1,0:T(8,128)(2,1)}, bf16[4,32,2432]{2,1,0:T(8,128)(2,1)S(1)}, u32[]{:S(2)}, u32[]{:S(2)}) %collective-permute-start.15) | collective-permute-done | bytes 622624 | tf_op jit(solution)/shard_map/ppermute | solution.py:69
  69.0 17.8 %collective-permute-done.25.refs_1_.refs_12_ = bf16[4,4,32,1024]{3,2,1,0:T(8,128)(2,1)S(1)} collective-permute-done((bf16[4,4,32,1024]{3,2,1,0:T(8,128)(2,1)}, bf16[4,4,32,1024]{3,2,1,0:T(8,128)(2,1)S(1)}, u32[]{:S(2)}, u32[]{:S(2)}) %collective-permute-start.25) | collective-permute-done | bytes 1048608 | tf_op jit(solution)/shard_map/ppermute | solution.py:69
  88.3 5.0 %collective-permute-start.17 = (bf16[4,4,32,1024]{3,2,1,0:T(8,128)(2,1)S(1)}, bf16[4,4,32,1024]{3,2,1,0:T(8,128)(2,1)S(1)}, u32[]{:S(2)}, u32[]{:S(2)}) collective-permute-start(bf16[4,4,32,1024]{3,2,1,0:T(8,128)(2,1)S(1)} %collective-permute-done.16.refs_1_.refs_8_), channel_id=1, source_target_pairs={{0,32},{1,97},{2,34},{3,99},{4,36},{5,101},{6,38},{7,103},{8,40},{... | collective-permute-start | bytes 3145736 | tf_op jit(solution)/shard_map/ppermute | solution.py:69
  96.0 8.0 %collective-permute-done.26.refs_2_.refs_13_ = bf16[4,4,32,1024]{3,2,1,0:T(8,128)(2,1)S(1)} collective-permute-done((bf16[4,4,32,1024]{3,2,1,0:T(8,128)(2,1)S(1)}, bf16[4,4,32,1024]{3,2,1,0:T(8,128)(2,1)S(1)}, u32[]{:S(2)}, u32[]{:S(2)}) %collective-permute-start.26) | collective-permute-done | bytes 1048608 | tf_op jit(solution)/shard_map/ppermute | solution.py:69
  104.0 3.5 %shard_map.109.refs_2_ = bf16[768,256]{1,0:T(8,128)(2,1)S(1)} custom-call(bf16[384,2048]{1,0:T(8,128)(2,1)S(1)} %copy-done.6, bf16[384,2048]{1,0:T(8,128)(2,1)S(1)} %collective-permute-done.other, f32[3,256]{1,0:T(4,128)S(1)} %get-tuple-element.41.taps, bf16[4,4,32,1024]{3,2,1,0:T(8,128)(2,1)S(1)} %copy-done.5, ...), custom_call_target="tpu_custom_call" | custom-call | flops 2415919104 | bytes 8000000 | tf_op jit(solution)/shard_map/pallas_call | solution.py:204
  107.5 6.3 %collective-permute-done.18.refs_3_.refs_10_ = bf16[4,4,32,1024]{3,2,1,0:T(8,128)(2,1)S(1)} collective-permute-done((bf16[4,4,32,1024]{3,2,1,0:T(8,128)(2,1)S(1)}, bf16[4,4,32,1024]{3,2,1,0:T(8,128)(2,1)S(1)}, u32[]{:S(2)}, u32[]{:S(2)}) %collective-permute-start.18) | collective-permute-done | bytes 1048608 | tf_op jit(solution)/shard_map/ppermute | solution.py:69
  116.2 3.5 %shard_map.106.refs_1_ = bf16[768,256]{1,0:T(8,128)(2,1)S(1)} custom-call(bf16[384,2048]{1,0:T(8,128)(2,1)S(1)} %copy-done.6, bf16[384,2048]{1,0:T(8,128)(2,1)S(1)} %collective-permute-done.other, f32[3,256]{1,0:T(4,128)S(1)} %get-tuple-element.43.taps, bf16[4,4,32,1024]{3,2,1,0:T(8,128)(2,1)S(1)} %copy-done.3, ...), custom_call_target="tpu_custom_call" | custom-call | flops 2415919104 | bytes 8000000 | tf_op jit(solution)/shard_map/pallas_call | solution.py:204
  119.7 3.6 %shard_map.103.refs_0_ = bf16[768,256]{1,0:T(8,128)(2,1)S(1)} custom-call(bf16[384,2048]{1,0:T(8,128)(2,1)S(1)} %copy-done.6, bf16[384,2048]{1,0:T(8,128)(2,1)S(1)} %collective-permute-done.other, f32[3,256]{1,0:T(4,128)S(1)} %get-tuple-element.42.taps, bf16[4,4,32,1024]{3,2,1,0:T(8,128)(2,1)S(1)} %copy-done.4, ...), custom_call_target="tpu_custom_call" | custom-call | flops 2415919104 | bytes 8000000 | tf_op jit(solution)/shard_map/pallas_call | solution.py:204
  123.3 5.0 %shard_map.110 = (f32[384,2048]{1,0:T(8,128)S(1)}, bf16[384,2048]{1,0:T(8,128)(2,1)S(1)}) custom-call(bf16[768,256]{1,0:T(8,128)(2,1)S(1)} %shard_map.103.refs_0_, bf16[768,256]{1,0:T(8,128)(2,1)S(1)} %shard_map.106.refs_1_, bf16[768,256]{1,0:T(8,128)(2,1)S(1)} %shard_map.109.refs_2_, bf16[4,4,32,1024]{3,2,1,0:T(8,128)(2,1)S(1)} %copy-done.4, ...), custom_call_target="tpu_custom_call" | custom-call | flops 2415919104 | bytes 9000000 | tf_op jit(solution)/shard_map/pallas_call | solution.py:253
  143.1 5.1 %collective-permute-done.36.refs_9_ = bf16[4,4,32,640]{3,2,1,0:T(8,128)(2,1)S(1)} collective-permute-done((bf16[4,4,32,640]{3,2,1,0:T(8,128)(2,1)}, bf16[4,4,32,640]{3,2,1,0:T(8,128)(2,1)S(1)}, u32[]{:S(2)}, u32[]{:S(2)}) %collective-permute-start.36) | collective-permute-done | bytes 655392 | tf_op jit(solution)/shard_map/ppermute | solution.py:69
  152.5 4.4 %collective-permute-done.39.refs_1_ = bf16[4,4,32,640]{3,2,1,0:T(8,128)(2,1)S(1)} collective-permute-done((bf16[4,4,32,640]{3,2,1,0:T(8,128)(2,1)}, bf16[4,4,32,640]{3,2,1,0:T(8,128)(2,1)S(1)}, u32[]{:S(2)}, u32[]{:S(2)}) %collective-permute-start.39) | collective-permute-done | bytes 655392 | tf_op jit(solution)/shard_map/ppermute | solution.py:69
  160.3 14.3 %collective-permute-done.44.refs_10_ = bf16[4,4,32,640]{3,2,1,0:T(8,128)(2,1)S(1)} collective-permute-done((bf16[4,4,32,640]{3,2,1,0:T(8,128)(2,1)S(1)}, bf16[4,4,32,640]{3,2,1,0:T(8,128)(2,1)S(1)}, u32[]{:S(2)}, u32[]{:S(2)}) %collective-permute-start.44) | collective-permute-done | bytes 655392 | tf_op jit(solution)/shard_map/ppermute | solution.py:69
  179.4 8.3 %collective-permute-done.40.refs_2_ = bf16[4,4,32,640]{3,2,1,0:T(8,128)(2,1)S(1)} collective-permute-done((bf16[4,4,32,640]{3,2,1,0:T(8,128)(2,1)S(1)}, bf16[4,4,32,640]{3,2,1,0:T(8,128)(2,1)S(1)}, u32[]{:S(2)}, u32[]{:S(2)}) %collective-permute-start.40) | collective-permute-done | bytes 655392 | tf_op jit(solution)/shard_map/ppermute | solution.py:69
  187.8 3.1 %collective-permute-start.31 = (bf16[4,4,32,768]{3,2,1,0:T(8,128)(2,1)S(1)}, bf16[4,4,32,768]{3,2,1,0:T(8,128)(2,1)S(1)}, u32[]{:S(2)}, u32[]{:S(2)}) collective-permute-start(bf16[4,4,32,768]{3,2,1,0:T(8,128)(2,1)S(1)} %collective-permute-done.30.refs_1_), channel_id=1, source_target_pairs={{0,8},{1,25},{2,10},{3,27},{4,12},{5,29},{6,14},{7,31},{8,16},{9,1... | collective-permute-start | bytes 2359304 | tf_op jit(solution)/shard_map/ppermute | solution.py:69
  191.4 11.4 %shard_map.115 = (f32[384,2048]{1,0:T(8,128)S(1)}, f32[384,2048]{1,0:T(8,128)S(1)}) custom-call(bf16[384,2048]{1,0:T(8,128)(2,1)S(1)} %shard_map.111.first_own.skip, bf16[384,2048]{1,0:T(8,128)(2,1)S(1)} %collective-permute-done.29.first_other, bf16[4,4,32,640]{3,2,1,0:T(8,128)(2,1)S(1)} %copy-done.14, ...), custom_call_target="tpu_custom_call" | custom-call | flops 6442450944 | bytes 20000000 | tf_op jit(solution)/shard_map/pallas_call | solution.py:321
  202.9 11.8 %shard_map.116 = (f32[384,2048]{1,0:T(8,128)S(1)}, bf16[384,2048]{1,0:T(8,128)(2,1)S(1)}) custom-call(bf16[384,2048]{1,0:T(8,128)(2,1)S(1)} %shard_map.111.first_own.skip, bf16[384,2048]{1,0:T(8,128)(2,1)S(1)} %collective-permute-done.29.first_other, bf16[4,4,32,768]{3,2,1,0:T(8,128)(2,1)S(1)} %copy-done.9, ...), custom_call_target="tpu_custom_call" | custom-call | flops 6442450944 | bytes 20000000 | tf_op jit(solution)/shard_map/pallas_call | solution.py:321
  214.8 3.4 %collective-permute-done.45.other = bf16[384,2048]{1,0:T(8,128)(2,1)S(1)} collective-permute-done((bf16[384,2048]{1,0:T(8,128)(2,1)S(1)}, bf16[384,2048]{1,0:T(8,128)(2,1)S(1)}, u32[]{:S(2)}, u32[]{:S(2)}) %collective-permute-start.45) | collective-permute-done | bytes 1572896 | tf_op jit(solution)/shard_map/ppermute | solution.py:78
  (125 shorter events, 71.3 us)
Async XLA Ops:
  13.8 30.2 %collective-permute-start.22 = (bf16[4,32,2304]{2,1,0:T(8,128)(2,1)}, bf16[4,32,2304]{2,1,0:T(8,128)(2,1)S(1)}, u32[]{:S(2)}, u32[]{:S(2)}) collective-permute-start(bf16[4,32,2304]{2,1,0:T(8,128)(2,1)} %shard_map.107.refs_0_), channel_id=1, source_target_pairs={{0,32},{1,97},{2,34},{3,99},{4,36},{5,101},{6,38},{7,103},{8,40},{... | collective-permute-start | bytes 1769480 | tf_op jit(solution)/shard_map/ppermute | solution.py:69
  28.6 18.8 %collective-permute-start.13 = (bf16[4,32,2432]{2,1,0:T(8,128)(2,1)}, bf16[4,32,2432]{2,1,0:T(8,128)(2,1)S(1)}, u32[]{:S(2)}, u32[]{:S(2)}) collective-permute-start(bf16[4,32,2432]{2,1,0:T(8,128)(2,1)} %shard_map.104.refs_0_), channel_id=1, source_target_pairs={{0,8},{1,25},{2,10},{3,27},{4,12},{5,29},{6,14},{7,31},{8,16},{9,1... | collective-permute-start | bytes 1867784 | tf_op jit(solution)/shard_map/ppermute | solution.py:69
  47.4 16.7 %collective-permute-start.15 = (bf16[4,32,2432]{2,1,0:T(8,128)(2,1)}, bf16[4,32,2432]{2,1,0:T(8,128)(2,1)S(1)}, u32[]{:S(2)}, u32[]{:S(2)}) collective-permute-start(bf16[4,32,2432]{2,1,0:T(8,128)(2,1)} %shard_map.104.refs_0_), channel_id=1, source_target_pairs={{0,24},{1,9},{2,26},{3,11},{4,28},{5,13},{6,30},{7,15},{8,0},{9,17... | collective-permute-start | bytes 1867784 | tf_op jit(solution)/shard_map/ppermute | solution.py:69
  47.4 16.7 %collective-permute-start.14 = (bf16[4,32,2432]{2,1,0:T(8,128)(2,1)S(1)}, bf16[4,32,2432]{2,1,0:T(8,128)(2,1)S(1)}, u32[]{:S(2)}, u32[]{:S(2)}) collective-permute-start(bf16[4,32,2432]{2,1,0:T(8,128)(2,1)S(1)} %collective-permute-done.13.refs_1_), channel_id=1, source_target_pairs={{0,8},{1,25},{2,10},{3,27},{4,12},{5,29},{6,14},{7,31},{8,16},{9,1... | collective-permute-start | bytes 1867784 | tf_op jit(solution)/shard_map/ppermute | solution.py:69
  50.1 38.2 %collective-permute-start = (bf16[384,2048]{1,0:T(8,128)(2,1)S(1)}, bf16[384,2048]{1,0:T(8,128)(2,1)S(1)}, u32[]{:S(2)}, u32[]{:S(2)}) collective-permute-start(bf16[384,2048]{1,0:T(8,128)(2,1)S(1)} %copy-done.6), channel_id=1, source_target_pairs={{0,1},{1,0},{2,3},{3,2},{4,5},{5,4},{6,7},{7,6},{8,9},{9,8},{10,11... | collective-permute-start | bytes 4718600 | tf_op jit(solution)/shard_map/ppermute | solution.py:78
  64.1 22.7 %collective-permute-start.25 = (bf16[4,4,32,1024]{3,2,1,0:T(8,128)(2,1)}, bf16[4,4,32,1024]{3,2,1,0:T(8,128)(2,1)S(1)}, u32[]{:S(2)}, u32[]{:S(2)}) collective-permute-start(bf16[4,4,32,1024]{3,2,1,0:T(8,128)(2,1)} %shard_map.108.refs_0_.refs_11_), channel_id=1, source_target_pairs={{0,2},{1,7},{2,4},{3,1},{4,6},{5,3},{6,0},{7,5},{8,10},{9,15},{10,... | collective-permute-start | bytes 3145736 | tf_op jit(solution)/shard_map/ppermute | solution.py:69
  65.2 23.1 %collective-permute-start.16 = (bf16[4,4,32,1024]{3,2,1,0:T(8,128)(2,1)}, bf16[4,4,32,1024]{3,2,1,0:T(8,128)(2,1)S(1)}, u32[]{:S(2)}, u32[]{:S(2)}) collective-permute-start(bf16[4,4,32,1024]{3,2,1,0:T(8,128)(2,1)} %shard_map.105.refs_0_.refs_7_), channel_id=1, source_target_pairs={{0,32},{1,97},{2,34},{3,99},{4,36},{5,101},{6,38},{7,103},{8,40},{... | collective-permute-start | bytes 3145736 | tf_op jit(solution)/shard_map/ppermute | solution.py:69
  65.6 27.7 %collective-permute-start.27 = (bf16[4,4,32,1024]{3,2,1,0:T(8,128)(2,1)S(1)}, bf16[4,4,32,1024]{3,2,1,0:T(8,128)(2,1)S(1)}, u32[]{:S(2)}, u32[]{:S(2)}) collective-permute-start(bf16[4,4,32,1024]{3,2,1,0:T(8,128)(2,1)S(1)} %copy-done.5), channel_id=1, source_target_pairs={{0,6},{1,3},{2,0},{3,5},{4,2},{5,7},{6,4},{7,1},{8,14},{9,11},{10,... | collective-permute-start | bytes 3145736 | tf_op jit(solution)/shard_map/ppermute | solution.py:69
  69.0 24.3 %collective-permute-start.7 = (bf16[4,4,32,1024]{3,2,1,0:T(8,128)(2,1)}, bf16[4,4,32,1024]{3,2,1,0:T(8,128)(2,1)S(1)}, u32[]{:S(2)}, u32[]{:S(2)}) collective-permute-start(bf16[4,4,32,1024]{3,2,1,0:T(8,128)(2,1)} %shard_map.102.refs_0_.refs_3_), channel_id=1, source_target_pairs={{0,8},{1,25},{2,10},{3,27},{4,12},{5,29},{6,14},{7,31},{8,16},{9,1... | collective-permute-start | bytes 3145736 | tf_op jit(solution)/shard_map/ppermute | solution.py:69
  86.9 17.1 %collective-permute-start.26 = (bf16[4,4,32,1024]{3,2,1,0:T(8,128)(2,1)S(1)}, bf16[4,4,32,1024]{3,2,1,0:T(8,128)(2,1)S(1)}, u32[]{:S(2)}, u32[]{:S(2)}) collective-permute-start(bf16[4,4,32,1024]{3,2,1,0:T(8,128)(2,1)S(1)} %collective-permute-done.25.refs_1_.refs_12_), channel_id=1, source_target_pairs={{0,2},{1,7},{2,4},{3,1},{4,6},{5,3},{6,0},{7,5},{8,10},{9,15},{10,... | collective-permute-start | bytes 3145736 | tf_op jit(solution)/shard_map/ppermute | solution.py:69
  88.3 25.5 %collective-permute-start.18 = (bf16[4,4,32,1024]{3,2,1,0:T(8,128)(2,1)S(1)}, bf16[4,4,32,1024]{3,2,1,0:T(8,128)(2,1)S(1)}, u32[]{:S(2)}, u32[]{:S(2)}) collective-permute-start(bf16[4,4,32,1024]{3,2,1,0:T(8,128)(2,1)S(1)} %copy-done.3), channel_id=1, source_target_pairs={{0,96},{1,33},{2,98},{3,35},{4,100},{5,37},{6,102},{7,39},{8,104},... | collective-permute-start | bytes 3145736 | tf_op jit(solution)/shard_map/ppermute | solution.py:69
  88.3 27.9 %collective-permute-start.17 = (bf16[4,4,32,1024]{3,2,1,0:T(8,128)(2,1)S(1)}, bf16[4,4,32,1024]{3,2,1,0:T(8,128)(2,1)S(1)}, u32[]{:S(2)}, u32[]{:S(2)}) collective-permute-start(bf16[4,4,32,1024]{3,2,1,0:T(8,128)(2,1)S(1)} %collective-permute-done.16.refs_1_.refs_8_), channel_id=1, source_target_pairs={{0,32},{1,97},{2,34},{3,99},{4,36},{5,101},{6,38},{7,103},{8,40},{... | collective-permute-start | bytes 3145736 | tf_op jit(solution)/shard_map/ppermute | solution.py:69
  93.3 26.5 %collective-permute-start.9 = (bf16[4,4,32,1024]{3,2,1,0:T(8,128)(2,1)}, bf16[4,4,32,1024]{3,2,1,0:T(8,128)(2,1)S(1)}, u32[]{:S(2)}, u32[]{:S(2)}) collective-permute-start(bf16[4,4,32,1024]{3,2,1,0:T(8,128)(2,1)} %shard_map.102.refs_0_.refs_3_), channel_id=1, source_target_pairs={{0,24},{1,9},{2,26},{3,11},{4,28},{5,13},{6,30},{7,15},{8,0},{9,17... | collective-permute-start | bytes 3145736 | tf_op jit(solution)/shard_map/ppermute | solution.py:69
  93.3 26.5 %collective-permute-start.8 = (bf16[4,4,32,1024]{3,2,1,0:T(8,128)(2,1)S(1)}, bf16[4,4,32,1024]{3,2,1,0:T(8,128)(2,1)S(1)}, u32[]{:S(2)}, u32[]{:S(2)}) collective-permute-start(bf16[4,4,32,1024]{3,2,1,0:T(8,128)(2,1)S(1)} %collective-permute-done.7.refs_1_.refs_4_), channel_id=1, source_target_pairs={{0,8},{1,25},{2,10},{3,27},{4,12},{5,29},{6,14},{7,31},{8,16},{9,1... | collective-permute-start | bytes 3145736 | tf_op jit(solution)/shard_map/ppermute | solution.py:69
  128.4 22.7 %collective-permute-start.28 = (bf16[384,2048]{1,0:T(8,128)(2,1)S(1)}, bf16[384,2048]{1,0:T(8,128)(2,1)S(1)}, u32[]{:S(2)}, u32[]{:S(2)}) collective-permute-start(bf16[384,2048]{1,0:T(8,128)(2,1)S(1)} %get-tuple-element.27), channel_id=1, source_target_pairs={{0,1},{1,0},{2,3},{3,2},{4,5},{5,4},{6,7},{7,6},{8,9},{9,8},{10,11... | collective-permute-start | bytes 4718600 | tf_op jit(solution)/shard_map/ppermute | solution.py:78
  131.4 16.9 %collective-permute-start.36 = (bf16[4,4,32,640]{3,2,1,0:T(8,128)(2,1)}, bf16[4,4,32,640]{3,2,1,0:T(8,128)(2,1)S(1)}, u32[]{:S(2)}, u32[]{:S(2)}) collective-permute-start(bf16[4,4,32,640]{3,2,1,0:T(8,128)(2,1)} %get-tuple-element.32.refs_8_), channel_id=1, source_target_pairs={{0,2},{1,7},{2,4},{3,1},{4,6},{5,3},{6,0},{7,5},{8,10},{9,15},{10,... | collective-permute-start | bytes 1966088 | tf_op jit(solution)/shard_map/ppermute | solution.py:69
  134.0 24.6 %collective-permute-start.41 = (bf16[4,4,32,768]{3,2,1,0:T(8,128)(2,1)}, bf16[4,4,32,768]{3,2,1,0:T(8,128)(2,1)S(1)}, u32[]{:S(2)}, u32[]{:S(2)}) collective-permute-start(bf16[4,4,32,768]{3,2,1,0:T(8,128)(2,1)} %get-tuple-element.35.refs_4_), channel_id=1, source_target_pairs={{0,32},{1,97},{2,34},{3,99},{4,36},{5,101},{6,38},{7,103},{8,40},{... | collective-permute-start | bytes 2359304 | tf_op jit(solution)/shard_map/ppermute | solution.py:69
  138.5 20.5 %collective-permute-start.30 = (bf16[4,4,32,768]{3,2,1,0:T(8,128)(2,1)}, bf16[4,4,32,768]{3,2,1,0:T(8,128)(2,1)S(1)}, u32[]{:S(2)}, u32[]{:S(2)}) collective-permute-start(bf16[4,4,32,768]{3,2,1,0:T(8,128)(2,1)} %get-tuple-element.28.refs_0_), channel_id=1, source_target_pairs={{0,8},{1,25},{2,10},{3,27},{4,12},{5,29},{6,14},{7,31},{8,16},{9,1... | collective-permute-start | bytes 2359304 | tf_op jit(solution)/shard_map/ppermute | solution.py:69
  141.2 15.7 %collective-permute-start.39 = (bf16[4,4,32,640]{3,2,1,0:T(8,128)(2,1)}, bf16[4,4,32,640]{3,2,1,0:T(8,128)(2,1)S(1)}, u32[]{:S(2)}, u32[]{:S(2)}) collective-permute-start(bf16[4,4,32,640]{3,2,1,0:T(8,128)(2,1)} %get-tuple-element.34.refs_0_), channel_id=1, source_target_pairs={{0,8},{1,25},{2,10},{3,27},{4,12},{5,29},{6,14},{7,31},{8,16},{9,1... | collective-permute-start | bytes 1966088 | tf_op jit(solution)/shard_map/ppermute | solution.py:69
  151.0 25.5 %collective-permute-start.38 = (bf16[4,4,32,1280]{3,2,1,0:T(8,128)(2,1)S(1)}, bf16[4,4,32,1280]{3,2,1,0:T(8,128)(2,1)S(1)}, u32[]{:S(2)}, u32[]{:S(2)}) collective-permute-start(bf16[4,4,32,1280]{3,2,1,0:T(8,128)(2,1)S(1)} %copy-done.18), channel_id=1, source_target_pairs={{0,6},{1,3},{2,0},{3,5},{4,2},{5,7},{6,4},{7,1},{8,14},{9,11},{10,... | collective-permute-start | bytes 3932168 | tf_op jit(solution)/shard_map/ppermute | solution.py:69
  156.9 34.5 %collective-permute-start.29 = (bf16[384,2048]{1,0:T(8,128)(2,1)S(1)}, bf16[384,2048]{1,0:T(8,128)(2,1)S(1)}, u32[]{:S(2)}, u32[]{:S(2)}) collective-permute-start(bf16[384,2048]{1,0:T(8,128)(2,1)S(1)} %shard_map.111.first_own.skip), channel_id=1, source_target_pairs={{0,1},{1,0},{2,3},{3,2},{4,5},{5,4},{6,7},{7,6},{8,9},{9,8},{10,11... | collective-permute-start | bytes 4718600 | tf_op jit(solution)/shard_map/ppermute | solution.py:78
  158.6 32.3 %collective-permute-start.32 = (bf16[4,4,32,1408]{3,2,1,0:T(8,128)(2,1)S(1)}, bf16[4,4,32,1408]{3,2,1,0:T(8,128)(2,1)S(1)}, u32[]{:S(2)}, u32[]{:S(2)}) collective-permute-start(bf16[4,4,32,1408]{3,2,1,0:T(8,128)(2,1)S(1)} %copy-done.17), channel_id=1, source_target_pairs={{0,24},{1,9},{2,26},{3,11},{4,28},{5,13},{6,30},{7,15},{8,0},{9,17... | collective-permute-start | bytes 4325384 | tf_op jit(solution)/shard_map/ppermute | solution.py:69
  158.6 32.3 %collective-permute-start.35 = (bf16[4,4,32,1408]{3,2,1,0:T(8,128)(2,1)S(1)}, bf16[4,4,32,1408]{3,2,1,0:T(8,128)(2,1)S(1)}, u32[]{:S(2)}, u32[]{:S(2)}) collective-permute-start(bf16[4,4,32,1408]{3,2,1,0:T(8,128)(2,1)S(1)} %copy-done.16), channel_id=1, source_target_pairs={{0,96},{1,33},{2,98},{3,35},{4,100},{5,37},{6,102},{7,39},{8,104},... | collective-permute-start | bytes 4325384 | tf_op jit(solution)/shard_map/ppermute | solution.py:69
  158.9 15.8 %collective-permute-start.44 = (bf16[4,4,32,640]{3,2,1,0:T(8,128)(2,1)S(1)}, bf16[4,4,32,640]{3,2,1,0:T(8,128)(2,1)S(1)}, u32[]{:S(2)}, u32[]{:S(2)}) collective-permute-start(bf16[4,4,32,640]{3,2,1,0:T(8,128)(2,1)S(1)} %collective-permute-done.43.refs_9_), channel_id=1, source_target_pairs={{0,2},{1,7},{2,4},{3,1},{4,6},{5,3},{6,0},{7,5},{8,10},{9,15},{10,... | collective-permute-start | bytes 1966088 | tf_op jit(solution)/shard_map/ppermute | solution.py:69
  (41 other events, 688.2 us)

commit v4 on v3

--- a/solution.py
+++ b/solution.py
@@ -129,13 +129,13 @@
     finish(copies)
 
 
-def placed(parts, axis, columns):
+def placed(parts, axis, columns, space):
     lead = parts[0].shape[:-1]
     return pl.pallas_call(
         functools.partial(place_kernel, axis, columns),
-        out_shape=[pltpu.HBM((4, *lead, width), bf) for _, width in columns],
+        out_shape=[space((4, *lead, width), bf) for _, width in columns],
         in_specs=[HBM] * 4,
-        out_specs=[HBM] * len(columns),
+        out_specs=[pl.BlockSpec(memory_space=space)] * len(columns),
         scratch_shapes=[pltpu.SemaphoreType.DMA((4 * len(columns),))],
         compiler_params=limit(4),
     )(*parts)
@@ -218,18 +218,17 @@
     )(own, other, taps, *blocks)
 
 
-def projected(left, whole, own, other, more=None):
-    half = own.shape[0]
-
+def projected(lefts, whole, outs, more=None):
     def step(j, _):
         rows = whole[j >> 2, j & 3].reshape(256, whole.shape[-1])
         cols = pl.ds(pl.multiple_of(j * 256, 256), 256)
-        sums = dot_t(left[...], rows)
-        ours, theirs = sums[:half], sums[half:]
-        if more is not None:
-            ours, theirs = ours + more[0][:, cols], theirs + more[1][:, cols]
-        own[:, cols] = ours.astype(own.dtype)
-        other[:, cols] = theirs.astype(other.dtype)
+        for left, parts in zip(lefts, outs):
+            sums = dot_t(left[...], rows)
+            if more is not None:
+                sums = sums + more[:, cols]
+            size = sums.shape[0] // len(parts)
+            for i, out in enumerate(parts):
+                out[:, cols] = sums[i * size : (i + 1) * size].astype(out.dtype)
         return 0
 
     lax.fori_loop(0, 8, step, 0)
@@ -245,7 +244,7 @@
         copies += fill(order, part, 3 * CHANNELS, CHANNELS, whole, at, sems, len(copies))
         left[:, at : at + CHANNELS] = mixed[c][...]
     finish(copies)
-    projected(left, whole, own, other)
+    projected([left], whole, [(own, other)])
 
 
 def mix_out_product(mixed, blocks):
@@ -253,8 +252,8 @@
     return pl.pallas_call(
         mix_out_kernel,
         out_shape=[
-            jax.ShapeDtypeStruct((rows // 2, D), jnp.float32),
-            jax.ShapeDtypeStruct((rows // 2, D), bf),
+            pltpu.VMEM((rows // 2, D), jnp.float32),
+            pltpu.VMEM((rows // 2, D), bf),
         ],
         in_specs=[VMEM] * 3 + [HBM] * 12,
         out_specs=[VMEM] * 2,
@@ -272,8 +271,11 @@
 
 def feed_kernel(stage, first_own, first_other, *refs):
     blocks, refs = refs[:12], refs[12:]
-    more, sums = refs[:2], refs[9:]
-    own, other, x, up, down, hidden, sems = refs[2:9] if stage else refs
+    half = first_own.shape[0]
+    if stage:
+        more, other, hidden_own, down, x, up, hidden, sems, sums = refs
+    else:
+        own, other, x, up, down, hidden, sems = refs
     tokens = both_tokens(first_own, first_other, x, sems, 0)
     used = 2
     ups, downs = [], []
@@ -287,9 +289,7 @@
             sets.append(fill(order, ring, start, n, whole, at, sems, used, shift))
             used += len(sets[-1])
     if stage:
-        for src, dst in zip(more, sums):
-            downs.append([pltpu.make_async_copy(src, dst, sems.at[used])])
-            used += 1
+        downs.append([pltpu.make_async_copy(more, sums, sems.at[used])])
     for copy in sum(ups + downs, tokens):
         copy.start()
     for copy in tokens:
@@ -298,7 +298,12 @@
     def step(j, _):
         cols = pl.ds(pl.multiple_of(j * 256, 256), 256)
         raised = jnp.maximum(dot(x[...], up[..., cols].reshape(D, 256)), 0.0)
-        hidden[:, cols] = (raised * raised).astype(bf)
+        squared = (raised * raised).astype(bf)
+        if stage:
+            hidden_own[:, cols] = squared[:half]
+            hidden[:, cols] = squared[half:]
+        else:
+            hidden[:, cols] = squared
         return 0
 
     done = 0
@@ -310,35 +315,59 @@
         done = ready
     for copy in sum(downs, []):
         copy.wait()
-    projected(hidden, down, own, other, sums if stage else None)
+    if stage:
+        projected([hidden], down, [(other,)], sums)
+    else:
+        projected([hidden], down, [(own, other)])
 
 
 def feed(stage, own, other, blocks, more=None):
     half = own.shape[0]
-    width = HIDDEN
-    extra = [] if more is None else list(more)
-    last = jnp.float32 if more is None else bf
-    return pl.pallas_call(
-        functools.partial(feed_kernel, stage),
-        out_shape=[
-            jax.ShapeDtypeStruct((half, D), jnp.float32),
-            jax.ShapeDtypeStruct((half, D), last),
-        ],
-        in_specs=[HBM] * (2 + len(blocks) + len(extra)),
-        out_specs=[VMEM] * 2,
-        scratch_shapes=[
-            pltpu.VMEM((2 * half, D), bf),
-            whole_scratch(width),
-            whole_scratch(width),
-            pltpu.VMEM((2 * half, width), bf),
+    down = (2, 4, 4, 2, ROWS, HIDDEN)
+    sums = pltpu.VMEM((half, D), jnp.float32)
+    if stage:
+        outs = [pltpu.VMEM((half, D), bf), pltpu.VMEM((half, HIDDEN), bf), pltpu.VMEM(down, bf)]
+        scratch = [pltpu.VMEM((half, HIDDEN), bf), pltpu.SemaphoreType.DMA((80,)), sums]
+        inputs = (*blocks, more)
+    else:
+        outs = [sums, sums]
+        scratch = [
+            whole_scratch(HIDDEN),
+            pltpu.VMEM((2 * half, HIDDEN), bf),
             pltpu.SemaphoreType.DMA((80,)),
         ]
-        + [pltpu.VMEM((half, D), jnp.float32) for _ in extra],
-        compiler_params=limit(21 + 5 * stage),
+        inputs = blocks
+    return pl.pallas_call(
+        functools.partial(feed_kernel, stage),
+        out_shape=outs,
+        in_specs=[HBM] * (2 + len(inputs)),
+        out_specs=[VMEM] * len(outs),
+        scratch_shapes=[pltpu.VMEM((2 * half, D), bf), whole_scratch(HIDDEN)] + scratch,
+        compiler_params=limit(21),
         cost_estimate=pl.CostEstimate(
-            flops=8 * half * D * width, bytes_accessed=20_000_000, transcendentals=0
+            flops=(6 if stage else 8) * half * D * HIDDEN,
+            bytes_accessed=20_000_000,
+            transcendentals=0,
         ),
-    )(own, other, *blocks, *extra)
+    )(own, other, *inputs)
+
+
+def finished_kernel(hidden, down, more, own):
+    projected([hidden], down, [(own,)], more)
+
+
+def finished(hidden, down, more):
+    half = hidden.shape[0]
+    return pl.pallas_call(
+        finished_kernel,
+        out_shape=pltpu.VMEM((half, D), jnp.float32),
+        in_specs=[VMEM] * 3,
+        out_specs=VMEM,
+        compiler_params=limit(18),
+        cost_estimate=pl.CostEstimate(
+            flops=2 * half * D * HIDDEN, bytes_accessed=10_000_000, transcendentals=0
+        ),
+    )(hidden, down, more)
 
 
 def joined_kernel(skip, own, other, gain, out):
@@ -355,7 +384,6 @@
 
 
 def joined(skip, own, other, gain):
-    other = swapped(other)
     return pl.pallas_call(
         joined_kernel,
         out_shape=jax.ShapeDtypeStruct(skip.shape, bf),
@@ -382,14 +410,14 @@
     near = []
     for c, order in enumerate(ORDERS):
         ring = around(parts[c], order[0])
-        near += placed(ring, order[0], [(0, parts[c].shape[-1])])
+        near += placed(ring, order[0], [(0, parts[c].shape[-1])], pltpu.VMEM)
     blocks = [[], [], []]
     for c, order in enumerate(ORDERS):
         ring = around(near[c], order[1])
         head, one, two = stage_widths(c)
-        (own,) = placed(ring, order[1], [(0, head)])
+        (own,) = placed(ring, order[1], [(0, head)], pltpu.VMEM)
         columns = [(head, one), (head + one, two), (head, one + two)]
-        *own_stages, own_both = placed(ring, order[1], columns)
+        *own_stages, own_both = placed(ring, order[1], columns, pltpu.HBM)
         blocks[0] += around(own, order[2])
         back = moved(own_both, order[2], 3)
         for s, own in enumerate(own_stages, 1):
@@ -401,10 +429,13 @@
         taps = conv_taps[:, c * CHANNELS : (c + 1) * CHANNELS]
         mixed.append(mixer(order, tokens, tokens_other, taps, blocks[0][4 * c : 4 * c + 4]))
     own, other = mix_out_product(mixed, blocks[0])
+    other = swapped(other)
     first = joined(tokens, own, other, norm_first)
     first_other = swapped(first)
-    sums = feed(0, first, first_other, blocks[1])
-    own, other = feed(1, first, first_other, blocks[2], sums)
+    own, other = feed(0, first, first_other, blocks[1])
+    other, hidden, down = feed(1, first, first_other, blocks[2], other)
+    other = swapped(other)
+    own = finished(hidden, down, own)
     return joined(first, own, other, norm_second)
 
 

time: 221 us -> 218 us (0.986)
    ppermute x4, waiting for transfers between devices: 3.4 us -> 0.12 us  [swapped(): return lax.ppermute(x, 'tp', [(0, 1), (1, 0)])]
    pallas_call x9, Pallas kernels: 10.8 us -> 7.8 us  [placed(): pl.pallas_call(functools.partial(place_kernel, axis, columns), out_shape=...]
    pallas_call x3 -> x4, Pallas kernels: 28.2 us -> 29.7 us  [the longest x2 21.4 us: feed(): pl.pallas_call(functools.partial(feed_kernel, stage), out_shape=outs, in_...]
  transfers between devices with their start and end apart: 46 -> 46, of which waited for: 23 -> 23; matrix products, arithmetic and copies ran while one was open for 0% -> 0% of each run, Pallas kernels for 13% -> 14%
where the time goes in v4:
time: 218 us
  waiting for transfers between devices  97.6 us (45%)
  starting transfers between devices  66.7 us (31%)
  Pallas kernels  53.3 us (24%)
    ppermute x42, waiting for transfers between devices, moved(): return lax.ppermute(block, REP_FS_TP, ring_pairs(axis, step))  97.5 us
    ppermute x42, starting transfers between devices, moved(): return lax.ppermute(block, REP_FS_TP, ring_pairs(axis, step))  64.7 us
    pallas_call x2, Pallas kernels, feed(): pl.pallas_call(functools.partial(feed_kernel, stage), out_shape=outs, in_...  21.4 us
    pallas_call x3, Pallas kernels, mixer(): pl.pallas_call(functools.partial(mixer_kernel, order), out_shape=jax.Shap...  10.6 us
    pallas_call x9, Pallas kernels, placed(): pl.pallas_call(functools.partial(place_kernel, axis, columns), out_shape=...  7.8 us
    pallas_call x1, Pallas kernels, mix_out_product(): pl.pallas_call(mix_out_kernel, out_shape=[pltpu.VMEM((rows // 2, D), jnp....  5.05 us
  transfers between devices with their start and end apart: 46, of which 23 were waited for; matrix products, arithmetic and copies ran while one was open for 0% of the time, Pallas kernels for 14%

profile of v4, /device:TPU:1, one launch (start us, length us, event | category | flops | bytes accessed | tf_op | source)
XLA Modules:
  0.0 218.1 jit_solution(9188801951002249670)
XLA Ops:
  1.3 3.6 %collective-permute-start.19 = (bf16[32,2304]{1,0:T(8,128)(2,1)S(1)}, bf16[32,2304]{1,0:T(8,128)(2,1)S(1)}, u32[]{:S(2)}, u32[]{:S(2)}) collective-permute-start(bf16[32,2304]{1,0:T(8,128)(2,1)S(1)} %get-tuple-element.26.refs_0_), channel_id=1, source_target_pairs={{0,8},{1,25},{2,10},{3,27},{4,12},{5,29},{6,14},{7,31},{8,16},{9,1... | collective-permute-start | bytes 442376 | tf_op jit(solution)/shard_map/ppermute | solution.py:69
  7.4 3.4 %collective-permute-start.20 = (bf16[32,2304]{1,0:T(8,128)(2,1)S(1)}, bf16[32,2304]{1,0:T(8,128)(2,1)S(1)}, u32[]{:S(2)}, u32[]{:S(2)}) collective-permute-start(bf16[32,2304]{1,0:T(8,128)(2,1)S(1)} %collective-permute-done.19.refs_1_), channel_id=1, source_target_pairs={{0,8},{1,25},{2,10},{3,27},{4,12},{5,29},{6,14},{7,31},{8,16},{9,1... | collective-permute-start | bytes 442376 | tf_op jit(solution)/shard_map/ppermute | solution.py:69
  13.7 3.7 %collective-permute-start.22 = (bf16[4,32,2304]{2,1,0:T(8,128)(2,1)S(1)}, bf16[4,32,2304]{2,1,0:T(8,128)(2,1)S(1)}, u32[]{:S(2)}, u32[]{:S(2)}) collective-permute-start(bf16[4,32,2304]{2,1,0:T(8,128)(2,1)S(1)} %shard_map.107.refs_0_), channel_id=1, source_target_pairs={{0,32},{1,97},{2,34},{3,99},{4,36},{5,101},{6,38},{7,103},{8,40},{... | collective-permute-start | bytes 1769480 | tf_op jit(solution)/shard_map/ppermute | solution.py:69
  22.0 3.4 %collective-permute-start.11 = (bf16[32,2432]{1,0:T(8,128)(2,1)S(1)}, bf16[32,2432]{1,0:T(8,128)(2,1)S(1)}, u32[]{:S(2)}, u32[]{:S(2)}) collective-permute-start(bf16[32,2432]{1,0:T(8,128)(2,1)S(1)} %collective-permute-done.10.refs_1_), channel_id=1, source_target_pairs={{0,2},{1,7},{2,4},{3,1},{4,6},{5,3},{6,0},{7,5},{8,10},{9,15},{10,... | collective-permute-start | bytes 466952 | tf_op jit(solution)/shard_map/ppermute | solution.py:69
  28.4 4.8 %collective-permute-start.13 = (bf16[4,32,2432]{2,1,0:T(8,128)(2,1)S(1)}, bf16[4,32,2432]{2,1,0:T(8,128)(2,1)S(1)}, u32[]{:S(2)}, u32[]{:S(2)}) collective-permute-start(bf16[4,32,2432]{2,1,0:T(8,128)(2,1)S(1)} %shard_map.104.refs_0_), channel_id=1, source_target_pairs={{0,8},{1,25},{2,10},{3,27},{4,12},{5,29},{6,14},{7,31},{8,16},{9,1... | collective-permute-start | bytes 1867784 | tf_op jit(solution)/shard_map/ppermute | solution.py:69
  40.2 3.6 %collective-permute-start.4 = (bf16[4,32,2432]{2,1,0:T(8,128)(2,1)S(1)}, bf16[4,32,2432]{2,1,0:T(8,128)(2,1)S(1)}, u32[]{:S(2)}, u32[]{:S(2)}) collective-permute-start(bf16[4,32,2432]{2,1,0:T(8,128)(2,1)S(1)} %shard_map.101.refs_0_), channel_id=1, source_target_pairs={{0,2},{1,7},{2,4},{3,1},{4,6},{5,3},{6,0},{7,5},{8,10},{9,15},{10,... | collective-permute-start | bytes 1867784 | tf_op jit(solution)/shard_map/ppermute | solution.py:69
  43.8 3.4 %collective-permute-start.23 = (bf16[4,32,2304]{2,1,0:T(8,128)(2,1)S(1)}, bf16[4,32,2304]{2,1,0:T(8,128)(2,1)S(1)}, u32[]{:S(2)}, u32[]{:S(2)}) collective-permute-start(bf16[4,32,2304]{2,1,0:T(8,128)(2,1)S(1)} %collective-permute-done.22.refs_1_), channel_id=1, source_target_pairs={{0,32},{1,97},{2,34},{3,99},{4,36},{5,101},{6,38},{7,103},{8,40},{... | collective-permute-start | bytes 1769480 | tf_op jit(solution)/shard_map/ppermute | solution.py:69
  54.5 9.0 %collective-permute-done.15.refs_3_ = bf16[4,32,2432]{2,1,0:T(8,128)(2,1)S(1)} collective-permute-done((bf16[4,32,2432]{2,1,0:T(8,128)(2,1)S(1)}, bf16[4,32,2432]{2,1,0:T(8,128)(2,1)S(1)}, u32[]{:S(2)}, u32[]{:S(2)}) %collective-permute-start.15) | collective-permute-done | bytes 622624 | tf_op jit(solution)/shard_map/ppermute | solution.py:69
  68.2 18.7 %collective-permute-done.25.refs_1_.refs_12_ = bf16[4,4,32,1024]{3,2,1,0:T(8,128)(2,1)S(1)} collective-permute-done((bf16[4,4,32,1024]{3,2,1,0:T(8,128)(2,1)S(1)}, bf16[4,4,32,1024]{3,2,1,0:T(8,128)(2,1)S(1)}, u32[]{:S(2)}, u32[]{:S(2)}) %collective-permute-start.25) | collective-permute-done | bytes 1048608 | tf_op jit(solution)/shard_map/ppermute | solution.py:69
  87.9 4.7 %collective-permute-start.17 = (bf16[4,4,32,1024]{3,2,1,0:T(8,128)(2,1)S(1)}, bf16[4,4,32,1024]{3,2,1,0:T(8,128)(2,1)S(1)}, u32[]{:S(2)}, u32[]{:S(2)}) collective-permute-start(bf16[4,4,32,1024]{3,2,1,0:T(8,128)(2,1)S(1)} %collective-permute-done.16.refs_1_.refs_8_), channel_id=1, source_target_pairs={{0,32},{1,97},{2,34},{3,99},{4,36},{5,101},{6,38},{7,103},{8,40},{... | collective-permute-start | bytes 3145736 | tf_op jit(solution)/shard_map/ppermute | solution.py:69
  95.2 8.6 %collective-permute-done.26.refs_2_.refs_13_ = bf16[4,4,32,1024]{3,2,1,0:T(8,128)(2,1)S(1)} collective-permute-done((bf16[4,4,32,1024]{3,2,1,0:T(8,128)(2,1)S(1)}, bf16[4,4,32,1024]{3,2,1,0:T(8,128)(2,1)S(1)}, u32[]{:S(2)}, u32[]{:S(2)}) %collective-permute-start.26) | collective-permute-done | bytes 1048608 | tf_op jit(solution)/shard_map/ppermute | solution.py:69
  103.8 3.5 %shard_map.109.refs_2_ = bf16[768,256]{1,0:T(8,128)(2,1)S(1)} custom-call(bf16[384,2048]{1,0:T(8,128)(2,1)S(1)} %copy-done, bf16[384,2048]{1,0:T(8,128)(2,1)S(1)} %collective-permute-done.other, f32[3,256]{1,0:T(4,128)S(1)} %get-tuple-element.43.taps, bf16[4,4,32,1024]{3,2,1,0:T(8,128)(2,1)S(1)} %shard_map.108.refs_0_.refs_11_, ...), custom_call_target="tpu_custom_call" | custom-call | flops 2415919104 | bytes 8000000 | tf_op jit(solution)/shard_map/pallas_call | solution.py:204
  107.3 5.5 %collective-permute-done.18.refs_3_.refs_10_ = bf16[4,4,32,1024]{3,2,1,0:T(8,128)(2,1)S(1)} collective-permute-done((bf16[4,4,32,1024]{3,2,1,0:T(8,128)(2,1)S(1)}, bf16[4,4,32,1024]{3,2,1,0:T(8,128)(2,1)S(1)}, u32[]{:S(2)}, u32[]{:S(2)}) %collective-permute-start.18) | collective-permute-done | bytes 1048608 | tf_op jit(solution)/shard_map/ppermute | solution.py:69
  115.2 3.5 %shard_map.106.refs_1_ = bf16[768,256]{1,0:T(8,128)(2,1)S(1)} custom-call(bf16[384,2048]{1,0:T(8,128)(2,1)S(1)} %copy-done, bf16[384,2048]{1,0:T(8,128)(2,1)S(1)} %collective-permute-done.other, f32[3,256]{1,0:T(4,128)S(1)} %get-tuple-element.45.taps, bf16[4,4,32,1024]{3,2,1,0:T(8,128)(2,1)S(1)} %shard_map.105.refs_0_.refs_7_, ...), custom_call_target="tpu_custom_call" | custom-call | flops 2415919104 | bytes 8000000 | tf_op jit(solution)/shard_map/pallas_call | solution.py:204
  118.7 3.6 %shard_map.103.refs_0_ = bf16[768,256]{1,0:T(8,128)(2,1)S(1)} custom-call(bf16[384,2048]{1,0:T(8,128)(2,1)S(1)} %copy-done, bf16[384,2048]{1,0:T(8,128)(2,1)S(1)} %collective-permute-done.other, f32[3,256]{1,0:T(4,128)S(1)} %get-tuple-element.44.taps, bf16[4,4,32,1024]{3,2,1,0:T(8,128)(2,1)S(1)} %shard_map.102.refs_0_.refs_3_, ...), custom_call_target="tpu_custom_call" | custom-call | flops 2415919104 | bytes 8000000 | tf_op jit(solution)/shard_map/pallas_call | solution.py:204
  122.3 5.0 %shard_map.110 = (f32[384,2048]{1,0:T(8,128)S(1)}, bf16[384,2048]{1,0:T(8,128)(2,1)S(1)}) custom-call(bf16[768,256]{1,0:T(8,128)(2,1)S(1)} %shard_map.103.refs_0_, bf16[768,256]{1,0:T(8,128)(2,1)S(1)} %shard_map.106.refs_1_, bf16[768,256]{1,0:T(8,128)(2,1)S(1)} %shard_map.109.refs_2_, bf16[4,4,32,1024]{3,2,1,0:T(8,128)(2,1)S(1)} %shard_map.102.refs_0_.refs_3_, ...), custom_call_target="tpu_custom_call" | custom-call | flops 2415919104 | bytes 9000000 | tf_op jit(solution)/shard_map/pallas_call | solution.py:252
  142.3 5.1 %collective-permute-done.36.refs_9_ = bf16[4,4,32,640]{3,2,1,0:T(8,128)(2,1)S(1)} collective-permute-done((bf16[4,4,32,640]{3,2,1,0:T(8,128)(2,1)}, bf16[4,4,32,640]{3,2,1,0:T(8,128)(2,1)S(1)}, u32[]{:S(2)}, u32[]{:S(2)}) %collective-permute-start.36) | collective-permute-done | bytes 655392 | tf_op jit(solution)/shard_map/ppermute | solution.py:69
  152.4 4.2 %collective-permute-done.39.refs_1_ = bf16[4,4,32,640]{3,2,1,0:T(8,128)(2,1)S(1)} collective-permute-done((bf16[4,4,32,640]{3,2,1,0:T(8,128)(2,1)}, bf16[4,4,32,640]{3,2,1,0:T(8,128)(2,1)S(1)}, u32[]{:S(2)}, u32[]{:S(2)}) %collective-permute-start.39) | collective-permute-done | bytes 655392 | tf_op jit(solution)/shard_map/ppermute | solution.py:69
  160.1 13.8 %collective-permute-done.44.refs_10_ = bf16[4,4,32,640]{3,2,1,0:T(8,128)(2,1)S(1)} collective-permute-done((bf16[4,4,32,640]{3,2,1,0:T(8,128)(2,1)S(1)}, bf16[4,4,32,640]{3,2,1,0:T(8,128)(2,1)S(1)}, u32[]{:S(2)}, u32[]{:S(2)}) %collective-permute-start.44) | collective-permute-done | bytes 655392 | tf_op jit(solution)/shard_map/ppermute | solution.py:69
  178.7 8.3 %collective-permute-done.40.refs_2_ = bf16[4,4,32,640]{3,2,1,0:T(8,128)(2,1)S(1)} collective-permute-done((bf16[4,4,32,640]{3,2,1,0:T(8,128)(2,1)S(1)}, bf16[4,4,32,640]{3,2,1,0:T(8,128)(2,1)S(1)}, u32[]{:S(2)}, u32[]{:S(2)}) %collective-permute-start.40) | collective-permute-done | bytes 655392 | tf_op jit(solution)/shard_map/ppermute | solution.py:69
  187.0 3.1 %collective-permute-start.31 = (bf16[4,4,32,768]{3,2,1,0:T(8,128)(2,1)S(1)}, bf16[4,4,32,768]{3,2,1,0:T(8,128)(2,1)S(1)}, u32[]{:S(2)}, u32[]{:S(2)}) collective-permute-start(bf16[4,4,32,768]{3,2,1,0:T(8,128)(2,1)S(1)} %collective-permute-done.30.refs_1_), channel_id=1, source_target_pairs={{0,8},{1,25},{2,10},{3,27},{4,12},{5,29},{6,14},{7,31},{8,16},{9,1... | collective-permute-start | bytes 2359304 | tf_op jit(solution)/shard_map/ppermute | solution.py:69
  190.6 11.4 %shard_map.115 = (f32[384,2048]{1,0:T(8,128)S(1)}, f32[384,2048]{1,0:T(8,128)S(1)}) custom-call(bf16[384,2048]{1,0:T(8,128)(2,1)S(1)} %shard_map.111.first_own.skip, bf16[384,2048]{1,0:T(8,128)(2,1)S(1)} %collective-permute-done.29.first_other, bf16[4,4,32,640]{3,2,1,0:T(8,128)(2,1)S(1)} %copy-done.8, ...), custom_call_target="tpu_custom_call" | custom-call | flops 6442450944 | bytes 20000000 | tf_op jit(solution)/shard_map/pallas_call | solution.py:340
  202.1 10.0 %shard_map.116 = (bf16[384,2048]{1,0:T(8,128)(2,1)S(1)}, bf16[384,1024]{1,0:T(8,128)(2,1)S(1)}, bf16[2,4,4,2,32,1024]{5,4,3,2,1,0:T(8,128)(2,1)S(1)}) custom-call(bf16[384,2048]{1,0:T(8,128)(2,1)S(1)} %shard_map.111.first_own.skip, bf16[384,2048]{1,0:T(8,128)(2,1)S(1)} %collective-permute-done.29.first_other, bf16[4,4,32,768]{3,2,1,0:T(8,128)(2,1)S(1)} %copy-done.3, ...), custom_call_target="tpu_custom_call" | custom-call | flops 4831838208 | bytes 20000000 | tf_op jit(solution)/shard_map/pallas_call | solution.py:340
  212.2 3.3 %shard_map.117.own = f32[384,2048]{1,0:T(8,128)S(1)} custom-call(bf16[384,1024]{1,0:T(8,128)(2,1)S(1)} %get-tuple-element.39.hidden, bf16[2,4,4,2,32,1024]{5,4,3,2,1,0:T(8,128)(2,1)S(1)} %get-tuple-element.40.down, f32[384,2048]{1,0:T(8,128)S(1)} %get-tuple-element.41.more), custom_call_target="tpu_custom_call" | custom-call | flops 1610612736 | bytes 10000000 | tf_op jit(solution)/shard_map/pallas_call | solution.py:361
  (114 shorter events, 70.4 us)
Async XLA Ops:
  13.7 30.1 %collective-permute-start.22 = (bf16[4,32,2304]{2,1,0:T(8,128)(2,1)S(1)}, bf16[4,32,2304]{2,1,0:T(8,128)(2,1)S(1)}, u32[]{:S(2)}, u32[]{:S(2)}) collective-permute-start(bf16[4,32,2304]{2,1,0:T(8,128)(2,1)S(1)} %shard_map.107.refs_0_), channel_id=1, source_target_pairs={{0,32},{1,97},{2,34},{3,99},{4,36},{5,101},{6,38},{7,103},{8,40},{... | collective-permute-start | bytes 1769480 | tf_op jit(solution)/shard_map/ppermute | solution.py:69
  28.4 18.7 %collective-permute-start.13 = (bf16[4,32,2432]{2,1,0:T(8,128)(2,1)S(1)}, bf16[4,32,2432]{2,1,0:T(8,128)(2,1)S(1)}, u32[]{:S(2)}, u32[]{:S(2)}) collective-permute-start(bf16[4,32,2432]{2,1,0:T(8,128)(2,1)S(1)} %shard_map.104.refs_0_), channel_id=1, source_target_pairs={{0,8},{1,25},{2,10},{3,27},{4,12},{5,29},{6,14},{7,31},{8,16},{9,1... | collective-permute-start | bytes 1867784 | tf_op jit(solution)/shard_map/ppermute | solution.py:69
  47.2 16.3 %collective-permute-start.15 = (bf16[4,32,2432]{2,1,0:T(8,128)(2,1)S(1)}, bf16[4,32,2432]{2,1,0:T(8,128)(2,1)S(1)}, u32[]{:S(2)}, u32[]{:S(2)}) collective-permute-start(bf16[4,32,2432]{2,1,0:T(8,128)(2,1)S(1)} %shard_map.104.refs_0_), channel_id=1, source_target_pairs={{0,24},{1,9},{2,26},{3,11},{4,28},{5,13},{6,30},{7,15},{8,0},{9,17... | collective-permute-start | bytes 1867784 | tf_op jit(solution)/shard_map/ppermute | solution.py:69
  47.2 16.3 %collective-permute-start.14 = (bf16[4,32,2432]{2,1,0:T(8,128)(2,1)S(1)}, bf16[4,32,2432]{2,1,0:T(8,128)(2,1)S(1)}, u32[]{:S(2)}, u32[]{:S(2)}) collective-permute-start(bf16[4,32,2432]{2,1,0:T(8,128)(2,1)S(1)} %collective-permute-done.13.refs_1_), channel_id=1, source_target_pairs={{0,8},{1,25},{2,10},{3,27},{4,12},{5,29},{6,14},{7,31},{8,16},{9,1... | collective-permute-start | bytes 1867784 | tf_op jit(solution)/shard_map/ppermute | solution.py:69
  49.9 38.0 %collective-permute-start = (bf16[384,2048]{1,0:T(8,128)(2,1)S(1)}, bf16[384,2048]{1,0:T(8,128)(2,1)S(1)}, u32[]{:S(2)}, u32[]{:S(2)}) collective-permute-start(bf16[384,2048]{1,0:T(8,128)(2,1)S(1)} %copy-done), channel_id=1, source_target_pairs={{0,1},{1,0},{2,3},{3,2},{4,5},{5,4},{6,7},{7,6},{8,9},{9,8},{10,11... | collective-permute-start | bytes 4718600 | tf_op jit(solution)/shard_map/ppermute | solution.py:78
  63.5 23.4 %collective-permute-start.25 = (bf16[4,4,32,1024]{3,2,1,0:T(8,128)(2,1)S(1)}, bf16[4,4,32,1024]{3,2,1,0:T(8,128)(2,1)S(1)}, u32[]{:S(2)}, u32[]{:S(2)}) collective-permute-start(bf16[4,4,32,1024]{3,2,1,0:T(8,128)(2,1)S(1)} %shard_map.108.refs_0_.refs_11_), channel_id=1, source_target_pairs={{0,2},{1,7},{2,4},{3,1},{4,6},{5,3},{6,0},{7,5},{8,10},{9,15},{10,... | collective-permute-start | bytes 3145736 | tf_op jit(solution)/shard_map/ppermute | solution.py:69
  63.6 24.2 %collective-permute-start.16 = (bf16[4,4,32,1024]{3,2,1,0:T(8,128)(2,1)S(1)}, bf16[4,4,32,1024]{3,2,1,0:T(8,128)(2,1)S(1)}, u32[]{:S(2)}, u32[]{:S(2)}) collective-permute-start(bf16[4,4,32,1024]{3,2,1,0:T(8,128)(2,1)S(1)} %shard_map.105.refs_0_.refs_7_), channel_id=1, source_target_pairs={{0,32},{1,97},{2,34},{3,99},{4,36},{5,101},{6,38},{7,103},{8,40},{... | collective-permute-start | bytes 3145736 | tf_op jit(solution)/shard_map/ppermute | solution.py:69
  64.5 28.0 %collective-permute-start.27 = (bf16[4,4,32,1024]{3,2,1,0:T(8,128)(2,1)S(1)}, bf16[4,4,32,1024]{3,2,1,0:T(8,128)(2,1)S(1)}, u32[]{:S(2)}, u32[]{:S(2)}) collective-permute-start(bf16[4,4,32,1024]{3,2,1,0:T(8,128)(2,1)S(1)} %shard_map.108.refs_0_.refs_11_), channel_id=1, source_target_pairs={{0,6},{1,3},{2,0},{3,5},{4,2},{5,7},{6,4},{7,1},{8,14},{9,11},{10,... | collective-permute-start | bytes 3145736 | tf_op jit(solution)/shard_map/ppermute | solution.py:69
  68.1 24.4 %collective-permute-start.7 = (bf16[4,4,32,1024]{3,2,1,0:T(8,128)(2,1)S(1)}, bf16[4,4,32,1024]{3,2,1,0:T(8,128)(2,1)S(1)}, u32[]{:S(2)}, u32[]{:S(2)}) collective-permute-start(bf16[4,4,32,1024]{3,2,1,0:T(8,128)(2,1)S(1)} %shard_map.102.refs_0_.refs_3_), channel_id=1, source_target_pairs={{0,8},{1,25},{2,10},{3,27},{4,12},{5,29},{6,14},{7,31},{8,16},{9,1... | collective-permute-start | bytes 3145736 | tf_op jit(solution)/shard_map/ppermute | solution.py:69
  86.9 16.9 %collective-permute-start.26 = (bf16[4,4,32,1024]{3,2,1,0:T(8,128)(2,1)S(1)}, bf16[4,4,32,1024]{3,2,1,0:T(8,128)(2,1)S(1)}, u32[]{:S(2)}, u32[]{:S(2)}) collective-permute-start(bf16[4,4,32,1024]{3,2,1,0:T(8,128)(2,1)S(1)} %collective-permute-done.25.refs_1_.refs_12_), channel_id=1, source_target_pairs={{0,2},{1,7},{2,4},{3,1},{4,6},{5,3},{6,0},{7,5},{8,10},{9,15},{10,... | collective-permute-start | bytes 3145736 | tf_op jit(solution)/shard_map/ppermute | solution.py:69
  87.9 25.0 %collective-permute-start.18 = (bf16[4,4,32,1024]{3,2,1,0:T(8,128)(2,1)S(1)}, bf16[4,4,32,1024]{3,2,1,0:T(8,128)(2,1)S(1)}, u32[]{:S(2)}, u32[]{:S(2)}) collective-permute-start(bf16[4,4,32,1024]{3,2,1,0:T(8,128)(2,1)S(1)} %shard_map.105.refs_0_.refs_7_), channel_id=1, source_target_pairs={{0,96},{1,33},{2,98},{3,35},{4,100},{5,37},{6,102},{7,39},{8,104},... | collective-permute-start | bytes 3145736 | tf_op jit(solution)/shard_map/ppermute | solution.py:69
  87.9 27.3 %collective-permute-start.17 = (bf16[4,4,32,1024]{3,2,1,0:T(8,128)(2,1)S(1)}, bf16[4,4,32,1024]{3,2,1,0:T(8,128)(2,1)S(1)}, u32[]{:S(2)}, u32[]{:S(2)}) collective-permute-start(bf16[4,4,32,1024]{3,2,1,0:T(8,128)(2,1)S(1)} %collective-permute-done.16.refs_1_.refs_8_), channel_id=1, source_target_pairs={{0,32},{1,97},{2,34},{3,99},{4,36},{5,101},{6,38},{7,103},{8,40},{... | collective-permute-start | bytes 3145736 | tf_op jit(solution)/shard_map/ppermute | solution.py:69
  92.5 26.2 %collective-permute-start.9 = (bf16[4,4,32,1024]{3,2,1,0:T(8,128)(2,1)S(1)}, bf16[4,4,32,1024]{3,2,1,0:T(8,128)(2,1)S(1)}, u32[]{:S(2)}, u32[]{:S(2)}) collective-permute-start(bf16[4,4,32,1024]{3,2,1,0:T(8,128)(2,1)S(1)} %shard_map.102.refs_0_.refs_3_), channel_id=1, source_target_pairs={{0,24},{1,9},{2,26},{3,11},{4,28},{5,13},{6,30},{7,15},{8,0},{9,17... | collective-permute-start | bytes 3145736 | tf_op jit(solution)/shard_map/ppermute | solution.py:69
  92.5 26.2 %collective-permute-start.8 = (bf16[4,4,32,1024]{3,2,1,0:T(8,128)(2,1)S(1)}, bf16[4,4,32,1024]{3,2,1,0:T(8,128)(2,1)S(1)}, u32[]{:S(2)}, u32[]{:S(2)}) collective-permute-start(bf16[4,4,32,1024]{3,2,1,0:T(8,128)(2,1)S(1)} %collective-permute-done.7.refs_1_.refs_4_), channel_id=1, source_target_pairs={{0,8},{1,25},{2,10},{3,27},{4,12},{5,29},{6,14},{7,31},{8,16},{9,1... | collective-permute-start | bytes 3145736 | tf_op jit(solution)/shard_map/ppermute | solution.py:69
  127.3 22.9 %collective-permute-start.28 = (bf16[384,2048]{1,0:T(8,128)(2,1)S(1)}, bf16[384,2048]{1,0:T(8,128)(2,1)S(1)}, u32[]{:S(2)}, u32[]{:S(2)}) collective-permute-start(bf16[384,2048]{1,0:T(8,128)(2,1)S(1)} %get-tuple-element.28), channel_id=1, source_target_pairs={{0,1},{1,0},{2,3},{3,2},{4,5},{5,4},{6,7},{7,6},{8,9},{9,8},{10,11... | collective-permute-start | bytes 4718600 | tf_op jit(solution)/shard_map/ppermute | solution.py:78
  130.5 17.0 %collective-permute-start.36 = (bf16[4,4,32,640]{3,2,1,0:T(8,128)(2,1)}, bf16[4,4,32,640]{3,2,1,0:T(8,128)(2,1)S(1)}, u32[]{:S(2)}, u32[]{:S(2)}) collective-permute-start(bf16[4,4,32,640]{3,2,1,0:T(8,128)(2,1)} %get-tuple-element.33.refs_8_), channel_id=1, source_target_pairs={{0,2},{1,7},{2,4},{3,1},{4,6},{5,3},{6,0},{7,5},{8,10},{9,15},{10,... | collective-permute-start | bytes 1966088 | tf_op jit(solution)/shard_map/ppermute | solution.py:69
  133.6 24.2 %collective-permute-start.41 = (bf16[4,4,32,768]{3,2,1,0:T(8,128)(2,1)}, bf16[4,4,32,768]{3,2,1,0:T(8,128)(2,1)S(1)}, u32[]{:S(2)}, u32[]{:S(2)}) collective-permute-start(bf16[4,4,32,768]{3,2,1,0:T(8,128)(2,1)} %get-tuple-element.36.refs_4_), channel_id=1, source_target_pairs={{0,32},{1,97},{2,34},{3,99},{4,36},{5,101},{6,38},{7,103},{8,40},{... | collective-permute-start | bytes 2359304 | tf_op jit(solution)/shard_map/ppermute | solution.py:69
  138.1 20.5 %collective-permute-start.30 = (bf16[4,4,32,768]{3,2,1,0:T(8,128)(2,1)}, bf16[4,4,32,768]{3,2,1,0:T(8,128)(2,1)S(1)}, u32[]{:S(2)}, u32[]{:S(2)}) collective-permute-start(bf16[4,4,32,768]{3,2,1,0:T(8,128)(2,1)} %get-tuple-element.29.refs_0_), channel_id=1, source_target_pairs={{0,8},{1,25},{2,10},{3,27},{4,12},{5,29},{6,14},{7,31},{8,16},{9,1... | collective-permute-start | bytes 2359304 | tf_op jit(solution)/shard_map/ppermute | solution.py:69
  140.4 16.1 %collective-permute-start.39 = (bf16[4,4,32,640]{3,2,1,0:T(8,128)(2,1)}, bf16[4,4,32,640]{3,2,1,0:T(8,128)(2,1)S(1)}, u32[]{:S(2)}, u32[]{:S(2)}) collective-permute-start(bf16[4,4,32,640]{3,2,1,0:T(8,128)(2,1)} %get-tuple-element.35.refs_0_), channel_id=1, source_target_pairs={{0,8},{1,25},{2,10},{3,27},{4,12},{5,29},{6,14},{7,31},{8,16},{9,1... | collective-permute-start | bytes 1966088 | tf_op jit(solution)/shard_map/ppermute | solution.py:69
  150.2 25.6 %collective-permute-start.38 = (bf16[4,4,32,1280]{3,2,1,0:T(8,128)(2,1)S(1)}, bf16[4,4,32,1280]{3,2,1,0:T(8,128)(2,1)S(1)}, u32[]{:S(2)}, u32[]{:S(2)}) collective-permute-start(bf16[4,4,32,1280]{3,2,1,0:T(8,128)(2,1)S(1)} %copy-done.12), channel_id=1, source_target_pairs={{0,6},{1,3},{2,0},{3,5},{4,2},{5,7},{6,4},{7,1},{8,14},{9,11},{10,... | collective-permute-start | bytes 3932168 | tf_op jit(solution)/shard_map/ppermute | solution.py:69
  156.5 34.1 %collective-permute-start.29 = (bf16[384,2048]{1,0:T(8,128)(2,1)S(1)}, bf16[384,2048]{1,0:T(8,128)(2,1)S(1)}, u32[]{:S(2)}, u32[]{:S(2)}) collective-permute-start(bf16[384,2048]{1,0:T(8,128)(2,1)S(1)} %shard_map.111.first_own.skip), channel_id=1, source_target_pairs={{0,1},{1,0},{2,3},{3,2},{4,5},{5,4},{6,7},{7,6},{8,9},{9,8},{10,11... | collective-permute-start | bytes 4718600 | tf_op jit(solution)/shard_map/ppermute | solution.py:78
  157.8 32.4 %collective-permute-start.32 = (bf16[4,4,32,1408]{3,2,1,0:T(8,128)(2,1)S(1)}, bf16[4,4,32,1408]{3,2,1,0:T(8,128)(2,1)S(1)}, u32[]{:S(2)}, u32[]{:S(2)}) collective-permute-start(bf16[4,4,32,1408]{3,2,1,0:T(8,128)(2,1)S(1)} %copy-done.11), channel_id=1, source_target_pairs={{0,24},{1,9},{2,26},{3,11},{4,28},{5,13},{6,30},{7,15},{8,0},{9,17... | collective-permute-start | bytes 4325384 | tf_op jit(solution)/shard_map/ppermute | solution.py:69
  157.8 32.3 %collective-permute-start.35 = (bf16[4,4,32,1408]{3,2,1,0:T(8,128)(2,1)S(1)}, bf16[4,4,32,1408]{3,2,1,0:T(8,128)(2,1)S(1)}, u32[]{:S(2)}, u32[]{:S(2)}) collective-permute-start(bf16[4,4,32,1408]{3,2,1,0:T(8,128)(2,1)S(1)} %copy-done.10), channel_id=1, source_target_pairs={{0,96},{1,33},{2,98},{3,35},{4,100},{5,37},{6,102},{7,39},{8,104},... | collective-permute-start | bytes 4325384 | tf_op jit(solution)/shard_map/ppermute | solution.py:69
  158.6 15.3 %collective-permute-start.44 = (bf16[4,4,32,640]{3,2,1,0:T(8,128)(2,1)S(1)}, bf16[4,4,32,640]{3,2,1,0:T(8,128)(2,1)S(1)}, u32[]{:S(2)}, u32[]{:S(2)}) collective-permute-start(bf16[4,4,32,640]{3,2,1,0:T(8,128)(2,1)S(1)} %collective-permute-done.43.refs_9_), channel_id=1, source_target_pairs={{0,2},{1,7},{2,4},{3,1},{4,6},{5,3},{6,0},{7,5},{8,10},{9,15},{10,... | collective-permute-start | bytes 1966088 | tf_op jit(solution)/shard_map/ppermute | solution.py:69
  (35 other events, 558.7 us)

commit v5 on v4

--- a/solution.py
+++ b/solution.py
@@ -370,25 +370,41 @@
     )(hidden, down, more)
 
 
-def joined_kernel(skip, own, other, gain, out):
+def joined_kernel(skip, own, other, gain, out, *scratch):
+    size = out.shape[0] // 3
+
+    def leaving(i, rows):
+        held, sems = scratch
+        return pltpu.make_async_copy(held.at[rows], out.at[rows], sems.at[i])
+
     def step(i, _):
-        rows = pl.ds(pl.multiple_of(i * 128, 128), 128)
+        rows = pl.ds(pl.multiple_of(i * size, size), size)
         values = residual_scale * skip[rows].astype(jnp.float32)
         values = values + (own[rows] + other[rows].astype(jnp.float32))
         center = values - jnp.mean(values, axis=-1, keepdims=True)
         spread = jnp.mean(center * center, axis=-1, keepdims=True)
-        out[rows] = (center * lax.rsqrt(spread + norm_epsilon) * gain[...]).astype(bf)
+        normed = (center * lax.rsqrt(spread + norm_epsilon) * gain[...]).astype(bf)
+        if scratch:
+            scratch[0][rows] = normed
+            leaving(i, rows).start()
+        else:
+            out[rows] = normed
         return 0
 
-    lax.fori_loop(0, out.shape[0] // 128, step, 0)
-
-
-def joined(skip, own, other, gain):
+    lax.fori_loop(0, 3, step, 0)
+    if scratch:
+        for i in range(3):
+            leaving(i, pl.ds(i * size, size)).wait()
+
+
+def joined(skip, own, other, gain, last):
+    scratch = [pltpu.VMEM(skip.shape, bf), pltpu.SemaphoreType.DMA((3,))]
     return pl.pallas_call(
         joined_kernel,
         out_shape=jax.ShapeDtypeStruct(skip.shape, bf),
         in_specs=[VMEM] * 4,
-        out_specs=VMEM,
+        out_specs=HBM if last else VMEM,
+        scratch_shapes=scratch if last else [],
         compiler_params=limit(16),
     )(skip, own, other, gain.reshape(1, -1))
 
@@ -430,13 +446,13 @@
         mixed.append(mixer(order, tokens, tokens_other, taps, blocks[0][4 * c : 4 * c + 4]))
     own, other = mix_out_product(mixed, blocks[0])
     other = swapped(other)
-    first = joined(tokens, own, other, norm_first)
+    first = joined(tokens, own, other, norm_first, False)
     first_other = swapped(first)
     own, other = feed(0, first, first_other, blocks[1])
     other, hidden, down = feed(1, first, first_other, blocks[2], other)
     other = swapped(other)
     own = finished(hidden, down, own)
-    return joined(first, own, other, norm_second)
+    return joined(first, own, other, norm_second, True)
 
 
 def solution(mesh):

time: 218 us -> 218 us (level)
  no operation moved by 1% of the time
where the time goes in v5:
time: 218 us
  waiting for transfers between devices  97.6 us (45%)
  starting transfers between devices  66.7 us (31%)
  Pallas kernels  52.9 us (24%)
    ppermute x42, waiting for transfers between devices, moved(): return lax.ppermute(block, REP_FS_TP, ring_pairs(axis, step))  97.5 us
    ppermute x42, starting transfers between devices, moved(): return lax.ppermute(block, REP_FS_TP, ring_pairs(axis, step))  64.7 us
    pallas_call x2, Pallas kernels, feed(): pl.pallas_call(functools.partial(feed_kernel, stage), out_shape=outs, in_...  21.4 us
    pallas_call x3, Pallas kernels, mixer(): pl.pallas_call(functools.partial(mixer_kernel, order), out_shape=jax.Shap...  10.6 us
    pallas_call x9, Pallas kernels, placed(): pl.pallas_call(functools.partial(place_kernel, axis, columns), out_shape=...  7.8 us
    pallas_call x1, Pallas kernels, mix_out_product(): pl.pallas_call(mix_out_kernel, out_shape=[pltpu.VMEM((rows // 2, D), jnp....  5.05 us
  transfers between devices with their start and end apart: 46, of which 23 were waited for; matrix products, arithmetic and copies ran while one was open for 0% of the time, Pallas kernels for 14%

profile of v5, /device:TPU:1, one launch (start us, length us, event | category | flops | bytes accessed | tf_op | source)
XLA Modules:
  0.0 217.9 jit_solution(9626088845515526862)
XLA Ops:
  1.3 3.6 %collective-permute-start.19 = (bf16[32,2304]{1,0:T(8,128)(2,1)S(1)}, bf16[32,2304]{1,0:T(8,128)(2,1)S(1)}, u32[]{:S(2)}, u32[]{:S(2)}) collective-permute-start(bf16[32,2304]{1,0:T(8,128)(2,1)S(1)} %get-tuple-element.26.refs_0_), channel_id=1, source_target_pairs={{0,8},{1,25},{2,10},{3,27},{4,12},{5,29},{6,14},{7,31},{8,16},{9,1... | collective-permute-start | bytes 442376 | tf_op jit(solution)/shard_map/ppermute | solution.py:69
  7.4 3.4 %collective-permute-start.20 = (bf16[32,2304]{1,0:T(8,128)(2,1)S(1)}, bf16[32,2304]{1,0:T(8,128)(2,1)S(1)}, u32[]{:S(2)}, u32[]{:S(2)}) collective-permute-start(bf16[32,2304]{1,0:T(8,128)(2,1)S(1)} %collective-permute-done.19.refs_1_), channel_id=1, source_target_pairs={{0,8},{1,25},{2,10},{3,27},{4,12},{5,29},{6,14},{7,31},{8,16},{9,1... | collective-permute-start | bytes 442376 | tf_op jit(solution)/shard_map/ppermute | solution.py:69
  13.7 3.7 %collective-permute-start.22 = (bf16[4,32,2304]{2,1,0:T(8,128)(2,1)S(1)}, bf16[4,32,2304]{2,1,0:T(8,128)(2,1)S(1)}, u32[]{:S(2)}, u32[]{:S(2)}) collective-permute-start(bf16[4,32,2304]{2,1,0:T(8,128)(2,1)S(1)} %shard_map.107.refs_0_), channel_id=1, source_target_pairs={{0,32},{1,97},{2,34},{3,99},{4,36},{5,101},{6,38},{7,103},{8,40},{... | collective-permute-start | bytes 1769480 | tf_op jit(solution)/shard_map/ppermute | solution.py:69
  22.0 3.4 %collective-permute-start.11 = (bf16[32,2432]{1,0:T(8,128)(2,1)S(1)}, bf16[32,2432]{1,0:T(8,128)(2,1)S(1)}, u32[]{:S(2)}, u32[]{:S(2)}) collective-permute-start(bf16[32,2432]{1,0:T(8,128)(2,1)S(1)} %collective-permute-done.10.refs_1_), channel_id=1, source_target_pairs={{0,2},{1,7},{2,4},{3,1},{4,6},{5,3},{6,0},{7,5},{8,10},{9,15},{10,... | collective-permute-start | bytes 466952 | tf_op jit(solution)/shard_map/ppermute | solution.py:69
  28.4 4.8 %collective-permute-start.13 = (bf16[4,32,2432]{2,1,0:T(8,128)(2,1)S(1)}, bf16[4,32,2432]{2,1,0:T(8,128)(2,1)S(1)}, u32[]{:S(2)}, u32[]{:S(2)}) collective-permute-start(bf16[4,32,2432]{2,1,0:T(8,128)(2,1)S(1)} %shard_map.104.refs_0_), channel_id=1, source_target_pairs={{0,8},{1,25},{2,10},{3,27},{4,12},{5,29},{6,14},{7,31},{8,16},{9,1... | collective-permute-start | bytes 1867784 | tf_op jit(solution)/shard_map/ppermute | solution.py:69
  40.2 3.6 %collective-permute-start.4 = (bf16[4,32,2432]{2,1,0:T(8,128)(2,1)S(1)}, bf16[4,32,2432]{2,1,0:T(8,128)(2,1)S(1)}, u32[]{:S(2)}, u32[]{:S(2)}) collective-permute-start(bf16[4,32,2432]{2,1,0:T(8,128)(2,1)S(1)} %shard_map.101.refs_0_), channel_id=1, source_target_pairs={{0,2},{1,7},{2,4},{3,1},{4,6},{5,3},{6,0},{7,5},{8,10},{9,15},{10,... | collective-permute-start | bytes 1867784 | tf_op jit(solution)/shard_map/ppermute | solution.py:69
  43.8 3.4 %collective-permute-start.23 = (bf16[4,32,2304]{2,1,0:T(8,128)(2,1)S(1)}, bf16[4,32,2304]{2,1,0:T(8,128)(2,1)S(1)}, u32[]{:S(2)}, u32[]{:S(2)}) collective-permute-start(bf16[4,32,2304]{2,1,0:T(8,128)(2,1)S(1)} %collective-permute-done.22.refs_1_), channel_id=1, source_target_pairs={{0,32},{1,97},{2,34},{3,99},{4,36},{5,101},{6,38},{7,103},{8,40},{... | collective-permute-start | bytes 1769480 | tf_op jit(solution)/shard_map/ppermute | solution.py:69
  54.5 9.0 %collective-permute-done.15.refs_3_ = bf16[4,32,2432]{2,1,0:T(8,128)(2,1)S(1)} collective-permute-done((bf16[4,32,2432]{2,1,0:T(8,128)(2,1)S(1)}, bf16[4,32,2432]{2,1,0:T(8,128)(2,1)S(1)}, u32[]{:S(2)}, u32[]{:S(2)}) %collective-permute-start.15) | collective-permute-done | bytes 622624 | tf_op jit(solution)/shard_map/ppermute | solution.py:69
  68.2 18.7 %collective-permute-done.25.refs_1_.refs_12_ = bf16[4,4,32,1024]{3,2,1,0:T(8,128)(2,1)S(1)} collective-permute-done((bf16[4,4,32,1024]{3,2,1,0:T(8,128)(2,1)S(1)}, bf16[4,4,32,1024]{3,2,1,0:T(8,128)(2,1)S(1)}, u32[]{:S(2)}, u32[]{:S(2)}) %collective-permute-start.25) | collective-permute-done | bytes 1048608 | tf_op jit(solution)/shard_map/ppermute | solution.py:69
  87.9 4.7 %collective-permute-start.17 = (bf16[4,4,32,1024]{3,2,1,0:T(8,128)(2,1)S(1)}, bf16[4,4,32,1024]{3,2,1,0:T(8,128)(2,1)S(1)}, u32[]{:S(2)}, u32[]{:S(2)}) collective-permute-start(bf16[4,4,32,1024]{3,2,1,0:T(8,128)(2,1)S(1)} %collective-permute-done.16.refs_1_.refs_8_), channel_id=1, source_target_pairs={{0,32},{1,97},{2,34},{3,99},{4,36},{5,101},{6,38},{7,103},{8,40},{... | collective-permute-start | bytes 3145736 | tf_op jit(solution)/shard_map/ppermute | solution.py:69
  95.2 8.6 %collective-permute-done.26.refs_2_.refs_13_ = bf16[4,4,32,1024]{3,2,1,0:T(8,128)(2,1)S(1)} collective-permute-done((bf16[4,4,32,1024]{3,2,1,0:T(8,128)(2,1)S(1)}, bf16[4,4,32,1024]{3,2,1,0:T(8,128)(2,1)S(1)}, u32[]{:S(2)}, u32[]{:S(2)}) %collective-permute-start.26) | collective-permute-done | bytes 1048608 | tf_op jit(solution)/shard_map/ppermute | solution.py:69
  103.8 3.5 %shard_map.109.refs_2_ = bf16[768,256]{1,0:T(8,128)(2,1)S(1)} custom-call(bf16[384,2048]{1,0:T(8,128)(2,1)S(1)} %copy-done, bf16[384,2048]{1,0:T(8,128)(2,1)S(1)} %collective-permute-done.other, f32[3,256]{1,0:T(4,128)S(1)} %get-tuple-element.43.taps, bf16[4,4,32,1024]{3,2,1,0:T(8,128)(2,1)S(1)} %shard_map.108.refs_0_.refs_11_, ...), custom_call_target="tpu_custom_call" | custom-call | flops 2415919104 | bytes 8000000 | tf_op jit(solution)/shard_map/pallas_call | solution.py:204
  107.3 5.5 %collective-permute-done.18.refs_3_.refs_10_ = bf16[4,4,32,1024]{3,2,1,0:T(8,128)(2,1)S(1)} collective-permute-done((bf16[4,4,32,1024]{3,2,1,0:T(8,128)(2,1)S(1)}, bf16[4,4,32,1024]{3,2,1,0:T(8,128)(2,1)S(1)}, u32[]{:S(2)}, u32[]{:S(2)}) %collective-permute-start.18) | collective-permute-done | bytes 1048608 | tf_op jit(solution)/shard_map/ppermute | solution.py:69
  115.2 3.5 %shard_map.106.refs_1_ = bf16[768,256]{1,0:T(8,128)(2,1)S(1)} custom-call(bf16[384,2048]{1,0:T(8,128)(2,1)S(1)} %copy-done, bf16[384,2048]{1,0:T(8,128)(2,1)S(1)} %collective-permute-done.other, f32[3,256]{1,0:T(4,128)S(1)} %get-tuple-element.45.taps, bf16[4,4,32,1024]{3,2,1,0:T(8,128)(2,1)S(1)} %shard_map.105.refs_0_.refs_7_, ...), custom_call_target="tpu_custom_call" | custom-call | flops 2415919104 | bytes 8000000 | tf_op jit(solution)/shard_map/pallas_call | solution.py:204
  118.7 3.6 %shard_map.103.refs_0_ = bf16[768,256]{1,0:T(8,128)(2,1)S(1)} custom-call(bf16[384,2048]{1,0:T(8,128)(2,1)S(1)} %copy-done, bf16[384,2048]{1,0:T(8,128)(2,1)S(1)} %collective-permute-done.other, f32[3,256]{1,0:T(4,128)S(1)} %get-tuple-element.44.taps, bf16[4,4,32,1024]{3,2,1,0:T(8,128)(2,1)S(1)} %shard_map.102.refs_0_.refs_3_, ...), custom_call_target="tpu_custom_call" | custom-call | flops 2415919104 | bytes 8000000 | tf_op jit(solution)/shard_map/pallas_call | solution.py:204
  122.3 5.0 %shard_map.110 = (f32[384,2048]{1,0:T(8,128)S(1)}, bf16[384,2048]{1,0:T(8,128)(2,1)S(1)}) custom-call(bf16[768,256]{1,0:T(8,128)(2,1)S(1)} %shard_map.103.refs_0_, bf16[768,256]{1,0:T(8,128)(2,1)S(1)} %shard_map.106.refs_1_, bf16[768,256]{1,0:T(8,128)(2,1)S(1)} %shard_map.109.refs_2_, bf16[4,4,32,1024]{3,2,1,0:T(8,128)(2,1)S(1)} %shard_map.102.refs_0_.refs_3_, ...), custom_call_target="tpu_custom_call" | custom-call | flops 2415919104 | bytes 9000000 | tf_op jit(solution)/shard_map/pallas_call | solution.py:252
  142.3 5.1 %collective-permute-done.36.refs_9_ = bf16[4,4,32,640]{3,2,1,0:T(8,128)(2,1)S(1)} collective-permute-done((bf16[4,4,32,640]{3,2,1,0:T(8,128)(2,1)}, bf16[4,4,32,640]{3,2,1,0:T(8,128)(2,1)S(1)}, u32[]{:S(2)}, u32[]{:S(2)}) %collective-permute-start.36) | collective-permute-done | bytes 655392 | tf_op jit(solution)/shard_map/ppermute | solution.py:69
  152.4 4.2 %collective-permute-done.39.refs_1_ = bf16[4,4,32,640]{3,2,1,0:T(8,128)(2,1)S(1)} collective-permute-done((bf16[4,4,32,640]{3,2,1,0:T(8,128)(2,1)}, bf16[4,4,32,640]{3,2,1,0:T(8,128)(2,1)S(1)}, u32[]{:S(2)}, u32[]{:S(2)}) %collective-permute-start.39) | collective-permute-done | bytes 655392 | tf_op jit(solution)/shard_map/ppermute | solution.py:69
  160.1 13.8 %collective-permute-done.44.refs_10_ = bf16[4,4,32,640]{3,2,1,0:T(8,128)(2,1)S(1)} collective-permute-done((bf16[4,4,32,640]{3,2,1,0:T(8,128)(2,1)S(1)}, bf16[4,4,32,640]{3,2,1,0:T(8,128)(2,1)S(1)}, u32[]{:S(2)}, u32[]{:S(2)}) %collective-permute-start.44) | collective-permute-done | bytes 655392 | tf_op jit(solution)/shard_map/ppermute | solution.py:69
  178.7 8.3 %collective-permute-done.40.refs_2_ = bf16[4,4,32,640]{3,2,1,0:T(8,128)(2,1)S(1)} collective-permute-done((bf16[4,4,32,640]{3,2,1,0:T(8,128)(2,1)S(1)}, bf16[4,4,32,640]{3,2,1,0:T(8,128)(2,1)S(1)}, u32[]{:S(2)}, u32[]{:S(2)}) %collective-permute-start.40) | collective-permute-done | bytes 655392 | tf_op jit(solution)/shard_map/ppermute | solution.py:69
  187.0 3.1 %collective-permute-start.31 = (bf16[4,4,32,768]{3,2,1,0:T(8,128)(2,1)S(1)}, bf16[4,4,32,768]{3,2,1,0:T(8,128)(2,1)S(1)}, u32[]{:S(2)}, u32[]{:S(2)}) collective-permute-start(bf16[4,4,32,768]{3,2,1,0:T(8,128)(2,1)S(1)} %collective-permute-done.30.refs_1_), channel_id=1, source_target_pairs={{0,8},{1,25},{2,10},{3,27},{4,12},{5,29},{6,14},{7,31},{8,16},{9,1... | collective-permute-start | bytes 2359304 | tf_op jit(solution)/shard_map/ppermute | solution.py:69
  190.6 11.4 %shard_map.115 = (f32[384,2048]{1,0:T(8,128)S(1)}, f32[384,2048]{1,0:T(8,128)S(1)}) custom-call(bf16[384,2048]{1,0:T(8,128)(2,1)S(1)} %shard_map.111.first_own.skip, bf16[384,2048]{1,0:T(8,128)(2,1)S(1)} %collective-permute-done.29.first_other, bf16[4,4,32,640]{3,2,1,0:T(8,128)(2,1)S(1)} %copy-done.8, ...), custom_call_target="tpu_custom_call" | custom-call | flops 6442450944 | bytes 20000000 | tf_op jit(solution)/shard_map/pallas_call | solution.py:340
  202.1 10.0 %shard_map.116 = (bf16[384,2048]{1,0:T(8,128)(2,1)S(1)}, bf16[384,1024]{1,0:T(8,128)(2,1)S(1)}, bf16[2,4,4,2,32,1024]{5,4,3,2,1,0:T(8,128)(2,1)S(1)}) custom-call(bf16[384,2048]{1,0:T(8,128)(2,1)S(1)} %shard_map.111.first_own.skip, bf16[384,2048]{1,0:T(8,128)(2,1)S(1)} %collective-permute-done.29.first_other, bf16[4,4,32,768]{3,2,1,0:T(8,128)(2,1)S(1)} %copy-done.3, ...), custom_call_target="tpu_custom_call" | custom-call | flops 4831838208 | bytes 20000000 | tf_op jit(solution)/shard_map/pallas_call | solution.py:340
  212.2 3.3 %shard_map.117.own = f32[384,2048]{1,0:T(8,128)S(1)} custom-call(bf16[384,1024]{1,0:T(8,128)(2,1)S(1)} %get-tuple-element.39.hidden, bf16[2,4,4,2,32,1024]{5,4,3,2,1,0:T(8,128)(2,1)S(1)} %get-tuple-element.40.down, f32[384,2048]{1,0:T(8,128)S(1)} %get-tuple-element.41.more), custom_call_target="tpu_custom_call" | custom-call | flops 1610612736 | bytes 10000000 | tf_op jit(solution)/shard_map/pallas_call | solution.py:361
  (114 shorter events, 70.1 us)
Async XLA Ops:
  13.7 30.1 %collective-permute-start.22 = (bf16[4,32,2304]{2,1,0:T(8,128)(2,1)S(1)}, bf16[4,32,2304]{2,1,0:T(8,128)(2,1)S(1)}, u32[]{:S(2)}, u32[]{:S(2)}) collective-permute-start(bf16[4,32,2304]{2,1,0:T(8,128)(2,1)S(1)} %shard_map.107.refs_0_), channel_id=1, source_target_pairs={{0,32},{1,97},{2,34},{3,99},{4,36},{5,101},{6,38},{7,103},{8,40},{... | collective-permute-start | bytes 1769480 | tf_op jit(solution)/shard_map/ppermute | solution.py:69
  28.4 18.7 %collective-permute-start.13 = (bf16[4,32,2432]{2,1,0:T(8,128)(2,1)S(1)}, bf16[4,32,2432]{2,1,0:T(8,128)(2,1)S(1)}, u32[]{:S(2)}, u32[]{:S(2)}) collective-permute-start(bf16[4,32,2432]{2,1,0:T(8,128)(2,1)S(1)} %shard_map.104.refs_0_), channel_id=1, source_target_pairs={{0,8},{1,25},{2,10},{3,27},{4,12},{5,29},{6,14},{7,31},{8,16},{9,1... | collective-permute-start | bytes 1867784 | tf_op jit(solution)/shard_map/ppermute | solution.py:69
  47.2 16.3 %collective-permute-start.15 = (bf16[4,32,2432]{2,1,0:T(8,128)(2,1)S(1)}, bf16[4,32,2432]{2,1,0:T(8,128)(2,1)S(1)}, u32[]{:S(2)}, u32[]{:S(2)}) collective-permute-start(bf16[4,32,2432]{2,1,0:T(8,128)(2,1)S(1)} %shard_map.104.refs_0_), channel_id=1, source_target_pairs={{0,24},{1,9},{2,26},{3,11},{4,28},{5,13},{6,30},{7,15},{8,0},{9,17... | collective-permute-start | bytes 1867784 | tf_op jit(solution)/shard_map/ppermute | solution.py:69
  47.2 16.3 %collective-permute-start.14 = (bf16[4,32,2432]{2,1,0:T(8,128)(2,1)S(1)}, bf16[4,32,2432]{2,1,0:T(8,128)(2,1)S(1)}, u32[]{:S(2)}, u32[]{:S(2)}) collective-permute-start(bf16[4,32,2432]{2,1,0:T(8,128)(2,1)S(1)} %collective-permute-done.13.refs_1_), channel_id=1, source_target_pairs={{0,8},{1,25},{2,10},{3,27},{4,12},{5,29},{6,14},{7,31},{8,16},{9,1... | collective-permute-start | bytes 1867784 | tf_op jit(solution)/shard_map/ppermute | solution.py:69
  49.9 38.0 %collective-permute-start = (bf16[384,2048]{1,0:T(8,128)(2,1)S(1)}, bf16[384,2048]{1,0:T(8,128)(2,1)S(1)}, u32[]{:S(2)}, u32[]{:S(2)}) collective-permute-start(bf16[384,2048]{1,0:T(8,128)(2,1)S(1)} %copy-done), channel_id=1, source_target_pairs={{0,1},{1,0},{2,3},{3,2},{4,5},{5,4},{6,7},{7,6},{8,9},{9,8},{10,11... | collective-permute-start | bytes 4718600 | tf_op jit(solution)/shard_map/ppermute | solution.py:78
  63.5 23.4 %collective-permute-start.25 = (bf16[4,4,32,1024]{3,2,1,0:T(8,128)(2,1)S(1)}, bf16[4,4,32,1024]{3,2,1,0:T(8,128)(2,1)S(1)}, u32[]{:S(2)}, u32[]{:S(2)}) collective-permute-start(bf16[4,4,32,1024]{3,2,1,0:T(8,128)(2,1)S(1)} %shard_map.108.refs_0_.refs_11_), channel_id=1, source_target_pairs={{0,2},{1,7},{2,4},{3,1},{4,6},{5,3},{6,0},{7,5},{8,10},{9,15},{10,... | collective-permute-start | bytes 3145736 | tf_op jit(solution)/shard_map/ppermute | solution.py:69
  63.6 24.2 %collective-permute-start.16 = (bf16[4,4,32,1024]{3,2,1,0:T(8,128)(2,1)S(1)}, bf16[4,4,32,1024]{3,2,1,0:T(8,128)(2,1)S(1)}, u32[]{:S(2)}, u32[]{:S(2)}) collective-permute-start(bf16[4,4,32,1024]{3,2,1,0:T(8,128)(2,1)S(1)} %shard_map.105.refs_0_.refs_7_), channel_id=1, source_target_pairs={{0,32},{1,97},{2,34},{3,99},{4,36},{5,101},{6,38},{7,103},{8,40},{... | collective-permute-start | bytes 3145736 | tf_op jit(solution)/shard_map/ppermute | solution.py:69
  64.5 28.0 %collective-permute-start.27 = (bf16[4,4,32,1024]{3,2,1,0:T(8,128)(2,1)S(1)}, bf16[4,4,32,1024]{3,2,1,0:T(8,128)(2,1)S(1)}, u32[]{:S(2)}, u32[]{:S(2)}) collective-permute-start(bf16[4,4,32,1024]{3,2,1,0:T(8,128)(2,1)S(1)} %shard_map.108.refs_0_.refs_11_), channel_id=1, source_target_pairs={{0,6},{1,3},{2,0},{3,5},{4,2},{5,7},{6,4},{7,1},{8,14},{9,11},{10,... | collective-permute-start | bytes 3145736 | tf_op jit(solution)/shard_map/ppermute | solution.py:69
  68.1 24.4 %collective-permute-start.7 = (bf16[4,4,32,1024]{3,2,1,0:T(8,128)(2,1)S(1)}, bf16[4,4,32,1024]{3,2,1,0:T(8,128)(2,1)S(1)}, u32[]{:S(2)}, u32[]{:S(2)}) collective-permute-start(bf16[4,4,32,1024]{3,2,1,0:T(8,128)(2,1)S(1)} %shard_map.102.refs_0_.refs_3_), channel_id=1, source_target_pairs={{0,8},{1,25},{2,10},{3,27},{4,12},{5,29},{6,14},{7,31},{8,16},{9,1... | collective-permute-start | bytes 3145736 | tf_op jit(solution)/shard_map/ppermute | solution.py:69
  86.9 16.9 %collective-permute-start.26 = (bf16[4,4,32,1024]{3,2,1,0:T(8,128)(2,1)S(1)}, bf16[4,4,32,1024]{3,2,1,0:T(8,128)(2,1)S(1)}, u32[]{:S(2)}, u32[]{:S(2)}) collective-permute-start(bf16[4,4,32,1024]{3,2,1,0:T(8,128)(2,1)S(1)} %collective-permute-done.25.refs_1_.refs_12_), channel_id=1, source_target_pairs={{0,2},{1,7},{2,4},{3,1},{4,6},{5,3},{6,0},{7,5},{8,10},{9,15},{10,... | collective-permute-start | bytes 3145736 | tf_op jit(solution)/shard_map/ppermute | solution.py:69
  87.9 25.0 %collective-permute-start.18 = (bf16[4,4,32,1024]{3,2,1,0:T(8,128)(2,1)S(1)}, bf16[4,4,32,1024]{3,2,1,0:T(8,128)(2,1)S(1)}, u32[]{:S(2)}, u32[]{:S(2)}) collective-permute-start(bf16[4,4,32,1024]{3,2,1,0:T(8,128)(2,1)S(1)} %shard_map.105.refs_0_.refs_7_), channel_id=1, source_target_pairs={{0,96},{1,33},{2,98},{3,35},{4,100},{5,37},{6,102},{7,39},{8,104},... | collective-permute-start | bytes 3145736 | tf_op jit(solution)/shard_map/ppermute | solution.py:69
  87.9 27.3 %collective-permute-start.17 = (bf16[4,4,32,1024]{3,2,1,0:T(8,128)(2,1)S(1)}, bf16[4,4,32,1024]{3,2,1,0:T(8,128)(2,1)S(1)}, u32[]{:S(2)}, u32[]{:S(2)}) collective-permute-start(bf16[4,4,32,1024]{3,2,1,0:T(8,128)(2,1)S(1)} %collective-permute-done.16.refs_1_.refs_8_), channel_id=1, source_target_pairs={{0,32},{1,97},{2,34},{3,99},{4,36},{5,101},{6,38},{7,103},{8,40},{... | collective-permute-start | bytes 3145736 | tf_op jit(solution)/shard_map/ppermute | solution.py:69
  92.5 26.2 %collective-permute-start.9 = (bf16[4,4,32,1024]{3,2,1,0:T(8,128)(2,1)S(1)}, bf16[4,4,32,1024]{3,2,1,0:T(8,128)(2,1)S(1)}, u32[]{:S(2)}, u32[]{:S(2)}) collective-permute-start(bf16[4,4,32,1024]{3,2,1,0:T(8,128)(2,1)S(1)} %shard_map.102.refs_0_.refs_3_), channel_id=1, source_target_pairs={{0,24},{1,9},{2,26},{3,11},{4,28},{5,13},{6,30},{7,15},{8,0},{9,17... | collective-permute-start | bytes 3145736 | tf_op jit(solution)/shard_map/ppermute | solution.py:69
  92.5 26.2 %collective-permute-start.8 = (bf16[4,4,32,1024]{3,2,1,0:T(8,128)(2,1)S(1)}, bf16[4,4,32,1024]{3,2,1,0:T(8,128)(2,1)S(1)}, u32[]{:S(2)}, u32[]{:S(2)}) collective-permute-start(bf16[4,4,32,1024]{3,2,1,0:T(8,128)(2,1)S(1)} %collective-permute-done.7.refs_1_.refs_4_), channel_id=1, source_target_pairs={{0,8},{1,25},{2,10},{3,27},{4,12},{5,29},{6,14},{7,31},{8,16},{9,1... | collective-permute-start | bytes 3145736 | tf_op jit(solution)/shard_map/ppermute | solution.py:69
  127.3 22.9 %collective-permute-start.28 = (bf16[384,2048]{1,0:T(8,128)(2,1)S(1)}, bf16[384,2048]{1,0:T(8,128)(2,1)S(1)}, u32[]{:S(2)}, u32[]{:S(2)}) collective-permute-start(bf16[384,2048]{1,0:T(8,128)(2,1)S(1)} %get-tuple-element.28), channel_id=1, source_target_pairs={{0,1},{1,0},{2,3},{3,2},{4,5},{5,4},{6,7},{7,6},{8,9},{9,8},{10,11... | collective-permute-start | bytes 4718600 | tf_op jit(solution)/shard_map/ppermute | solution.py:78
  130.5 17.0 %collective-permute-start.36 = (bf16[4,4,32,640]{3,2,1,0:T(8,128)(2,1)}, bf16[4,4,32,640]{3,2,1,0:T(8,128)(2,1)S(1)}, u32[]{:S(2)}, u32[]{:S(2)}) collective-permute-start(bf16[4,4,32,640]{3,2,1,0:T(8,128)(2,1)} %get-tuple-element.33.refs_8_), channel_id=1, source_target_pairs={{0,2},{1,7},{2,4},{3,1},{4,6},{5,3},{6,0},{7,5},{8,10},{9,15},{10,... | collective-permute-start | bytes 1966088 | tf_op jit(solution)/shard_map/ppermute | solution.py:69
  133.6 24.2 %collective-permute-start.41 = (bf16[4,4,32,768]{3,2,1,0:T(8,128)(2,1)}, bf16[4,4,32,768]{3,2,1,0:T(8,128)(2,1)S(1)}, u32[]{:S(2)}, u32[]{:S(2)}) collective-permute-start(bf16[4,4,32,768]{3,2,1,0:T(8,128)(2,1)} %get-tuple-element.36.refs_4_), channel_id=1, source_target_pairs={{0,32},{1,97},{2,34},{3,99},{4,36},{5,101},{6,38},{7,103},{8,40},{... | collective-permute-start | bytes 2359304 | tf_op jit(solution)/shard_map/ppermute | solution.py:69
  138.1 20.5 %collective-permute-start.30 = (bf16[4,4,32,768]{3,2,1,0:T(8,128)(2,1)}, bf16[4,4,32,768]{3,2,1,0:T(8,128)(2,1)S(1)}, u32[]{:S(2)}, u32[]{:S(2)}) collective-permute-start(bf16[4,4,32,768]{3,2,1,0:T(8,128)(2,1)} %get-tuple-element.29.refs_0_), channel_id=1, source_target_pairs={{0,8},{1,25},{2,10},{3,27},{4,12},{5,29},{6,14},{7,31},{8,16},{9,1... | collective-permute-start | bytes 2359304 | tf_op jit(solution)/shard_map/ppermute | solution.py:69
  140.4 16.1 %collective-permute-start.39 = (bf16[4,4,32,640]{3,2,1,0:T(8,128)(2,1)}, bf16[4,4,32,640]{3,2,1,0:T(8,128)(2,1)S(1)}, u32[]{:S(2)}, u32[]{:S(2)}) collective-permute-start(bf16[4,4,32,640]{3,2,1,0:T(8,128)(2,1)} %get-tuple-element.35.refs_0_), channel_id=1, source_target_pairs={{0,8},{1,25},{2,10},{3,27},{4,12},{5,29},{6,14},{7,31},{8,16},{9,1... | collective-permute-start | bytes 1966088 | tf_op jit(solution)/shard_map/ppermute | solution.py:69
  150.2 25.6 %collective-permute-start.38 = (bf16[4,4,32,1280]{3,2,1,0:T(8,128)(2,1)S(1)}, bf16[4,4,32,1280]{3,2,1,0:T(8,128)(2,1)S(1)}, u32[]{:S(2)}, u32[]{:S(2)}) collective-permute-start(bf16[4,4,32,1280]{3,2,1,0:T(8,128)(2,1)S(1)} %copy-done.12), channel_id=1, source_target_pairs={{0,6},{1,3},{2,0},{3,5},{4,2},{5,7},{6,4},{7,1},{8,14},{9,11},{10,... | collective-permute-start | bytes 3932168 | tf_op jit(solution)/shard_map/ppermute | solution.py:69
  156.5 34.1 %collective-permute-start.29 = (bf16[384,2048]{1,0:T(8,128)(2,1)S(1)}, bf16[384,2048]{1,0:T(8,128)(2,1)S(1)}, u32[]{:S(2)}, u32[]{:S(2)}) collective-permute-start(bf16[384,2048]{1,0:T(8,128)(2,1)S(1)} %shard_map.111.first_own.skip), channel_id=1, source_target_pairs={{0,1},{1,0},{2,3},{3,2},{4,5},{5,4},{6,7},{7,6},{8,9},{9,8},{10,11... | collective-permute-start | bytes 4718600 | tf_op jit(solution)/shard_map/ppermute | solution.py:78
  157.8 32.4 %collective-permute-start.32 = (bf16[4,4,32,1408]{3,2,1,0:T(8,128)(2,1)S(1)}, bf16[4,4,32,1408]{3,2,1,0:T(8,128)(2,1)S(1)}, u32[]{:S(2)}, u32[]{:S(2)}) collective-permute-start(bf16[4,4,32,1408]{3,2,1,0:T(8,128)(2,1)S(1)} %copy-done.11), channel_id=1, source_target_pairs={{0,24},{1,9},{2,26},{3,11},{4,28},{5,13},{6,30},{7,15},{8,0},{9,17... | collective-permute-start | bytes 4325384 | tf_op jit(solution)/shard_map/ppermute | solution.py:69
  157.8 32.3 %collective-permute-start.35 = (bf16[4,4,32,1408]{3,2,1,0:T(8,128)(2,1)S(1)}, bf16[4,4,32,1408]{3,2,1,0:T(8,128)(2,1)S(1)}, u32[]{:S(2)}, u32[]{:S(2)}) collective-permute-start(bf16[4,4,32,1408]{3,2,1,0:T(8,128)(2,1)S(1)} %copy-done.10), channel_id=1, source_target_pairs={{0,96},{1,33},{2,98},{3,35},{4,100},{5,37},{6,102},{7,39},{8,104},... | collective-permute-start | bytes 4325384 | tf_op jit(solution)/shard_map/ppermute | solution.py:69
  158.6 15.3 %collective-permute-start.44 = (bf16[4,4,32,640]{3,2,1,0:T(8,128)(2,1)S(1)}, bf16[4,4,32,640]{3,2,1,0:T(8,128)(2,1)S(1)}, u32[]{:S(2)}, u32[]{:S(2)}) collective-permute-start(bf16[4,4,32,640]{3,2,1,0:T(8,128)(2,1)S(1)} %collective-permute-done.43.refs_9_), channel_id=1, source_target_pairs={{0,2},{1,7},{2,4},{3,1},{4,6},{5,3},{6,0},{7,5},{8,10},{9,15},{10,... | collective-permute-start | bytes 1966088 | tf_op jit(solution)/shard_map/ppermute | solution.py:69
  (35 other events, 558.7 us)
